TPU v7x, 128 devices: a whole 4x4x4 slice. The times are simulated.
128 devices in a mesh: sp: 16 (over z, y), tp: 8 (over x, core).
Axes of the slice: x: 4, y: 4, z: 4, core: 2. Of those that a mesh axis runs over, the one named last changes fastest.
Arguments:
- query_proj: bfloat16 [16384, 2048], P('sp', 'tp'), may hold values from -6 to 6
- key_proj: bfloat16 [16384, 2048], P('sp', 'tp'), may hold values from -6 to 6
- value_proj: bfloat16 [16384, 4096], P('sp', 'tp'), may hold values from -6 to 6
- gate_proj: bfloat16 [16384, 4096], P('sp', 'tp'), may hold values from -6 to 6
- log_decay: float32 [16384, 8], P('sp', 'tp'), may hold values from -0.75 to 0, as said below
- residual: bfloat16 [16384, 2048], P('sp'), may hold values from -4 to 4
- out_weight: bfloat16 [4096, 2048], P('tp'), may hold values from -0.09375 to 0.09375
- norm_gain: float32 [2, 2048], replicated, may hold values from 0.1 to 1.9
- norm_bias: float32 [2, 2048], replicated, may hold values from -1.5 to 1.5
- up_gate: bfloat16 [2048, 5632], P('sp', 'tp'), may hold values from -0.125 to 0.125
- up_value: bfloat16 [2048, 5632], P('sp', 'tp'), may hold values from -0.125 to 0.125
- conv_weight: float32 [2, 3, 5632], P(None, None, 'tp'), may hold values from -3 to 3
- conv_bias: float32 [2, 5632], P(None, 'tp'), may hold values from -1.5 to 1.5
- down_weight: bfloat16 [5632, 2048], P('tp', 'sp'), may hold values from -0.078125 to 0.078125
Outputs:
- layer_output: bfloat16 [16384, 2048], P(('sp', 'tp'))
Inputs may be any that keep to these rules, and one draw needn't show every extreme that they name: `log_decay`: all entries are negative.
All inputs are finite; a program needn't handle non-finite values.
Results may differ from a plain program's by a relative error of at most 0.023.
Values may be sent and summed in bfloat16 or wider, within the bound.
No kernel may reach another device: no remote copies, remote signals or barrier semaphores. Data moves between devices by JAX's collectives and lax.ppermute only.
A program may use at most 128 MiB of HBM per device.

v0:
```python
import functools

import jax
import jax.numpy as jnp
import numpy as np
from jax import lax
from jax.experimental import pallas as pl
from jax.experimental.pallas import tpu as pltpu
from jax.sharding import Mesh
from jax.sharding import PartitionSpec as P


BLOCK = 256
SP = ("z", "y")
TP = ("x", "c")
f32 = jnp.float32
bf16 = jnp.bfloat16

ALPHA = 8.0**0.25
ROPE_BASE = 10000.0
EPS = 1e-05
EXTRA = 16
HIGHEST = lax.Precision.HIGHEST


def ring(shift, size=4):
    return [(i, (i + shift) % size) for i in range(size)]


def shift_by(x, axis, by):
    return lax.ppermute(x, axis, ring(by))


def everyone(x, axis):
    return [x] + [shift_by(x, axis, d) for d in (1, 2, 3)]


def swap_cores(x):
    return lax.ppermute(x, "c", [(0, 1), (1, 0)])


def run(kernel, sc, args, outs, scratch=(), flops=0, limit=8, far=0, far_outs=0):
    near, away = pl.BlockSpec(memory_space=pltpu.VMEM), pl.BlockSpec(memory_space=pltpu.HBM)
    split, kept = len(args) - far, len(outs) - far_outs
    args = [pltpu.with_memory_space_constraint(a, pltpu.VMEM if i < split else pltpu.HBM) for i, a in enumerate(args)]
    spaces = [pltpu.VMEM] * kept + [pltpu.HBM] * far_outs
    return pl.pallas_call(
        kernel,
        in_specs=[pl.BlockSpec(memory_space=pltpu.SMEM)] + [near] * split + [away] * far,
        out_specs=[near] * kept + [away] * far_outs,
        out_shape=[space(shape, dtype) for space, (shape, dtype) in zip(spaces, outs)],
        scratch_shapes=scratch,
        cost_estimate=pl.CostEstimate(flops=flops, transcendentals=0, bytes_accessed=0),
        compiler_params=pltpu.CompilerParams(vmem_limit_bytes=limit << 20),
    )(sc, *args)


def trig_tables(half, rows, count):
    freq = ROPE_BASE ** (-2.0 * np.arange(half, dtype=np.float64) / (2 * half))
    low = np.arange(rows, dtype=np.float64)[:, None] * freq[None, :]
    high = rows * np.arange(count, dtype=np.float64)[:, None] * freq[None, :]
    return np.stack([np.cos(low), np.sin(low), np.cos(high), np.sin(high)]).astype(np.float32)


def angles(at, tables):
    high_cos, high_sin = tables[2, pl.ds(at, 1), :], tables[3, pl.ds(at, 1), :]
    cos = high_cos * tables[0] - high_sin * tables[1]
    return cos, high_sin * tables[0] + high_cos * tables[1]


def rotated(x, cos, sin):
    half = cos.shape[1]
    front, second = x[:, :half], x[:, half:]
    return jnp.concatenate([front * cos - second * sin, front * sin + second * cos], axis=1)


def triangle(n):
    r = lax.broadcasted_iota(jnp.int32, (n, n), 0)
    c = lax.broadcasted_iota(jnp.int32, (n, n), 1)
    return r >= c


def running_logs(row, lower):
    n = lower.shape[0]
    rows = jnp.broadcast_to(row, (8, n))
    tri = lower.astype(f32)
    down = lax.dot_general(tri, rows, (((1,), (1,)), ((), ())), precision=HIGHEST, preferred_element_type=f32)
    across = lax.dot_general(rows, tri, (((1,), (1,)), ((), ())), precision=HIGHEST, preferred_element_type=f32)
    return down[:, 0:1], across[0:1, :]


def log_rows(total, width):
    a = total.astype(bf16)
    b = (total - a.astype(f32)).astype(bf16)
    c = (total - a.astype(f32) - b.astype(f32)).astype(bf16)
    at = lax.broadcasted_iota(jnp.int32, (EXTRA, width), 0)
    pick = jnp.where(at == 0, a.astype(f32), jnp.where(at == 1, b.astype(f32), c.astype(f32)))
    return jnp.where(at < 3, pick, 0.0).astype(bf16)


def log_of(rows):
    return rows[0:1, 0:1] + rows[1:2, 0:1] + rows[2:3, 0:1]


def states_kernel(sc, log, k, v, tables, kr, cosine, sine, prefix, p0, p1, p2, p3, state):
    lower = triangle(BLOCK)
    state[...] = jnp.zeros_like(state)

    def step(b, _):
        at = pl.ds(pl.multiple_of(b * BLOCK, BLOCK), BLOCK)
        cum, _ = running_logs(log[:, at], lower)
        total = cum[BLOCK - 1 : BLOCK, :]
        span = tables.shape[1]
        for i in range(BLOCK // span):
            turn = angles((4 * sc[0] + sc[1]) * (tables.shape[1] // 16) + b * (BLOCK // span) + i, tables)
            here = pl.ds(pl.multiple_of(b * BLOCK + i * span, span), span)
            cosine[here, :], sine[here, :] = turn
        key = rotated(k[at, :].astype(f32), cosine[at, :], sine[at, :]) * k.shape[1] ** (-0.5)
        key = key.astype(bf16)
        kr[at, :] = key
        faded = (key.astype(f32) * jnp.exp(total - cum)).astype(bf16)
        add = lax.dot_general(faded, v[at, :], (((0,), (0,)), ((), ())), preferred_element_type=f32)
        prefix[b] = state[...].astype(bf16)
        state[...] = jnp.exp(total) * state[...] + add
        return 0

    lax.fori_loop(0, log.shape[1] // BLOCK, step, 0)
    everything = jnp.sum(log[...], axis=1, keepdims=True)
    tail = log_rows(everything, state.shape[1])
    rows = state.shape[0] // 4
    for d, out in enumerate((p0, p1, p2, p3)):
        at = pl.multiple_of(lax.rem(sc[1] + d, 4) * rows, rows)
        out[:rows] = state[pl.ds(at, rows), :].astype(bf16)
        out[rows:] = tail


def line_kernel(sc, r0, r1, r2, r3, total, entry, logs, pieces):
    rows = entry.shape[1]
    for d, r in enumerate((r0, r1, r2, r3)):
        pieces[lax.rem(sc[1] + 4 - d, 4)] = r[...]
    run = jnp.zeros(entry.shape[1:], f32)
    passed = jnp.zeros((1, 1), f32)
    for j in range(4):
        entry[j] = run
        logs[j : j + 1, :] = jnp.broadcast_to(passed, (1, logs.shape[1]))
        here = log_of(pieces[j, rows:].astype(f32))
        run = jnp.exp(here) * run + pieces[j, :rows].astype(f32)
        passed = passed + here
    total[:rows] = run.astype(bf16)
    total[rows:] = log_rows(passed, total.shape[1])


def incoming_kernel(sc, t1, t2, t3, entry, logs, o0, o1, o2, o3):
    rows = entry.shape[1]
    run = jnp.zeros(entry.shape[1:], f32)
    for d, t in ((3, t3), (2, t2), (1, t1)):
        new = jnp.exp(log_of(t[rows:].astype(f32))) * run + t[:rows].astype(f32)
        run = jnp.where(sc[0] >= d, new, run)
    for d, out in enumerate((o0, o1, o2, o3)):
        at = lax.rem(sc[1] + d, 4)
        fade = jnp.exp(logs[pl.ds(at, 1), 0:1])
        out[...] = (fade * run + entry[at]).astype(bf16)


def within_kernel(sc, log, kr, cosine, sine, prefix, q, v, within, scaled):
    lower = triangle(BLOCK)
    n = BLOCK // 4

    def step(b, _):
        at = pl.ds(pl.multiple_of(b * BLOCK, BLOCK), BLOCK)
        cum, across = running_logs(log[:, at], lower)
        query = rotated(q[at, :].astype(f32), cosine[at, :], sine[at, :]).astype(bf16)
        score = lax.dot_general(query, kr[at, :], (((1,), (1,)), ((), ())), preferred_element_type=f32)
        weight = jnp.where(lower, jnp.exp(jnp.where(lower, cum - across, 0.0)), 0.0)
        result = jnp.dot((score * weight).astype(bf16), v[at, :], preferred_element_type=f32)
        faded = (query.astype(f32) * jnp.exp(cum)).astype(bf16)
        result = result + jnp.dot(faded, prefix[b], preferred_element_type=f32)
        for i in range(4):
            to = pl.ds(pl.multiple_of((2 * b + i // 2) * n, n), n)
            within[i % 2, to, :] = result[i * n : (i + 1) * n]
            scaled[i % 2, to, :] = faded[i * n : (i + 1) * n]
        return 0

    lax.fori_loop(0, log.shape[1] // BLOCK, step, 0)


def heads_kernel(sc, log, i0, i1, i2, i3, within, scaled, gate, weight, keep, send, start, carried, chunk):
    rows = i0.shape[0]
    for d, piece in enumerate((i0, i1, i2, i3)):
        at = pl.multiple_of(lax.rem(sc[1] + 4 - d, 4) * rows, rows)
        start[pl.ds(at, rows), :] = piece[...]
    order = lax.broadcasted_iota(jnp.int32, log.shape, 1)
    n = keep.shape[1]
    south = sc[3] == 0
    carried[...] = jnp.dot(scaled[chunk], start[...], preferred_element_type=f32)
    gated = []
    for b in range(log.shape[1] // BLOCK):
        passed = jnp.sum(jnp.where(order < b * BLOCK, log[...], 0.0), axis=1, keepdims=True)
        at = slice(2 * b * n, 2 * (b + 1) * n)
        mixed = within[chunk, at, :] + jnp.exp(passed) * carried[at, :]
        centred = mixed - jnp.mean(mixed, axis=1, keepdims=True)
        spread = jnp.mean(centred * centred, axis=1, keepdims=True)
        g = jnp.concatenate([gate[2 * b, chunk], gate[2 * b + 1, chunk]], axis=0).astype(f32)
        gated.append((g * jax.nn.sigmoid(g) * (centred * lax.rsqrt(spread + EPS))).astype(bf16))
    gated = jnp.concatenate(gated, axis=0)
    place(keep, send, sc, south, lambda cols: jnp.dot(gated, weight[:, cols], preferred_element_type=f32))


def place(keep, send, sc, south, product, tile=512):
    n = keep.shape[1]
    for j in range(keep.shape[2] // tile):
        cols = slice(j * tile, (j + 1) * tile)
        part = product(cols).astype(bf16)
        for xx in range(4):
            lo, hi = part[2 * xx * n : (2 * xx + 1) * n], part[(2 * xx + 1) * n : (2 * xx + 2) * n]
            at = lax.rem(xx + 4 - sc[2], 4)
            keep[at, :, cols] = jnp.where(south, lo, hi)
            send[at, :, cols] = jnp.where(south, hi, lo)


def scatter_kernel(sc, keep, got, s1, s2, s3):
    for d, out in ((1, s1), (2, s2), (3, s3)):
        out[...] = (keep[d].astype(f32) + got[d].astype(f32)).astype(bf16)


def norm_kernel(sc, keep, got, r1, r2, r3, base, gain, shift, *rest, row, group):
    out, rows = rest[-1], keep.shape[1]
    total = keep[0].astype(f32) + got[0].astype(f32) + r1[...].astype(f32)
    total = total + r2[...].astype(f32) + r3[...].astype(f32)
    at = 0 if group is None else 4 * sc[2] + 2 * sc[3] + group
    total = total + ALPHA * base[at].astype(f32)
    centred = total - jnp.mean(total, axis=1, keepdims=True)
    spread = jnp.mean(centred * centred, axis=1, keepdims=True)
    if len(rest) > 1:
        out[rows:] = rest[0][...]
    out[:rows] = (
        centred * lax.rsqrt(spread + EPS) * gain[row : row + 1, :] + shift[row : row + 1, :]
    ).astype(bf16)


def reduce_and_norm(sc, keep, send, base, gain, shift, row, group, *after):
    _, rows, width = keep.shape
    piece = ((rows, width), bf16)
    got = swap_cores(send)
    size = rows * width
    sums = run(scatter_kernel, sc, (keep, got), [piece] * 3, flops=size * 400)
    far = [shift_by(s, "x", d) for d, s in zip((1, 2, 3), sums)]
    return run(
        functools.partial(norm_kernel, row=row, group=group),
        sc, (keep, got, *far, base, gain, shift, *after), [((rows * (1 + len(after)), width), bf16)], flops=size * 400,
    )[0]


def gather_rows(own):
    mine = everyone(own, "x")
    return mine + [swap_cores(m) for m in mine]


def opening_kernel(sc, *refs):
    sources, gate, value, down = refs[:5], *refs[5:8]
    homes, shard = refs[8:13], refs[13]
    gate_v, value_v, down_v, both, sems, weight_sems = refs[14:]
    loads = [
        pltpu.make_async_copy(src, dst, weight_sems.at[i])
        for i, (src, dst) in enumerate(((gate, gate_v), (value, value_v), (down, down_v)))
    ]
    moves = [pltpu.make_async_copy(src, dst, sems.at[i]) for i, (src, dst) in enumerate(zip(sources, homes))]
    for copy in loads + moves:
        copy.start()
    for copy in loads:
        copy.wait()
    parts = [r[...].astype(f32).T for r in (gate_v, value_v, down_v)]
    rest = both.shape[1] - sum(p.shape[1] for p in parts)
    both[...] = jnp.concatenate(parts + [jnp.zeros((both.shape[0], rest), f32)], axis=1).astype(bf16)
    out = pltpu.make_async_copy(both, shard, weight_sems.at[3])
    out.start()
    for copy in moves:
        copy.wait()
    out.wait()


def gather_into(sc, pieces, rows):
    n = pieces[0].shape[0]
    for i, piece in enumerate(pieces):
        core = sc[3] if i < 4 else 1 - sc[3]
        at = pl.multiple_of((2 * lax.rem(sc[2] + 4 - i % 4, 4) + core) * n, n)
        rows[pl.ds(at, n), :] = piece[...]


def first_up_kernel(sc, *refs):
    pieces, weight, out, up, down, rows, total, sems = refs[:8], *refs[8:]
    steps = sems.shape[0] - 1
    deep = up.shape[0] // steps
    parts = [slice(i * deep, (i + 1) * deep) for i in range(steps)]
    loads = [
        pltpu.make_async_copy(weight.at[p, pl.ds(0, up.shape[1])], up.at[p], sems.at[i]) for i, p in enumerate(parts)
    ]
    loads.append(pltpu.make_async_copy(weight.at[:, pl.ds(up.shape[1], down.shape[1])], down, sems.at[steps]))
    for load in loads:
        load.start()
    gather_into(sc, pieces, rows)
    for i, p in enumerate(parts):
        loads[i].wait()
        part = jnp.dot(rows[:, p], up[p, :], preferred_element_type=f32)
        if i == 0:
            total[...] = part
        elif i < steps - 1:
            total[...] += part
        else:
            out[...] = (total[...] + part).astype(bf16)
    loads[steps].wait()


def second_up_kernel(sc, *refs):
    pieces, weight, out, rows = refs[:8], *refs[8:]
    gather_into(sc, pieces, rows)
    out[...] = jnp.dot(rows[...], weight[...], preferred_element_type=f32).astype(bf16)


def first_up(sc, pieces, weights, hidden):
    n, width = pieces[0].shape
    return run(
        first_up_kernel, sc, (*pieces, weights),
        [((8 * n, hidden), bf16), ((width, hidden), bf16), ((width, weights.shape[1] - hidden), bf16)],
        scratch=[
            pltpu.VMEM((8 * n, width), bf16), pltpu.VMEM((8 * n, hidden), f32), pltpu.SemaphoreType.DMA((5,))
        ],
        flops=16 * n * width * hidden, limit=16, far=1,
    )


def second_up(sc, pieces, weights, hidden):
    n, width = pieces[0].shape
    return run(
        second_up_kernel, sc, (*pieces, weights), [((8 * n, hidden), bf16)],
        scratch=[pltpu.VMEM((8 * n, width), bf16)], flops=16 * n * width * hidden, limit=16,
    )[0]


def down_kernel(sc, mine, other, edge, taps, bias, weight, keep, send, active, padded, chunk):
    n = keep.shape[1]
    hidden = active.shape[1]

    def conv_group(t, _):
        at = pl.multiple_of(t * n, n)
        if chunk == 1:
            halo = other[pl.ds(pl.multiple_of(at + n - 16, 16), 16), :][8:]
        else:
            before = pl.multiple_of(jnp.maximum(at - 16, 0), 16)
            halo = jnp.where(t == 0, edge[8:].astype(f32), other[pl.ds(before, 16), :][8:].astype(f32))
        padded[0:8] = halo.astype(f32)
        padded[8:] = mine[pl.ds(at, n), :].astype(f32)
        conv = bias[0:1, :] + padded[6 : 6 + n] * taps[0:1, :]
        conv = conv + padded[7 : 7 + n] * taps[1:2, :]
        conv = conv + padded[8 : 8 + n] * taps[2:3, :]
        active[pl.ds(at, n), :] = (jax.nn.gelu(conv[:, :hidden]) * conv[:, hidden:]).astype(bf16)
        return 0

    lax.fori_loop(0, 8, conv_group, 0)
    place(keep, send, sc, sc[3] == 0, lambda cols: lax.dot_general(
        active[...], weight[cols, :hidden], (((1,), (1,)), ((), ())), preferred_element_type=f32
    ))


def down_project(sc, mine, other, edge, taps, bias, weights, width, chunk):
    rows, double = mine.shape
    n = rows // 8
    shape = ((4, n, width), bf16)
    return run(
        functools.partial(down_kernel, chunk=chunk), sc,
        (mine, other, edge, taps, bias, weights), [shape, shape],
        scratch=[pltpu.VMEM((rows, double // 2), bf16), pltpu.VMEM((n + 8, double), f32)],
        flops=rows * width * double * 2, limit=16,
    )


def shards(
    query_proj, key_proj, value_proj, gate_proj, log_decay, residual, out_weight, norm_gain,
    norm_bias, up_gate, up_value, conv_weight, conv_bias, down_weight,
):
    tok, dk = query_proj.shape
    dv = value_proj.shape[1]
    width = residual.shape[1]
    hidden = up_gate.shape[1]
    blocks = tok // BLOCK
    n = tok // 16
    taps = jnp.concatenate([conv_weight[0], conv_weight[1]], axis=1)
    bias = jnp.concatenate([conv_bias[0:1], conv_bias[1:2]], axis=1)
    sc = jnp.stack([lax.axis_index(a) for a in ("z", "y", "x", "c")]).astype(jnp.int32)

    tables = jnp.asarray(trig_tables(dk // 2, 128, 128))
    padded = -(-3 * hidden // 128) * 128
    near = (log_decay.T, query_proj, key_proj, value_proj, tables)
    column = ((hidden, up_gate.shape[0]), bf16)
    log, query, key, value, tables, shard = run(
        opening_kernel, sc, (*near, up_gate.T, up_value.T, down_weight),
        [(a.shape, a.dtype) for a in near] + [((up_gate.shape[0], padded), bf16)],
        scratch=[pltpu.VMEM(*column)] * 3
        + [pltpu.VMEM((up_gate.shape[0], padded), bf16), pltpu.SemaphoreType.DMA((5,)), pltpu.SemaphoreType.DMA((4,))],
        flops=1 << 26, far=8, far_outs=1,
    )
    weights = lax.all_gather(shard, SP, axis=0, tiled=True)
    piece = ((dk // 4 + EXTRA, dv), bf16)
    turn = ((tok, dk // 2), f32)
    key_rot, cosine, sine, prefix, *pieces = run(
        states_kernel, sc, (log, key, value, tables),
        [((tok, dk), bf16), turn, turn, ((blocks, dk, dv), bf16)] + [piece] * 4,
        scratch=[pltpu.VMEM((dk, dv), f32)], flops=4 * tok * dk * dv,
    )
    got = [pieces[0]] + [shift_by(pieces[d], "y", d) for d in (1, 2, 3)]
    within, scaled = run(
        within_kernel, sc, (log, key_rot, cosine, sine, prefix, query, value),
        [((2, tok // 2, dv), f32), ((2, tok // 2, dk), bf16)],
        flops=4 * tok * BLOCK * (dk + dv),
    )
    total, entry, logs = run(
        line_kernel, sc, got, [piece, ((4, dk // 4, dv), f32), ((8, 128), f32)],
        scratch=[pltpu.VMEM((4,) + piece[0], bf16)], flops=100 * dk * dv,
    )
    lines = everyone(total, "z")[1:]
    quarter = ((dk // 4, dv), bf16)
    outgoing = run(incoming_kernel, sc, (*lines, entry, logs), [quarter] * 4, flops=100 * dk * dv)
    incoming = [outgoing[0]] + [shift_by(outgoing[d], "y", d) for d in (1, 2, 3)]
    gates = gate_proj.reshape(8, 2, n, dv)
    bases = residual.reshape(16, n, width)
    normed, ups, rows = [None, None], [None, None], [None, None]
    for k in (1, 0):
        shape = ((4, n, width), bf16)
        keep, send = run(
            functools.partial(heads_kernel, chunk=k), sc,
            (log, *incoming, within, scaled, gates, out_weight), [shape, shape],
            scratch=[pltpu.VMEM((dk, dv), bf16), pltpu.VMEM((tok // 2, dv), f32)], flops=tok * dv * (dk + width),
        )
        normed[k] = reduce_and_norm(sc, keep, send, bases, norm_gain, norm_bias, 0, k)
        rows[k] = gather_rows(normed[k])
    ups[1], weights, down_weights = first_up(sc, rows[1], weights, 2 * hidden)
    ups[0] = second_up(sc, rows[0], weights, 2 * hidden)
    edge = lax.ppermute(ups[1][8 * n - 16 :], SP, [(i, i + 1) for i in range(15)])
    outs = [None, None]
    for k in (1, 0):
        keep, send = down_project(sc, ups[k], ups[1 - k], edge, taps, bias, down_weights, width, k)
        outs[k] = reduce_and_norm(sc, keep, send, normed[k][None], norm_gain, norm_bias, 1, None, *outs[k + 1 :])
    return outs[0]


def solution(mesh):
    torus = Mesh(mesh.devices.reshape(4, 4, 4, 2), SP + TP)
    return jax.shard_map(
        shards,
        mesh=torus,
        in_specs=(
            P(SP, TP),
            P(SP, TP),
            P(SP, TP),
            P(SP, TP),
            P(SP, TP),
            P(SP, None),
            P(TP, None),
            P(),
            P(),
            P(SP, TP),
            P(SP, TP),
            P(None, None, TP),
            P(None, TP),
            P(TP, SP),
        ),
        out_specs=P(SP + TP, None),
        check_vma=False,
    )
```

profile of v0, /device:TPU:0, one launch (start us, length us, event | category | flops | bytes accessed | tf_op | source)
XLA Modules:
  0.0 164.4 jit_solution(13433061578326203284)
XLA Ops:
  6.6 3.4 %shard_map.145 = (f32[1,1024]{1,0:T(1,128)S(1)}, bf16[1024,256]{1,0:T(8,128)(2,1)S(1)}, bf16[1024,256]{1,0:T(8,128)(2,1)S(1)}, bf16[1024,512]{1,0:T(8,128)(2,1)S...) custom-call(s32[4]{0:T(128)S(1)} %pad_add_fusion.sc, f32[1,1024]{1,0:T(1,128)} %bitcast.23, ...), custom_call_target="tpu_custom_call" | custom-call | flops 67108864 | tf_op jit(solution)/shard_map/pallas_call | solution.py:47
  10.0 4.0 %shard_map.146 = (bf16[1024,256]{1,0:T(8,128)(2,1)S(1)}, f32[1024,128]{1,0:T(8,128)S(1)}, f32[1024,128]{1,0:T(8,128)S(1)}, bf16[4,256,512]{2,1,0:T(8,128)(2,1)S(...) custom-call(s32[4]{0:T(128)S(1)} %pad_add_fusion.sc, ...), custom_call_target="tpu_custom_call" | custom-call | flops 536870912 | tf_op jit(solution)/shard_map/pallas_call | solution.py:47
  14.0 1.8 %collective-permute-start = (bf16[80,512]{1,0:T(8,128)(2,1)S(1)}, bf16[80,512]{1,0:T(8,128)(2,1)S(1)}, u32[]{:S(2)}, u32[]{:S(2)}) collective-permute-start(bf16[80,512]{1,0:T(8,128)(2,1)S(1)} %get-tuple-element.56), channel_id=1, source_target_pairs={{0,8},{8,16},{16,24},{24,0},{1,9},{9,17},{17,25},{25,1},{2,10},{10... | collective-permute-start | bytes 245768 | tf_op jit(solution)/shard_map/ppermute | solution.py:31
  15.8 2.9 %collective-permute-start.1 = (bf16[80,512]{1,0:T(8,128)(2,1)S(1)}, bf16[80,512]{1,0:T(8,128)(2,1)S(1)}, u32[]{:S(2)}, u32[]{:S(2)}) collective-permute-start(bf16[80,512]{1,0:T(8,128)(2,1)S(1)} %get-tuple-element.57), channel_id=1, source_target_pairs={{0,16},{8,24},{16,0},{24,8},{1,17},{9,25},{17,1},{25,9},{2,18},{10... | collective-permute-start | bytes 245768 | tf_op jit(solution)/shard_map/ppermute | solution.py:31
  18.7 1.3 collective-permute-start.2
  20.0 2.6 %collective-permute-done.1.r2 = bf16[80,512]{1,0:T(8,128)(2,1)S(1)} collective-permute-done((bf16[80,512]{1,0:T(8,128)(2,1)S(1)}, bf16[80,512]{1,0:T(8,128)(2,1)S(1)}, u32[]{:S(2)}, u32[]{:S(2)}) %collective-permute-start.1) | collective-permute-done | bytes 81952 | tf_op jit(solution)/shard_map/ppermute | solution.py:31
  22.6 0.5 collective-permute-done.2.r3
  23.1 0.7 shard_map.147
  23.8 2.0 %collective-permute-start.3 = (bf16[80,512]{1,0:T(8,128)(2,1)S(1)}, bf16[80,512]{1,0:T(8,128)(2,1)S(1)}, u32[]{:S(2)}, u32[]{:S(2)}) collective-permute-start(bf16[80,512]{1,0:T(8,128)(2,1)S(1)} %get-tuple-element.59), channel_id=1, source_target_pairs={{0,32},{32,64},{64,96},{96,0},{1,33},{33,65},{65,97},{97,1},{2,34}... | collective-permute-start | bytes 245768 | tf_op jit(solution)/shard_map/ppermute | solution.py:31
  25.8 3.6 %collective-permute-start.4 = (bf16[80,512]{1,0:T(8,128)(2,1)S(1)}, bf16[80,512]{1,0:T(8,128)(2,1)S(1)}, u32[]{:S(2)}, u32[]{:S(2)}) collective-permute-start(bf16[80,512]{1,0:T(8,128)(2,1)S(1)} %get-tuple-element.59), channel_id=1, source_target_pairs={{0,64},{32,96},{64,0},{96,32},{1,65},{33,97},{65,1},{97,33},{2,66}... | collective-permute-start | bytes 245768 | tf_op jit(solution)/shard_map/ppermute | solution.py:31
  29.4 1.0 collective-permute-start.5
  30.4 2.2 %collective-permute-done.3.t1 = bf16[80,512]{1,0:T(8,128)(2,1)S(1)} collective-permute-done((bf16[80,512]{1,0:T(8,128)(2,1)S(1)}, bf16[80,512]{1,0:T(8,128)(2,1)S(1)}, u32[]{:S(2)}, u32[]{:S(2)}) %collective-permute-start.3) | collective-permute-done | bytes 81952 | tf_op jit(solution)/shard_map/ppermute | solution.py:31
  32.6 4.1 %collective-permute-done.4.t2 = bf16[80,512]{1,0:T(8,128)(2,1)S(1)} collective-permute-done((bf16[80,512]{1,0:T(8,128)(2,1)S(1)}, bf16[80,512]{1,0:T(8,128)(2,1)S(1)}, u32[]{:S(2)}, u32[]{:S(2)}) %collective-permute-start.4) | collective-permute-done | bytes 81952 | tf_op jit(solution)/shard_map/ppermute | solution.py:31
  36.7 0.7 shard_map.148
  37.4 1.1 collective-permute-start.6
  38.5 3.3 %collective-permute-start.7 = (bf16[64,512]{1,0:T(8,128)(2,1)S(1)}, bf16[64,512]{1,0:T(8,128)(2,1)S(1)}, u32[]{:S(2)}, u32[]{:S(2)}) collective-permute-start(bf16[64,512]{1,0:T(8,128)(2,1)S(1)} %get-tuple-element.64), channel_id=1, source_target_pairs={{0,16},{8,24},{16,0},{24,8},{1,17},{9,25},{17,1},{25,9},{2,18},{10... | collective-permute-start | bytes 196616 | tf_op jit(solution)/shard_map/ppermute | solution.py:31
  41.8 0.6 collective-permute-start.8
  42.4 3.8 %shard_map.149 = (f32[2,512,512]{2,1,0:T(8,128)S(1)}, bf16[2,512,256]{2,1,0:T(8,128)(2,1)S(1)}) custom-call(s32[4]{0:T(128)S(1)} %pad_add_fusion.sc, f32[1,1024]{1,0:T(1,128)S(1)} %get-tuple-element.51.log, bf16[1024,256]{1,0:T(8,128)(2,1)S(1)} %get-tuple-element.66.kr, f32[1024,128]{1,0:T(8,128)S(1)} %get-tuple-element.67.cosine, ...), custom_call_target="tpu_custom_call" | custom-call | flops 805306368 | tf_op jit(solution)/shard_map/pallas_call | solution.py:47
  46.2 2.3 %shard_map.150 = (bf16[4,64,2048]{2,1,0:T(8,128)(2,1)S(1)}, bf16[4,64,2048]{2,1,0:T(8,128)(2,1)S(1)}) custom-call(s32[4]{0:T(128)S(1)} %pad_add_fusion.sc, f32[1,1024]{1,0:T(1,128)S(1)} %get-tuple-element.51.log, bf16[64,512]{1,0:T(8,128)(2,1)S(1)} %get-tuple-element.62.i0, bf16[64,512]{1,0:T(8,128)(2,1)S(1)} %collective-permute-done.6.i1, ...), custom_call_target="tpu_custom_call" | custom-call | flops 1207959552 | tf_op jit(solution)/shard_map/pallas_call | solution.py:47
  48.7 2.3 %shard_map.153 = (bf16[4,64,2048]{2,1,0:T(8,128)(2,1)S(1)}, bf16[4,64,2048]{2,1,0:T(8,128)(2,1)S(1)}) custom-call(s32[4]{0:T(128)S(1)} %pad_add_fusion.sc, f32[1,1024]{1,0:T(1,128)S(1)} %get-tuple-element.51.log, bf16[64,512]{1,0:T(8,128)(2,1)S(1)} %get-tuple-element.62.i0, bf16[64,512]{1,0:T(8,128)(2,1)S(1)} %collective-permute-done.6.i1, ...), custom_call_target="tpu_custom_call" | custom-call | flops 1207959552 | tf_op jit(solution)/shard_map/pallas_call | solution.py:47
  51.1 0.6 collective-permute-start.20
  51.6 0.7 shard_map.151
  52.4 1.5 collective-permute-start.10
  53.9 2.7 %collective-permute-start.11 = (bf16[64,2048]{1,0:T(8,128)(2,1)S(1)}, bf16[64,2048]{1,0:T(8,128)(2,1)S(1)}, u32[]{:S(2)}, u32[]{:S(2)}) collective-permute-start(bf16[64,2048]{1,0:T(8,128)(2,1)S(1)} %get-tuple-element.76), channel_id=1, source_target_pairs={{0,4},{2,6},{4,0},{6,2},{1,5},{3,7},{5,1},{7,3},{8,12},{10,14},{12... | collective-permute-start | bytes 786440 | tf_op jit(solution)/shard_map/ppermute | solution.py:31
  56.6 1.4 collective-permute-start.12
  58.1 0.7 shard_map.154
  58.8 0.6 collective-permute-start.21
  59.5 0.9 collective-permute-start.22
  60.4 1.5 collective-permute-done.10.r1
  61.9 2.5 %collective-permute-start.23 = (bf16[64,2048]{1,0:T(8,128)(2,1)S(1)}, bf16[64,2048]{1,0:T(8,128)(2,1)S(1)}, u32[]{:S(2)}, u32[]{:S(2)}) collective-permute-start(bf16[64,2048]{1,0:T(8,128)(2,1)S(1)} %get-tuple-element.82), channel_id=1, source_target_pairs={{0,6},{2,0},{4,2},{6,4},{1,7},{3,1},{5,3},{7,5},{8,14},{10,8},{12,... | collective-permute-start | bytes 786440 | tf_op jit(solution)/shard_map/ppermute | solution.py:31
  64.4 5.1 %collective-permute-done.11.r2 = bf16[64,2048]{1,0:T(8,128)(2,1)S(1)} collective-permute-done((bf16[64,2048]{1,0:T(8,128)(2,1)S(1)}, bf16[64,2048]{1,0:T(8,128)(2,1)S(1)}, u32[]{:S(2)}, u32[]{:S(2)}) %collective-permute-start.11) | collective-permute-done | bytes 262176 | tf_op jit(solution)/shard_map/ppermute | solution.py:31
  69.5 1.0 shard_map.152.refs_0_
  70.5 2.6 %collective-permute-start.13 = (bf16[64,2048]{1,0:T(8,128)(2,1)S(1)}, bf16[64,2048]{1,0:T(8,128)(2,1)S(1)}, u32[]{:S(2)}, u32[]{:S(2)}) collective-permute-start(bf16[64,2048]{1,0:T(8,128)(2,1)S(1)} %shard_map.152.refs_0_), channel_id=1, source_target_pairs={{0,2},{2,4},{4,6},{6,0},{1,3},{3,5},{5,7},{7,1},{8,10},{10,12},{12... | collective-permute-start | bytes 786440 | tf_op jit(solution)/shard_map/ppermute | solution.py:31
  73.0 1.8 %collective-permute-start.14 = (bf16[64,2048]{1,0:T(8,128)(2,1)S(1)}, bf16[64,2048]{1,0:T(8,128)(2,1)S(1)}, u32[]{:S(2)}, u32[]{:S(2)}) collective-permute-start(bf16[64,2048]{1,0:T(8,128)(2,1)S(1)} %shard_map.152.refs_0_), channel_id=1, source_target_pairs={{0,4},{2,6},{4,0},{6,2},{1,5},{3,7},{5,1},{7,3},{8,12},{10,14},{12... | collective-permute-start | bytes 786440 | tf_op jit(solution)/shard_map/ppermute | solution.py:31
  74.8 6.0 %collective-permute-done.22.r2 = bf16[64,2048]{1,0:T(8,128)(2,1)S(1)} collective-permute-done((bf16[64,2048]{1,0:T(8,128)(2,1)S(1)}, bf16[64,2048]{1,0:T(8,128)(2,1)S(1)}, u32[]{:S(2)}, u32[]{:S(2)}) %collective-permute-start.22) | collective-permute-done | bytes 262176 | tf_op jit(solution)/shard_map/ppermute | solution.py:31
  80.8 1.0 shard_map.155.refs_0_
  81.7 0.8 collective-permute-start.24
  82.5 3.1 %collective-permute-start.25 = (bf16[64,2048]{1,0:T(8,128)(2,1)S(1)}, bf16[64,2048]{1,0:T(8,128)(2,1)S(1)}, u32[]{:S(2)}, u32[]{:S(2)}) collective-permute-start(bf16[64,2048]{1,0:T(8,128)(2,1)S(1)} %shard_map.155.refs_0_), channel_id=1, source_target_pairs={{0,4},{2,6},{4,0},{6,2},{1,5},{3,7},{5,1},{7,3},{8,12},{10,14},{12... | collective-permute-start | bytes 786440 | tf_op jit(solution)/shard_map/ppermute | solution.py:31
  85.6 1.6 collective-permute-start.26
  87.4 4.6 %collective-permute-done.14.refs_2_ = bf16[64,2048]{1,0:T(8,128)(2,1)S(1)} collective-permute-done((bf16[64,2048]{1,0:T(8,128)(2,1)S(1)}, bf16[64,2048]{1,0:T(8,128)(2,1)S(1)}, u32[]{:S(2)}, u32[]{:S(2)}) %collective-permute-start.14) | collective-permute-done | bytes 262176 | tf_op jit(solution)/shard_map/ppermute | solution.py:31
  92.0 4.4 %collective-permute-done.24.refs_1_ = bf16[64,2048]{1,0:T(8,128)(2,1)S(1)} collective-permute-done((bf16[64,2048]{1,0:T(8,128)(2,1)S(1)}, bf16[64,2048]{1,0:T(8,128)(2,1)S(1)}, u32[]{:S(2)}, u32[]{:S(2)}) %collective-permute-start.24) | collective-permute-done | bytes 262176 | tf_op jit(solution)/shard_map/ppermute | solution.py:31
  96.4 5.9 %collective-permute-done.25.refs_2_ = bf16[64,2048]{1,0:T(8,128)(2,1)S(1)} collective-permute-done((bf16[64,2048]{1,0:T(8,128)(2,1)S(1)}, bf16[64,2048]{1,0:T(8,128)(2,1)S(1)}, u32[]{:S(2)}, u32[]{:S(2)}) %collective-permute-start.25) | collective-permute-done | bytes 262176 | tf_op jit(solution)/shard_map/ppermute | solution.py:31
  102.3 0.5 collective-permute-start.30
  104.2 5.7 %shard_map.156 = (bf16[512,1408]{1,0:T(8,128)(2,1)S(1)}, bf16[2048,1408]{1,0:T(8,128)(2,1)S(1)}, bf16[2048,768]{1,0:T(8,128)(2,1)S(1)}) custom-call(s32[4]{0:T(128)S(1)} %pad_add_fusion.sc, bf16[64,2048]{1,0:T(8,128)(2,1)S(1)} %shard_map.155.refs_0_, bf16[64,2048]{1,0:T(8,128)(2,1)S(1)} %collective-permute-done.24.refs_1_, ...), custom_call_target="tpu_custom_call" | custom-call | flops 2952790016 | tf_op jit(solution)/shard_map/pallas_call | solution.py:47
  110.0 3.3 %collective-permute-start.31 = (bf16[16,1408]{1,0:T(8,128)(2,1)S(1)}, bf16[16,1408]{1,0:T(8,128)(2,1)S(1)}, u32[]{:S(2)}, u32[]{:S(2)}) collective-permute-start(bf16[16,1408]{1,0:T(8,128)(2,1)S(1)} %slice.15), channel_id=1, source_target_pairs={{0,8},{8,16},{16,24},{24,32},{32,40},{40,48},{48,56},{56,64},{64,7... | collective-permute-start | bytes 135176 | tf_op jit(solution)/shard_map/ppermute | solution.py:438
  113.3 4.6 %shard_map.157.mine.other = bf16[512,1408]{1,0:T(8,128)(2,1)S(1)} custom-call(s32[4]{0:T(128)S(1)} %pad_add_fusion.sc, bf16[64,2048]{1,0:T(8,128)(2,1)S(1)} %shard_map.152.refs_0_, bf16[64,2048]{1,0:T(8,128)(2,1)S(1)} %collective-permute-done.13.refs_1_, bf16[64,2048]{1,0:T(8,128)(2,1)S(1)} %collective-permute-done.14.refs_2_, ...), custom_call_target="tpu_custom_call" | custom-call | flops 2952790016 | tf_op jit(solution)/shard_map/pallas_call | solution.py:47
  118.0 4.6 %shard_map.160 = (bf16[4,64,2048]{2,1,0:T(8,128)(2,1)S(1)}, bf16[4,64,2048]{2,1,0:T(8,128)(2,1)S(1)}) custom-call(s32[4]{0:T(128)S(1)} %pad_add_fusion.sc, bf16[512,1408]{1,0:T(8,128)(2,1)S(1)} %get-tuple-element.85.other.mine, bf16[512,1408]{1,0:T(8,128)(2,1)S(1)} %shard_map.157.mine.other, bf16[16,1408]{1,0:T(8,128)(2,1)S(1)} %collective-permute-done.31.edge, ...), custom_call_target="tpu_custom_call" | custom-call | flops 2952790016 | tf_op jit(solution)/shard_map/pallas_call | solution.py:47
  122.9 4.6 %shard_map.158 = (bf16[4,64,2048]{2,1,0:T(8,128)(2,1)S(1)}, bf16[4,64,2048]{2,1,0:T(8,128)(2,1)S(1)}) custom-call(s32[4]{0:T(128)S(1)} %pad_add_fusion.sc, bf16[512,1408]{1,0:T(8,128)(2,1)S(1)} %shard_map.157.mine.other, bf16[512,1408]{1,0:T(8,128)(2,1)S(1)} %get-tuple-element.85.other.mine, bf16[16,1408]{1,0:T(8,128)(2,1)S(1)} %collective-permute-done.31.edge, ...), custom_call_target="tpu_custom_call" | custom-call | flops 2952790016 | tf_op jit(solution)/shard_map/pallas_call | solution.py:47
  127.5 0.6 collective-permute-start.32
  128.1 0.7 shard_map.161
  128.8 1.2 collective-permute-start.37
  130.0 2.4 %collective-permute-start.38 = (bf16[64,2048]{1,0:T(8,128)(2,1)S(1)}, bf16[64,2048]{1,0:T(8,128)(2,1)S(1)}, u32[]{:S(2)}, u32[]{:S(2)}) collective-permute-start(bf16[64,2048]{1,0:T(8,128)(2,1)S(1)} %get-tuple-element.95), channel_id=1, source_target_pairs={{0,4},{2,6},{4,0},{6,2},{1,5},{3,7},{5,1},{7,3},{8,12},{10,14},{12... | collective-permute-start | bytes 786440 | tf_op jit(solution)/shard_map/ppermute | solution.py:31
  132.3 0.9 collective-permute-start.39
  133.2 0.7 shard_map.159
  134.0 1.2 collective-permute-start.33
  135.2 1.1 collective-permute-start.34
  136.3 8.3 %collective-permute-done.37.r1 = bf16[64,2048]{1,0:T(8,128)(2,1)S(1)} collective-permute-done((bf16[64,2048]{1,0:T(8,128)(2,1)S(1)}, bf16[64,2048]{1,0:T(8,128)(2,1)S(1)}, u32[]{:S(2)}, u32[]{:S(2)}) %collective-permute-start.37) | collective-permute-done | bytes 262176 | tf_op jit(solution)/shard_map/ppermute | solution.py:31
  144.6 0.6 collective-permute-done.38.r2
  145.2 0.6 collective-permute-done.39.r3
  145.8 1.0 shard_map.162.rest_0_
  146.7 3.5 %collective-permute-done.33.r1 = bf16[64,2048]{1,0:T(8,128)(2,1)S(1)} collective-permute-done((bf16[64,2048]{1,0:T(8,128)(2,1)S(1)}, bf16[64,2048]{1,0:T(8,128)(2,1)S(1)}, u32[]{:S(2)}, u32[]{:S(2)}) %collective-permute-start.33) | collective-permute-done | bytes 262176 | tf_op jit(solution)/shard_map/ppermute | solution.py:31
  150.2 5.3 %collective-permute-done.34.r2 = bf16[64,2048]{1,0:T(8,128)(2,1)S(1)} collective-permute-done((bf16[64,2048]{1,0:T(8,128)(2,1)S(1)}, bf16[64,2048]{1,0:T(8,128)(2,1)S(1)}, u32[]{:S(2)}, u32[]{:S(2)}) %collective-permute-start.34) | collective-permute-done | bytes 262176 | tf_op jit(solution)/shard_map/ppermute | solution.py:31
  155.8 1.0 shard_map.163
  156.8 0.8 copy.22
  (60 shorter events, 2.5 us)
Async XLA Ops:
  6.5 97.7 %all-gather.2.cloned.1.call-start = ((), (), s32[]{:S(2)}) async-start(), calls=%async_computation | async-start | bytes 9469952 | tf_op jit(solution)/shard_map/all_gather | solution.py:402
  14.0 32.2 %copy-start.1 = (bf16[512,2048]{1,0:T(8,128)(2,1)S(1)}, bf16[512,2048]{1,0:T(8,128)(2,1)}, u32[]{:S(2)}) copy-start(bf16[512,2048]{1,0:T(8,128)(2,1)} %weight.3) | copy-start | bytes 6291460
  14.0 32.2 %copy-start.2 = (bf16[1024,512]{1,0:T(8,128)(2,1)S(1)}, bf16[1024,512]{1,0:T(8,128)(2,1)}, u32[]{:S(2)}) copy-start(bf16[1024,512]{1,0:T(8,128)(2,1)} %param.18) | copy-start | bytes 3145732
  14.0 6.0 %collective-permute-start = (bf16[80,512]{1,0:T(8,128)(2,1)S(1)}, bf16[80,512]{1,0:T(8,128)(2,1)S(1)}, u32[]{:S(2)}, u32[]{:S(2)}) collective-permute-start(bf16[80,512]{1,0:T(8,128)(2,1)S(1)} %get-tuple-element.56), channel_id=1, source_target_pairs={{0,8},{8,16},{16,24},{24,0},{1,9},{9,17},{17,25},{25,1},{2,10},{10... | collective-permute-start | bytes 245768 | tf_op jit(solution)/shard_map/ppermute | solution.py:31
  15.8 6.8 %collective-permute-start.1 = (bf16[80,512]{1,0:T(8,128)(2,1)S(1)}, bf16[80,512]{1,0:T(8,128)(2,1)S(1)}, u32[]{:S(2)}, u32[]{:S(2)}) collective-permute-start(bf16[80,512]{1,0:T(8,128)(2,1)S(1)} %get-tuple-element.57), channel_id=1, source_target_pairs={{0,16},{8,24},{16,0},{24,8},{1,17},{9,25},{17,1},{25,9},{2,18},{10... | collective-permute-start | bytes 245768 | tf_op jit(solution)/shard_map/ppermute | solution.py:31
  18.7 4.4 %collective-permute-start.2 = (bf16[80,512]{1,0:T(8,128)(2,1)S(1)}, bf16[80,512]{1,0:T(8,128)(2,1)S(1)}, u32[]{:S(2)}, u32[]{:S(2)}) collective-permute-start(bf16[80,512]{1,0:T(8,128)(2,1)S(1)} %get-tuple-element.58), channel_id=1, source_target_pairs={{0,24},{8,0},{16,8},{24,16},{1,25},{9,1},{17,9},{25,17},{2,26},{10... | collective-permute-start | bytes 245768 | tf_op jit(solution)/shard_map/ppermute | solution.py:31
  23.8 8.8 %collective-permute-start.3 = (bf16[80,512]{1,0:T(8,128)(2,1)S(1)}, bf16[80,512]{1,0:T(8,128)(2,1)S(1)}, u32[]{:S(2)}, u32[]{:S(2)}) collective-permute-start(bf16[80,512]{1,0:T(8,128)(2,1)S(1)} %get-tuple-element.59), channel_id=1, source_target_pairs={{0,32},{32,64},{64,96},{96,0},{1,33},{33,65},{65,97},{97,1},{2,34}... | collective-permute-start | bytes 245768 | tf_op jit(solution)/shard_map/ppermute | solution.py:31
  25.8 10.9 %collective-permute-start.4 = (bf16[80,512]{1,0:T(8,128)(2,1)S(1)}, bf16[80,512]{1,0:T(8,128)(2,1)S(1)}, u32[]{:S(2)}, u32[]{:S(2)}) collective-permute-start(bf16[80,512]{1,0:T(8,128)(2,1)S(1)} %get-tuple-element.59), channel_id=1, source_target_pairs={{0,64},{32,96},{64,0},{96,32},{1,65},{33,97},{65,1},{97,33},{2,66}... | collective-permute-start | bytes 245768 | tf_op jit(solution)/shard_map/ppermute | solution.py:31
  29.4 7.3 %collective-permute-start.5 = (bf16[80,512]{1,0:T(8,128)(2,1)S(1)}, bf16[80,512]{1,0:T(8,128)(2,1)S(1)}, u32[]{:S(2)}, u32[]{:S(2)}) collective-permute-start(bf16[80,512]{1,0:T(8,128)(2,1)S(1)} %get-tuple-element.59), channel_id=1, source_target_pairs={{0,96},{32,0},{64,32},{96,64},{1,97},{33,1},{65,33},{97,65},{2,98}... | collective-permute-start | bytes 245768 | tf_op jit(solution)/shard_map/ppermute | solution.py:31
  37.4 8.8 %collective-permute-start.6 = (bf16[64,512]{1,0:T(8,128)(2,1)S(1)}, bf16[64,512]{1,0:T(8,128)(2,1)S(1)}, u32[]{:S(2)}, u32[]{:S(2)}) collective-permute-start(bf16[64,512]{1,0:T(8,128)(2,1)S(1)} %get-tuple-element.63), channel_id=1, source_target_pairs={{0,8},{8,16},{16,24},{24,0},{1,9},{9,17},{17,25},{25,1},{2,10},{10... | collective-permute-start | bytes 196616 | tf_op jit(solution)/shard_map/ppermute | solution.py:31
  38.5 7.7 %collective-permute-start.7 = (bf16[64,512]{1,0:T(8,128)(2,1)S(1)}, bf16[64,512]{1,0:T(8,128)(2,1)S(1)}, u32[]{:S(2)}, u32[]{:S(2)}) collective-permute-start(bf16[64,512]{1,0:T(8,128)(2,1)S(1)} %get-tuple-element.64), channel_id=1, source_target_pairs={{0,16},{8,24},{16,0},{24,8},{1,17},{9,25},{17,1},{25,9},{2,18},{10... | collective-permute-start | bytes 196616 | tf_op jit(solution)/shard_map/ppermute | solution.py:31
  41.8 4.4 %collective-permute-start.8 = (bf16[64,512]{1,0:T(8,128)(2,1)S(1)}, bf16[64,512]{1,0:T(8,128)(2,1)S(1)}, u32[]{:S(2)}, u32[]{:S(2)}) collective-permute-start(bf16[64,512]{1,0:T(8,128)(2,1)S(1)} %get-tuple-element.65), channel_id=1, source_target_pairs={{0,24},{8,0},{16,8},{24,16},{1,25},{9,1},{17,9},{25,17},{2,26},{10... | collective-permute-start | bytes 196616 | tf_op jit(solution)/shard_map/ppermute | solution.py:31
  48.6 3.0 %collective-permute-start.9 = (bf16[4,64,2048]{2,1,0:T(8,128)(2,1)S(1)}, bf16[4,64,2048]{2,1,0:T(8,128)(2,1)S(1)}, u32[]{:S(2)}, u32[]{:S(2)}) collective-permute-start(bf16[4,64,2048]{2,1,0:T(8,128)(2,1)S(1)} %get-tuple-element.74), channel_id=1, source_target_pairs={{0,1},{1,0},{2,3},{3,2},{4,5},{5,4},{6,7},{7,6},{8,9},{9,8},{10,11... | collective-permute-start | bytes 3145736 | tf_op jit(solution)/shard_map/ppermute | solution.py:39
  48.7 15.7 %copy-start.5 = (f32[2,3,704]{2,0,1:T(2,128)S(1)}, f32[2,3,704]{2,0,1:T(2,128)}, u32[]{:S(2)}) copy-start(f32[2,3,704]{2,0,1:T(2,128)} %param.26) | copy-start | bytes 50692
  51.0 18.4 %copy-start = (bf16[1024,2048]{1,0:T(8,128)(2,1)S(1)}, bf16[1024,2048]{1,0:T(8,128)(2,1)}, u32[]{:S(2)}) copy-start(bf16[1024,2048]{1,0:T(8,128)(2,1)} %param.20) | copy-start | bytes 12582916
  51.0 18.4 %copy-start.3 = (f32[2,2048]{1,0:T(2,128)S(1)}, f32[2,2048]{1,0:T(2,128)}, u32[]{:S(2)}) copy-start(f32[2,2048]{1,0:T(2,128)} %gain.7) | copy-start | bytes 49156
  51.1 18.4 %copy-start.4 = (f32[2,2048]{1,0:T(2,128)S(1)}, f32[2,2048]{1,0:T(2,128)}, u32[]{:S(2)}) copy-start(f32[2,2048]{1,0:T(2,128)} %shift.7) | copy-start | bytes 49156
  51.1 7.0 %collective-permute-start.20 = (bf16[4,64,2048]{2,1,0:T(8,128)(2,1)S(1)}, bf16[4,64,2048]{2,1,0:T(8,128)(2,1)S(1)}, u32[]{:S(2)}, u32[]{:S(2)}) collective-permute-start(bf16[4,64,2048]{2,1,0:T(8,128)(2,1)S(1)} %get-tuple-element.79), channel_id=1, source_target_pairs={{0,1},{1,0},{2,3},{3,2},{4,5},{5,4},{6,7},{7,6},{8,9},{9,8},{10,11... | collective-permute-start | bytes 3145736 | tf_op jit(solution)/shard_map/ppermute | solution.py:39
  52.4 9.5 %collective-permute-start.10 = (bf16[64,2048]{1,0:T(8,128)(2,1)S(1)}, bf16[64,2048]{1,0:T(8,128)(2,1)S(1)}, u32[]{:S(2)}, u32[]{:S(2)}) collective-permute-start(bf16[64,2048]{1,0:T(8,128)(2,1)S(1)} %get-tuple-element.75), channel_id=1, source_target_pairs={{0,2},{2,4},{4,6},{6,0},{1,3},{3,5},{5,7},{7,1},{8,10},{10,12},{12... | collective-permute-start | bytes 786440 | tf_op jit(solution)/shard_map/ppermute | solution.py:31
  53.9 15.5 %collective-permute-start.11 = (bf16[64,2048]{1,0:T(8,128)(2,1)S(1)}, bf16[64,2048]{1,0:T(8,128)(2,1)S(1)}, u32[]{:S(2)}, u32[]{:S(2)}) collective-permute-start(bf16[64,2048]{1,0:T(8,128)(2,1)S(1)} %get-tuple-element.76), channel_id=1, source_target_pairs={{0,4},{2,6},{4,0},{6,2},{1,5},{3,7},{5,1},{7,3},{8,12},{10,14},{12... | collective-permute-start | bytes 786440 | tf_op jit(solution)/shard_map/ppermute | solution.py:31
  56.6 12.8 %collective-permute-start.12 = (bf16[64,2048]{1,0:T(8,128)(2,1)S(1)}, bf16[64,2048]{1,0:T(8,128)(2,1)S(1)}, u32[]{:S(2)}, u32[]{:S(2)}) collective-permute-start(bf16[64,2048]{1,0:T(8,128)(2,1)S(1)} %get-tuple-element.77), channel_id=1, source_target_pairs={{0,6},{2,0},{4,2},{6,4},{1,7},{3,1},{5,3},{7,5},{8,14},{10,8},{12,... | collective-permute-start | bytes 786440 | tf_op jit(solution)/shard_map/ppermute | solution.py:31
  58.8 16.0 %collective-permute-start.21 = (bf16[64,2048]{1,0:T(8,128)(2,1)S(1)}, bf16[64,2048]{1,0:T(8,128)(2,1)S(1)}, u32[]{:S(2)}, u32[]{:S(2)}) collective-permute-start(bf16[64,2048]{1,0:T(8,128)(2,1)S(1)} %get-tuple-element.80), channel_id=1, source_target_pairs={{0,2},{2,4},{4,6},{6,0},{1,3},{3,5},{5,7},{7,1},{8,10},{10,12},{12... | collective-permute-start | bytes 786440 | tf_op jit(solution)/shard_map/ppermute | solution.py:31
  59.5 21.3 %collective-permute-start.22 = (bf16[64,2048]{1,0:T(8,128)(2,1)S(1)}, bf16[64,2048]{1,0:T(8,128)(2,1)S(1)}, u32[]{:S(2)}, u32[]{:S(2)}) collective-permute-start(bf16[64,2048]{1,0:T(8,128)(2,1)S(1)} %get-tuple-element.81), channel_id=1, source_target_pairs={{0,4},{2,6},{4,0},{6,2},{1,5},{3,7},{5,1},{7,3},{8,12},{10,14},{12... | collective-permute-start | bytes 786440 | tf_op jit(solution)/shard_map/ppermute | solution.py:31
  61.9 18.8 %collective-permute-start.23 = (bf16[64,2048]{1,0:T(8,128)(2,1)S(1)}, bf16[64,2048]{1,0:T(8,128)(2,1)S(1)}, u32[]{:S(2)}, u32[]{:S(2)}) collective-permute-start(bf16[64,2048]{1,0:T(8,128)(2,1)S(1)} %get-tuple-element.82), channel_id=1, source_target_pairs={{0,6},{2,0},{4,2},{6,4},{1,7},{3,1},{5,3},{7,5},{8,14},{10,8},{12,... | collective-permute-start | bytes 786440 | tf_op jit(solution)/shard_map/ppermute | solution.py:31
  70.5 16.8 %copy-start.6 = (f32[2,704]{1,0:T(2,128)S(1)}, f32[2,704]{1,0:T(2,128)}, u32[]{:S(2)}) copy-start(f32[2,704]{1,0:T(2,128)} %param.27) | copy-start | bytes 16900
  70.5 16.8 %collective-permute-start.13 = (bf16[64,2048]{1,0:T(8,128)(2,1)S(1)}, bf16[64,2048]{1,0:T(8,128)(2,1)S(1)}, u32[]{:S(2)}, u32[]{:S(2)}) collective-permute-start(bf16[64,2048]{1,0:T(8,128)(2,1)S(1)} %shard_map.152.refs_0_), channel_id=1, source_target_pairs={{0,2},{2,4},{4,6},{6,0},{1,3},{3,5},{5,7},{7,1},{8,10},{10,12},{12... | collective-permute-start | bytes 786440 | tf_op jit(solution)/shard_map/ppermute | solution.py:31
  73.0 19.0 %collective-permute-start.14 = (bf16[64,2048]{1,0:T(8,128)(2,1)S(1)}, bf16[64,2048]{1,0:T(8,128)(2,1)S(1)}, u32[]{:S(2)}, u32[]{:S(2)}) collective-permute-start(bf16[64,2048]{1,0:T(8,128)(2,1)S(1)} %shard_map.152.refs_0_), channel_id=1, source_target_pairs={{0,4},{2,6},{4,0},{6,2},{1,5},{3,7},{5,1},{7,3},{8,12},{10,14},{12... | collective-permute-start | bytes 786440 | tf_op jit(solution)/shard_map/ppermute | solution.py:31
  81.7 14.7 %collective-permute-start.24 = (bf16[64,2048]{1,0:T(8,128)(2,1)S(1)}, bf16[64,2048]{1,0:T(8,128)(2,1)S(1)}, u32[]{:S(2)}, u32[]{:S(2)}) collective-permute-start(bf16[64,2048]{1,0:T(8,128)(2,1)S(1)} %shard_map.155.refs_0_), channel_id=1, source_target_pairs={{0,2},{2,4},{4,6},{6,0},{1,3},{3,5},{5,7},{7,1},{8,10},{10,12},{12... | collective-permute-start | bytes 786440 | tf_op jit(solution)/shard_map/ppermute | solution.py:31
  82.5 19.8 %collective-permute-start.25 = (bf16[64,2048]{1,0:T(8,128)(2,1)S(1)}, bf16[64,2048]{1,0:T(8,128)(2,1)S(1)}, u32[]{:S(2)}, u32[]{:S(2)}) collective-permute-start(bf16[64,2048]{1,0:T(8,128)(2,1)S(1)} %shard_map.155.refs_0_), channel_id=1, source_target_pairs={{0,4},{2,6},{4,0},{6,2},{1,5},{3,7},{5,1},{7,3},{8,12},{10,14},{12... | collective-permute-start | bytes 786440 | tf_op jit(solution)/shard_map/ppermute | solution.py:31
  85.6 16.7 %collective-permute-start.26 = (bf16[64,2048]{1,0:T(8,128)(2,1)S(1)}, bf16[64,2048]{1,0:T(8,128)(2,1)S(1)}, u32[]{:S(2)}, u32[]{:S(2)}) collective-permute-start(bf16[64,2048]{1,0:T(8,128)(2,1)S(1)} %shard_map.155.refs_0_), channel_id=1, source_target_pairs={{0,6},{2,0},{4,2},{6,4},{1,7},{3,1},{5,3},{7,5},{8,14},{10,8},{12,... | collective-permute-start | bytes 786440 | tf_op jit(solution)/shard_map/ppermute | solution.py:31
  87.3 15.7 %collective-permute-start.15 = (bf16[64,2048]{1,0:T(8,128)(2,1)S(1)}, bf16[64,2048]{1,0:T(8,128)(2,1)S(1)}, u32[]{:S(2)}, u32[]{:S(2)}) collective-permute-start(bf16[64,2048]{1,0:T(8,128)(2,1)S(1)} %shard_map.152.refs_0_), channel_id=1, source_target_pairs={{0,6},{2,0},{4,2},{6,4},{1,7},{3,1},{5,3},{7,5},{8,14},{10,8},{12,... | collective-permute-start | bytes 786440 | tf_op jit(solution)/shard_map/ppermute | solution.py:31
  92.0 11.0 %collective-permute-start.27 = (bf16[64,2048]{1,0:T(8,128)(2,1)S(1)}, bf16[64,2048]{1,0:T(8,128)(2,1)S(1)}, u32[]{:S(2)}, u32[]{:S(2)}) collective-permute-start(bf16[64,2048]{1,0:T(8,128)(2,1)S(1)} %shard_map.155.refs_0_), channel_id=1, source_target_pairs={{0,1},{1,0},{2,3},{3,2},{4,5},{5,4},{6,7},{7,6},{8,9},{9,8},{10,11... | collective-permute-start | bytes 786440 | tf_op jit(solution)/shard_map/ppermute | solution.py:39
  96.4 7.1 %collective-permute-start.28 = (bf16[64,2048]{1,0:T(8,128)(2,1)S(1)}, bf16[64,2048]{1,0:T(8,128)(2,1)S(1)}, u32[]{:S(2)}, u32[]{:S(2)}) collective-permute-start(bf16[64,2048]{1,0:T(8,128)(2,1)S(1)} %collective-permute-done.24.refs_1_), channel_id=1, source_target_pairs={{0,1},{1,0},{2,3},{3,2},{4,5},{5,4},{6,7},{7,6},{8,9},{9,8},{10,11... | collective-permute-start | bytes 786440 | tf_op jit(solution)/shard_map/ppermute | solution.py:39
  102.3 1.5 collective-permute-start.29
  102.3 1.9 %collective-permute-start.30 = (bf16[64,2048]{1,0:T(8,128)(2,1)S(1)}, bf16[64,2048]{1,0:T(8,128)(2,1)S(1)}, u32[]{:S(2)}, u32[]{:S(2)}) collective-permute-start(bf16[64,2048]{1,0:T(8,128)(2,1)S(1)} %collective-permute-done.26.refs_3_), channel_id=1, source_target_pairs={{0,1},{1,0},{2,3},{3,2},{4,5},{5,4},{6,7},{7,6},{8,9},{9,8},{10,11... | collective-permute-start | bytes 786440 | tf_op jit(solution)/shard_map/ppermute | solution.py:39
  103.0 10.3 %collective-permute-start.16 = (bf16[64,2048]{1,0:T(8,128)(2,1)S(1)}, bf16[64,2048]{1,0:T(8,128)(2,1)S(1)}, u32[]{:S(2)}, u32[]{:S(2)}) collective-permute-start(bf16[64,2048]{1,0:T(8,128)(2,1)S(1)} %shard_map.152.refs_0_), channel_id=1, source_target_pairs={{0,1},{1,0},{2,3},{3,2},{4,5},{5,4},{6,7},{7,6},{8,9},{9,8},{10,11... | collective-permute-start | bytes 786440 | tf_op jit(solution)/shard_map/ppermute | solution.py:39
  103.0 10.3 %collective-permute-start.17 = (bf16[64,2048]{1,0:T(8,128)(2,1)S(1)}, bf16[64,2048]{1,0:T(8,128)(2,1)}, u32[]{:S(2)}, u32[]{:S(2)}) collective-permute-start(bf16[64,2048]{1,0:T(8,128)(2,1)S(1)} %collective-permute-done.13.refs_1_), channel_id=1, source_target_pairs={{0,1},{1,0},{2,3},{3,2},{4,5},{5,4},{6,7},{7,6},{8,9},{9,8},{10,11... | collective-permute-start | bytes 786440 | tf_op jit(solution)/shard_map/ppermute | solution.py:39
  103.5 9.8 %collective-permute-start.18 = (bf16[64,2048]{1,0:T(8,128)(2,1)S(1)}, bf16[64,2048]{1,0:T(8,128)(2,1)}, u32[]{:S(2)}, u32[]{:S(2)}) collective-permute-start(bf16[64,2048]{1,0:T(8,128)(2,1)S(1)} %collective-permute-done.14.refs_2_), channel_id=1, source_target_pairs={{0,1},{1,0},{2,3},{3,2},{4,5},{5,4},{6,7},{7,6},{8,9},{9,8},{10,11... | collective-permute-start | bytes 786440 | tf_op jit(solution)/shard_map/ppermute | solution.py:39
  103.9 9.5 %collective-permute-start.19 = (bf16[64,2048]{1,0:T(8,128)(2,1)S(1)}, bf16[64,2048]{1,0:T(8,128)(2,1)}, u32[]{:S(2)}, u32[]{:S(2)}) collective-permute-start(bf16[64,2048]{1,0:T(8,128)(2,1)S(1)} %collective-permute-done.15.refs_3_), channel_id=1, source_target_pairs={{0,1},{1,0},{2,3},{3,2},{4,5},{5,4},{6,7},{7,6},{8,9},{9,8},{10,11... | collective-permute-start | bytes 786440 | tf_op jit(solution)/shard_map/ppermute | solution.py:39
  110.0 8.0 %collective-permute-start.31 = (bf16[16,1408]{1,0:T(8,128)(2,1)S(1)}, bf16[16,1408]{1,0:T(8,128)(2,1)S(1)}, u32[]{:S(2)}, u32[]{:S(2)}) collective-permute-start(bf16[16,1408]{1,0:T(8,128)(2,1)S(1)} %slice.15), channel_id=1, source_target_pairs={{0,8},{8,16},{16,24},{24,32},{32,40},{40,48},{48,56},{56,64},{64,7... | collective-permute-start | bytes 135176 | tf_op jit(solution)/shard_map/ppermute | solution.py:438
  122.6 5.5 %collective-permute-start.36 = (bf16[4,64,2048]{2,1,0:T(8,128)(2,1)S(1)}, bf16[4,64,2048]{2,1,0:T(8,128)(2,1)S(1)}, u32[]{:S(2)}, u32[]{:S(2)}) collective-permute-start(bf16[4,64,2048]{2,1,0:T(8,128)(2,1)S(1)} %get-tuple-element.93), channel_id=1, source_target_pairs={{0,1},{1,0},{2,3},{3,2},{4,5},{5,4},{6,7},{7,6},{8,9},{9,8},{10,11... | collective-permute-start | bytes 3145736 | tf_op jit(solution)/shard_map/ppermute | solution.py:39
  127.5 5.8 %collective-permute-start.32 = (bf16[4,64,2048]{2,1,0:T(8,128)(2,1)S(1)}, bf16[4,64,2048]{2,1,0:T(8,128)(2,1)S(1)}, u32[]{:S(2)}, u32[]{:S(2)}) collective-permute-start(bf16[4,64,2048]{2,1,0:T(8,128)(2,1)S(1)} %get-tuple-element.88), channel_id=1, source_target_pairs={{0,1},{1,0},{2,3},{3,2},{4,5},{5,4},{6,7},{7,6},{8,9},{9,8},{10,11... | collective-permute-start | bytes 3145736 | tf_op jit(solution)/shard_map/ppermute | solution.py:39
  128.8 15.8 %collective-permute-start.37 = (bf16[64,2048]{1,0:T(8,128)(2,1)S(1)}, bf16[64,2048]{1,0:T(8,128)(2,1)S(1)}, u32[]{:S(2)}, u32[]{:S(2)}) collective-permute-start(bf16[64,2048]{1,0:T(8,128)(2,1)S(1)} %get-tuple-element.94), channel_id=1, source_target_pairs={{0,2},{2,4},{4,6},{6,0},{1,3},{3,5},{5,7},{7,1},{8,10},{10,12},{12... | collective-permute-start | bytes 786440 | tf_op jit(solution)/shard_map/ppermute | solution.py:31
  130.0 15.2 %collective-permute-start.38 = (bf16[64,2048]{1,0:T(8,128)(2,1)S(1)}, bf16[64,2048]{1,0:T(8,128)(2,1)S(1)}, u32[]{:S(2)}, u32[]{:S(2)}) collective-permute-start(bf16[64,2048]{1,0:T(8,128)(2,1)S(1)} %get-tuple-element.95), channel_id=1, source_target_pairs={{0,4},{2,6},{4,0},{6,2},{1,5},{3,7},{5,1},{7,3},{8,12},{10,14},{12... | collective-permute-start | bytes 786440 | tf_op jit(solution)/shard_map/ppermute | solution.py:31
  132.3 13.4 %collective-permute-start.39 = (bf16[64,2048]{1,0:T(8,128)(2,1)S(1)}, bf16[64,2048]{1,0:T(8,128)(2,1)S(1)}, u32[]{:S(2)}, u32[]{:S(2)}) collective-permute-start(bf16[64,2048]{1,0:T(8,128)(2,1)S(1)} %get-tuple-element.96), channel_id=1, source_target_pairs={{0,6},{2,0},{4,2},{6,4},{1,7},{3,1},{5,3},{7,5},{8,14},{10,8},{12,... | collective-permute-start | bytes 786440 | tf_op jit(solution)/shard_map/ppermute | solution.py:31
  134.0 16.2 %collective-permute-start.33 = (bf16[64,2048]{1,0:T(8,128)(2,1)S(1)}, bf16[64,2048]{1,0:T(8,128)(2,1)S(1)}, u32[]{:S(2)}, u32[]{:S(2)}) collective-permute-start(bf16[64,2048]{1,0:T(8,128)(2,1)S(1)} %get-tuple-element.89), channel_id=1, source_target_pairs={{0,2},{2,4},{4,6},{6,0},{1,3},{3,5},{5,7},{7,1},{8,10},{10,12},{12... | collective-permute-start | bytes 786440 | tf_op jit(solution)/shard_map/ppermute | solution.py:31
  135.2 20.3 %collective-permute-start.34 = (bf16[64,2048]{1,0:T(8,128)(2,1)S(1)}, bf16[64,2048]{1,0:T(8,128)(2,1)S(1)}, u32[]{:S(2)}, u32[]{:S(2)}) collective-permute-start(bf16[64,2048]{1,0:T(8,128)(2,1)S(1)} %get-tuple-element.90), channel_id=1, source_target_pairs={{0,4},{2,6},{4,0},{6,2},{1,5},{3,7},{5,1},{7,3},{8,12},{10,14},{12... | collective-permute-start | bytes 786440 | tf_op jit(solution)/shard_map/ppermute | solution.py:31
  144.6 11.3 %collective-permute-start.35 = (bf16[64,2048]{1,0:T(8,128)(2,1)S(1)}, bf16[64,2048]{1,0:T(8,128)(2,1)S(1)}, u32[]{:S(2)}, u32[]{:S(2)}) collective-permute-start(bf16[64,2048]{1,0:T(8,128)(2,1)S(1)} %get-tuple-element.91), channel_id=1, source_target_pairs={{0,6},{2,0},{4,2},{6,4},{1,7},{3,1},{5,3},{7,5},{8,14},{10,8},{12,... | collective-permute-start | bytes 786440 | tf_op jit(solution)/shard_map/ppermute | solution.py:31
Sparse Core Ops, SparseCore 0:
  10.2 77.6 all-gather.1
where the time goes:
time: 165 us; the launch traced here: 164 us
  waiting for transfers between devices  55.9 us (34%)
  starting transfers between devices  50.3 us (30%)
  Pallas kernels  43.4 us (26%)
  between operations  13.8 us (8%)
    ppermute x27, waiting for transfers between devices, shift_by(): return lax.ppermute(x, axis, ring(by))  55.5 us
    ppermute x27, starting transfers between devices, shift_by(): return lax.ppermute(x, axis, ring(by))  44.1 us
    pallas_call x19, Pallas kernels, run(): pl.pallas_call(kernel, in_specs=[pl.BlockSpec(memory_space=pltpu.SMEM)] +...  43.4 us
    ppermute x1, starting transfers between devices, shards(): lax.ppermute(ups[1][8 * n - 16:], SP, [(i, i + 1) for i in range(15)])  3.33 us
  transfers between devices with their start and end apart: 41, of which 18 were waited for; matrix products, arithmetic and copies ran while one was open for 0% of the time, Pallas kernels for 21%

commit v1 on v0

--- a/solution.py
+++ b/solution.py
@@ -20,7 +20,6 @@
 ROPE_BASE = 10000.0
 EPS = 1e-05
 EXTRA = 16
-HIGHEST = lax.Precision.HIGHEST
 
 
 def ring(shift, size=4):
@@ -80,13 +79,33 @@
     return r >= c
 
 
-def running_logs(row, lower):
-    n = lower.shape[0]
-    rows = jnp.broadcast_to(row, (8, n))
-    tri = lower.astype(f32)
-    down = lax.dot_general(tri, rows, (((1,), (1,)), ((), ())), precision=HIGHEST, preferred_element_type=f32)
-    across = lax.dot_general(rows, tri, (((1,), (1,)), ((), ())), precision=HIGHEST, preferred_element_type=f32)
-    return down[:, 0:1], across[0:1, :]
+def split_logs(log):
+    blocks = log.shape[1] // BLOCK
+    whole = jnp.concatenate([log[:, b * BLOCK : (b + 1) * BLOCK] for b in range(blocks)], axis=0)
+    first = whole.astype(bf16).astype(f32)
+    second = (whole - first).astype(bf16).astype(f32)
+    third = whole - first - second
+    return jnp.concatenate([first, second, third, jnp.zeros_like(whole)], axis=0).astype(bf16)
+
+
+def running_logs(log, down, across):
+    terms = split_logs(log[...])
+    lower = triangle(BLOCK).astype(f32).astype(bf16)
+    last = (((1,), (1,)), ((), ()))
+    down[...] = lax.dot_general(lower, terms, last, preferred_element_type=f32)
+    across[...] = lax.dot_general(terms, lower, last, preferred_element_type=f32)
+
+
+def log_column(down, b):
+    lane = lax.broadcasted_iota(jnp.int32, down.shape, 1)
+    blocks = down.shape[1] // 4
+    mine = (lane == b) | (lane == b + blocks) | (lane == b + 2 * blocks)
+    return jnp.sum(jnp.where(mine, down[...], 0.0), axis=1, keepdims=True)
+
+
+def log_row(across, b):
+    blocks = across.shape[0] // 4
+    return across[pl.ds(b, 1), :] + across[pl.ds(b + blocks, 1), :] + across[pl.ds(b + 2 * blocks, 1), :]
 
 
 def log_rows(total, width):
@@ -102,13 +121,13 @@
     return rows[0:1, 0:1] + rows[1:2, 0:1] + rows[2:3, 0:1]
 
 
-def states_kernel(sc, log, k, v, tables, kr, cosine, sine, prefix, p0, p1, p2, p3, state):
-    lower = triangle(BLOCK)
+def states_kernel(sc, log, k, v, tables, kr, cosine, sine, prefix, down, across, p0, p1, p2, p3, state):
+    running_logs(log, down, across)
     state[...] = jnp.zeros_like(state)
 
     def step(b, _):
         at = pl.ds(pl.multiple_of(b * BLOCK, BLOCK), BLOCK)
-        cum, _ = running_logs(log[:, at], lower)
+        cum = log_column(down, b)
         total = cum[BLOCK - 1 : BLOCK, :]
         span = tables.shape[1]
         for i in range(BLOCK // span):
@@ -162,16 +181,16 @@
         out[...] = (fade * run + entry[at]).astype(bf16)
 
 
-def within_kernel(sc, log, kr, cosine, sine, prefix, q, v, within, scaled):
+def within_kernel(sc, down, across, kr, cosine, sine, prefix, q, v, within, scaled):
     lower = triangle(BLOCK)
     n = BLOCK // 4
 
     def step(b, _):
         at = pl.ds(pl.multiple_of(b * BLOCK, BLOCK), BLOCK)
-        cum, across = running_logs(log[:, at], lower)
+        cum, row = log_column(down, b), log_row(across, b)
         query = rotated(q[at, :].astype(f32), cosine[at, :], sine[at, :]).astype(bf16)
         score = lax.dot_general(query, kr[at, :], (((1,), (1,)), ((), ())), preferred_element_type=f32)
-        weight = jnp.where(lower, jnp.exp(jnp.where(lower, cum - across, 0.0)), 0.0)
+        weight = jnp.where(lower, jnp.exp(jnp.where(lower, cum - row, 0.0)), 0.0)
         result = jnp.dot((score * weight).astype(bf16), v[at, :], preferred_element_type=f32)
         faded = (query.astype(f32) * jnp.exp(cum)).astype(bf16)
         result = result + jnp.dot(faded, prefix[b], preferred_element_type=f32)
@@ -181,7 +200,7 @@
             scaled[i % 2, to, :] = faded[i * n : (i + 1) * n]
         return 0
 
-    lax.fori_loop(0, log.shape[1] // BLOCK, step, 0)
+    lax.fori_loop(0, kr.shape[0] // BLOCK, step, 0)
 
 
 def heads_kernel(sc, log, i0, i1, i2, i3, within, scaled, gate, weight, keep, send, start, carried, chunk):
@@ -224,7 +243,7 @@
 
 
 def norm_kernel(sc, keep, got, r1, r2, r3, base, gain, shift, *rest, row, group):
-    out, rows = rest[-1], keep.shape[1]
+    out, rows = rest[0], keep.shape[1]
     total = keep[0].astype(f32) + got[0].astype(f32) + r1[...].astype(f32)
     total = total + r2[...].astype(f32) + r3[...].astype(f32)
     at = 0 if group is None else 4 * sc[2] + 2 * sc[3] + group
@@ -232,10 +251,20 @@
     centred = total - jnp.mean(total, axis=1, keepdims=True)
     spread = jnp.mean(centred * centred, axis=1, keepdims=True)
     if len(rest) > 1:
-        out[rows:] = rest[0][...]
-    out[:rows] = (
+        after, target, own, sems = rest
+        later = pltpu.make_async_copy(after, target.at[pl.ds(rows, after.shape[0])], sems.at[1])
+        later.start()
+    result = (
         centred * lax.rsqrt(spread + EPS) * gain[row : row + 1, :] + shift[row : row + 1, :]
     ).astype(bf16)
+    if len(rest) == 1:
+        out[...] = result
+        return
+    own[...] = result
+    mine = pltpu.make_async_copy(own, target.at[pl.ds(0, rows)], sems.at[0])
+    mine.start()
+    mine.wait()
+    later.wait()
 
 
 def reduce_and_norm(sc, keep, send, base, gain, shift, row, group, *after):
@@ -248,6 +277,7 @@
     return run(
         functools.partial(norm_kernel, row=row, group=group),
         sc, (keep, got, *far, base, gain, shift, *after), [((rows * (1 + len(after)), width), bf16)], flops=size * 400,
+        far_outs=len(after), scratch=[pltpu.VMEM(*piece), pltpu.SemaphoreType.DMA((2,))] if after else [],
     )[0]
 
 
@@ -269,9 +299,9 @@
         copy.start()
     for copy in loads:
         copy.wait()
-    parts = [r[...].astype(f32).T for r in (gate_v, value_v, down_v)]
-    rest = both.shape[1] - sum(p.shape[1] for p in parts)
-    both[...] = jnp.concatenate(parts + [jnp.zeros((both.shape[0], rest), f32)], axis=1).astype(bf16)
+    parts = [r[...] for r in (gate_v, value_v, down_v)]
+    rest = both.shape[1] - sum(p.shape[0] for p in parts)
+    both[...] = jnp.concatenate(parts + [jnp.zeros((rest, both.shape[0]), bf16)], axis=0).T
     out = pltpu.make_async_copy(both, shard, weight_sems.at[3])
     out.start()
     for copy in moves:
@@ -337,7 +367,7 @@
     )[0]
 
 
-def down_kernel(sc, mine, other, edge, taps, bias, weight, keep, send, active, padded, chunk):
+def down_kernel(sc, mine, other, edge, taps, bias, weight, keep, send, active, chunk):
     n = keep.shape[1]
     hidden = active.shape[1]
 
@@ -348,11 +378,10 @@
         else:
             before = pl.multiple_of(jnp.maximum(at - 16, 0), 16)
             halo = jnp.where(t == 0, edge[8:].astype(f32), other[pl.ds(before, 16), :][8:].astype(f32))
-        padded[0:8] = halo.astype(f32)
-        padded[8:] = mine[pl.ds(at, n), :].astype(f32)
-        conv = bias[0:1, :] + padded[6 : 6 + n] * taps[0:1, :]
-        conv = conv + padded[7 : 7 + n] * taps[1:2, :]
-        conv = conv + padded[8 : 8 + n] * taps[2:3, :]
+        rows = jnp.concatenate([halo.astype(f32), mine[pl.ds(at, n), :].astype(f32)], axis=0)
+        conv = bias[0:1, :] + pltpu.roll(rows, 2, 0)[8:] * taps[0:1, :]
+        conv = conv + pltpu.roll(rows, 1, 0)[8:] * taps[1:2, :]
+        conv = conv + rows[8:] * taps[2:3, :]
         active[pl.ds(at, n), :] = (jax.nn.gelu(conv[:, :hidden]) * conv[:, hidden:]).astype(bf16)
         return 0
 
@@ -369,7 +398,7 @@
     return run(
         functools.partial(down_kernel, chunk=chunk), sc,
         (mine, other, edge, taps, bias, weights), [shape, shape],
-        scratch=[pltpu.VMEM((rows, double // 2), bf16), pltpu.VMEM((n + 8, double), f32)],
+        scratch=[pltpu.VMEM((rows, double // 2), bf16)],
         flops=rows * width * double * 2, limit=16,
     )
 
@@ -402,14 +431,15 @@
     weights = lax.all_gather(shard, SP, axis=0, tiled=True)
     piece = ((dk // 4 + EXTRA, dv), bf16)
     turn = ((tok, dk // 2), f32)
-    key_rot, cosine, sine, prefix, *pieces = run(
+    key_rot, cosine, sine, prefix, down_logs, across_logs, *pieces = run(
         states_kernel, sc, (log, key, value, tables),
-        [((tok, dk), bf16), turn, turn, ((blocks, dk, dv), bf16)] + [piece] * 4,
+        [((tok, dk), bf16), turn, turn, ((blocks, dk, dv), bf16), ((BLOCK, 4 * blocks), f32), ((4 * blocks, BLOCK), f32)]
+        + [piece] * 4,
         scratch=[pltpu.VMEM((dk, dv), f32)], flops=4 * tok * dk * dv,
     )
     got = [pieces[0]] + [shift_by(pieces[d], "y", d) for d in (1, 2, 3)]
     within, scaled = run(
-        within_kernel, sc, (log, key_rot, cosine, sine, prefix, query, value),
+        within_kernel, sc, (down_logs, across_logs, key_rot, cosine, sine, prefix, query, value),
         [((2, tok // 2, dv), f32), ((2, tok // 2, dk), bf16)],
         flops=4 * tok * BLOCK * (dk + dv),
     )

time: 165 us -> 161 us (0.976)
  Pallas kernels: 43.4 us -> 40.3 us
  starting transfers between devices: 50.3 us -> 47.9 us
  waiting for transfers between devices: 55.9 us -> 58 us
    pallas_call x19, Pallas kernels: 43.4 us -> 40.3 us  [run(): pl.pallas_call(kernel, in_specs=[pl.BlockSpec(memory_space=pltpu.SMEM)] +...]
    ppermute x27, waiting for transfers between devices: 55.5 us -> 57.5 us  [shift_by(): return lax.ppermute(x, axis, ring(by))]
  transfers between devices with their start and end apart: 41 -> 41, of which waited for: 18 -> 20; matrix products, arithmetic and copies ran while one was open for 0% -> 0% of each run, Pallas kernels for 21% -> 19%
where the time goes in v1:
time: 161 us; the launch traced here: 160 us
  waiting for transfers between devices  58 us (36%)
  starting transfers between devices  47.9 us (30%)
  Pallas kernels  40.3 us (25%)
  between operations  13.7 us (9%)
    ppermute x27, waiting for transfers between devices, shift_by(): return lax.ppermute(x, axis, ring(by))  57.5 us
    ppermute x27, starting transfers between devices, shift_by(): return lax.ppermute(x, axis, ring(by))  42.8 us
    pallas_call x19, Pallas kernels, run(): pl.pallas_call(kernel, in_specs=[pl.BlockSpec(memory_space=pltpu.SMEM)] +...  40.3 us
  transfers between devices with their start and end apart: 41, of which 20 were waited for; matrix products, arithmetic and copies ran while one was open for 0% of the time, Pallas kernels for 19%

profile of v1, /device:TPU:0, one launch (start us, length us, event | category | flops | bytes accessed | tf_op | source)
XLA Modules:
  0.0 160.3 jit_solution(14973861510725465985)
XLA Ops:
  6.6 3.3 %shard_map.145 = (f32[1,1024]{1,0:T(1,128)S(1)}, bf16[1024,256]{1,0:T(8,128)(2,1)S(1)}, bf16[1024,256]{1,0:T(8,128)(2,1)S(1)}, bf16[1024,512]{1,0:T(8,128)(2,1)S...) custom-call(s32[4]{0:T(128)S(1)} %pad_add_fusion.sc, f32[1,1024]{1,0:T(1,128)} %bitcast.23, ...), custom_call_target="tpu_custom_call" | custom-call | flops 67108864 | tf_op jit(solution)/shard_map/pallas_call | solution.py:46
  9.9 2.3 %shard_map.146 = (bf16[1024,256]{1,0:T(8,128)(2,1)S(1)}, f32[1024,128]{1,0:T(8,128)S(1)}, f32[1024,128]{1,0:T(8,128)S(1)}, bf16[4,256,512]{2,1,0:T(8,128)(2,1)S(...) custom-call(s32[4]{0:T(128)S(1)} %pad_add_fusion.sc, ...), custom_call_target="tpu_custom_call" | custom-call | flops 536870912 | tf_op jit(solution)/shard_map/pallas_call | solution.py:46
  12.3 1.8 %collective-permute-start = (bf16[80,512]{1,0:T(8,128)(2,1)S(1)}, bf16[80,512]{1,0:T(8,128)(2,1)S(1)}, u32[]{:S(2)}, u32[]{:S(2)}) collective-permute-start(bf16[80,512]{1,0:T(8,128)(2,1)S(1)} %get-tuple-element.58), channel_id=1, source_target_pairs={{0,8},{8,16},{16,24},{24,0},{1,9},{9,17},{17,25},{25,1},{2,10},{10... | collective-permute-start | bytes 245768 | tf_op jit(solution)/shard_map/ppermute | solution.py:30
  14.1 2.9 %collective-permute-start.1 = (bf16[80,512]{1,0:T(8,128)(2,1)S(1)}, bf16[80,512]{1,0:T(8,128)(2,1)S(1)}, u32[]{:S(2)}, u32[]{:S(2)}) collective-permute-start(bf16[80,512]{1,0:T(8,128)(2,1)S(1)} %get-tuple-element.59), channel_id=1, source_target_pairs={{0,16},{8,24},{16,0},{24,8},{1,17},{9,25},{17,1},{25,9},{2,18},{10... | collective-permute-start | bytes 245768 | tf_op jit(solution)/shard_map/ppermute | solution.py:30
  17.0 1.3 collective-permute-start.2
  18.3 2.6 %collective-permute-done.1.r2 = bf16[80,512]{1,0:T(8,128)(2,1)S(1)} collective-permute-done((bf16[80,512]{1,0:T(8,128)(2,1)S(1)}, bf16[80,512]{1,0:T(8,128)(2,1)S(1)}, u32[]{:S(2)}, u32[]{:S(2)}) %collective-permute-start.1) | collective-permute-done | bytes 81952 | tf_op jit(solution)/shard_map/ppermute | solution.py:30
  20.9 0.5 collective-permute-done.2.r3
  21.4 0.7 shard_map.147
  22.1 2.0 %collective-permute-start.3 = (bf16[80,512]{1,0:T(8,128)(2,1)S(1)}, bf16[80,512]{1,0:T(8,128)(2,1)S(1)}, u32[]{:S(2)}, u32[]{:S(2)}) collective-permute-start(bf16[80,512]{1,0:T(8,128)(2,1)S(1)} %get-tuple-element.61), channel_id=1, source_target_pairs={{0,32},{32,64},{64,96},{96,0},{1,33},{33,65},{65,97},{97,1},{2,34}... | collective-permute-start | bytes 245768 | tf_op jit(solution)/shard_map/ppermute | solution.py:30
  24.1 3.6 %collective-permute-start.4 = (bf16[80,512]{1,0:T(8,128)(2,1)S(1)}, bf16[80,512]{1,0:T(8,128)(2,1)S(1)}, u32[]{:S(2)}, u32[]{:S(2)}) collective-permute-start(bf16[80,512]{1,0:T(8,128)(2,1)S(1)} %get-tuple-element.61), channel_id=1, source_target_pairs={{0,64},{32,96},{64,0},{96,32},{1,65},{33,97},{65,1},{97,33},{2,66}... | collective-permute-start | bytes 245768 | tf_op jit(solution)/shard_map/ppermute | solution.py:30
  27.7 1.0 collective-permute-start.5
  28.7 2.1 %collective-permute-done.3.t1 = bf16[80,512]{1,0:T(8,128)(2,1)S(1)} collective-permute-done((bf16[80,512]{1,0:T(8,128)(2,1)S(1)}, bf16[80,512]{1,0:T(8,128)(2,1)S(1)}, u32[]{:S(2)}, u32[]{:S(2)}) %collective-permute-start.3) | collective-permute-done | bytes 81952 | tf_op jit(solution)/shard_map/ppermute | solution.py:30
  30.8 4.2 %collective-permute-done.4.t2 = bf16[80,512]{1,0:T(8,128)(2,1)S(1)} collective-permute-done((bf16[80,512]{1,0:T(8,128)(2,1)S(1)}, bf16[80,512]{1,0:T(8,128)(2,1)S(1)}, u32[]{:S(2)}, u32[]{:S(2)}) %collective-permute-start.4) | collective-permute-done | bytes 81952 | tf_op jit(solution)/shard_map/ppermute | solution.py:30
  35.0 0.7 shard_map.148
  35.8 3.7 %collective-permute-start.7 = (bf16[64,512]{1,0:T(8,128)(2,1)S(1)}, bf16[64,512]{1,0:T(8,128)(2,1)S(1)}, u32[]{:S(2)}, u32[]{:S(2)}) collective-permute-start(bf16[64,512]{1,0:T(8,128)(2,1)S(1)} %get-tuple-element.66), channel_id=1, source_target_pairs={{0,16},{8,24},{16,0},{24,8},{1,17},{9,25},{17,1},{25,9},{2,18},{10... | collective-permute-start | bytes 196616 | tf_op jit(solution)/shard_map/ppermute | solution.py:30
  39.7 2.4 %shard_map.149 = (f32[2,512,512]{2,1,0:T(8,128)S(1)}, bf16[2,512,256]{2,1,0:T(8,128)(2,1)S(1)}) custom-call(s32[4]{0:T(128)S(1)} %pad_add_fusion.sc, f32[256,16]{1,0:T(8,128)S(1)} %get-tuple-element.68.down, f32[16,256]{1,0:T(8,128)S(1)} %get-tuple-element.69.across, bf16[1024,256]{1,0:T(8,128)(2,1)S(1)} %get-tuple-element.70.kr, ...), custom_call_target="tpu_custom_call" | custom-call | flops 805306368 | tf_op jit(solution)/shard_map/pallas_call | solution.py:46
  42.5 1.3 collective-permute-done.8.i3
  43.8 2.4 %shard_map.150 = (bf16[4,64,2048]{2,1,0:T(8,128)(2,1)S(1)}, bf16[4,64,2048]{2,1,0:T(8,128)(2,1)S(1)}) custom-call(s32[4]{0:T(128)S(1)} %pad_add_fusion.sc, f32[1,1024]{1,0:T(1,128)S(1)} %get-tuple-element.53.log, bf16[64,512]{1,0:T(8,128)(2,1)S(1)} %get-tuple-element.64.i0, bf16[64,512]{1,0:T(8,128)(2,1)S(1)} %collective-permute-done.6.i1, ...), custom_call_target="tpu_custom_call" | custom-call | flops 1207959552 | tf_op jit(solution)/shard_map/pallas_call | solution.py:46
  46.3 2.4 %shard_map.153 = (bf16[4,64,2048]{2,1,0:T(8,128)(2,1)S(1)}, bf16[4,64,2048]{2,1,0:T(8,128)(2,1)S(1)}) custom-call(s32[4]{0:T(128)S(1)} %pad_add_fusion.sc, f32[1,1024]{1,0:T(1,128)S(1)} %get-tuple-element.53.log, bf16[64,512]{1,0:T(8,128)(2,1)S(1)} %get-tuple-element.64.i0, bf16[64,512]{1,0:T(8,128)(2,1)S(1)} %collective-permute-done.6.i1, ...), custom_call_target="tpu_custom_call" | custom-call | flops 1207959552 | tf_op jit(solution)/shard_map/pallas_call | solution.py:46
  48.7 0.6 collective-permute-start.20
  49.3 0.7 shard_map.151
  50.0 1.6 collective-permute-start.10
  51.6 2.8 %collective-permute-start.11 = (bf16[64,2048]{1,0:T(8,128)(2,1)S(1)}, bf16[64,2048]{1,0:T(8,128)(2,1)S(1)}, u32[]{:S(2)}, u32[]{:S(2)}) collective-permute-start(bf16[64,2048]{1,0:T(8,128)(2,1)S(1)} %get-tuple-element.80), channel_id=1, source_target_pairs={{0,4},{2,6},{4,0},{6,2},{1,5},{3,7},{5,1},{7,3},{8,12},{10,14},{12... | collective-permute-start | bytes 786440 | tf_op jit(solution)/shard_map/ppermute | solution.py:30
  54.3 1.4 collective-permute-start.12
  55.7 0.7 shard_map.154
  56.5 0.7 collective-permute-start.21
  57.2 0.8 collective-permute-start.22
  58.0 1.5 collective-permute-done.10.r1
  59.5 2.5 %collective-permute-start.23 = (bf16[64,2048]{1,0:T(8,128)(2,1)S(1)}, bf16[64,2048]{1,0:T(8,128)(2,1)S(1)}, u32[]{:S(2)}, u32[]{:S(2)}) collective-permute-start(bf16[64,2048]{1,0:T(8,128)(2,1)S(1)} %get-tuple-element.86), channel_id=1, source_target_pairs={{0,6},{2,0},{4,2},{6,4},{1,7},{3,1},{5,3},{7,5},{8,14},{10,8},{12,... | collective-permute-start | bytes 786440 | tf_op jit(solution)/shard_map/ppermute | solution.py:30
  62.1 5.1 %collective-permute-done.11.r2 = bf16[64,2048]{1,0:T(8,128)(2,1)S(1)} collective-permute-done((bf16[64,2048]{1,0:T(8,128)(2,1)S(1)}, bf16[64,2048]{1,0:T(8,128)(2,1)S(1)}, u32[]{:S(2)}, u32[]{:S(2)}) %collective-permute-start.11) | collective-permute-done | bytes 262176 | tf_op jit(solution)/shard_map/ppermute | solution.py:30
  67.2 1.0 shard_map.152.refs_0_
  68.2 2.3 %collective-permute-start.13 = (bf16[64,2048]{1,0:T(8,128)(2,1)S(1)}, bf16[64,2048]{1,0:T(8,128)(2,1)S(1)}, u32[]{:S(2)}, u32[]{:S(2)}) collective-permute-start(bf16[64,2048]{1,0:T(8,128)(2,1)S(1)} %shard_map.152.refs_0_), channel_id=1, source_target_pairs={{0,2},{2,4},{4,6},{6,0},{1,3},{3,5},{5,7},{7,1},{8,10},{10,12},{12... | collective-permute-start | bytes 786440 | tf_op jit(solution)/shard_map/ppermute | solution.py:30
  70.5 1.7 %collective-permute-start.14 = (bf16[64,2048]{1,0:T(8,128)(2,1)S(1)}, bf16[64,2048]{1,0:T(8,128)(2,1)S(1)}, u32[]{:S(2)}, u32[]{:S(2)}) collective-permute-start(bf16[64,2048]{1,0:T(8,128)(2,1)S(1)} %shard_map.152.refs_0_), channel_id=1, source_target_pairs={{0,4},{2,6},{4,0},{6,2},{1,5},{3,7},{5,1},{7,3},{8,12},{10,14},{12... | collective-permute-start | bytes 786440 | tf_op jit(solution)/shard_map/ppermute | solution.py:30
  72.2 6.2 %collective-permute-done.22.r2 = bf16[64,2048]{1,0:T(8,128)(2,1)S(1)} collective-permute-done((bf16[64,2048]{1,0:T(8,128)(2,1)S(1)}, bf16[64,2048]{1,0:T(8,128)(2,1)S(1)}, u32[]{:S(2)}, u32[]{:S(2)}) %collective-permute-start.22) | collective-permute-done | bytes 262176 | tf_op jit(solution)/shard_map/ppermute | solution.py:30
  78.4 1.0 shard_map.155.refs_0_
  79.4 0.7 collective-permute-start.24
  80.1 3.1 %collective-permute-start.25 = (bf16[64,2048]{1,0:T(8,128)(2,1)S(1)}, bf16[64,2048]{1,0:T(8,128)(2,1)S(1)}, u32[]{:S(2)}, u32[]{:S(2)}) collective-permute-start(bf16[64,2048]{1,0:T(8,128)(2,1)S(1)} %shard_map.155.refs_0_), channel_id=1, source_target_pairs={{0,4},{2,6},{4,0},{6,2},{1,5},{3,7},{5,1},{7,3},{8,12},{10,14},{12... | collective-permute-start | bytes 786440 | tf_op jit(solution)/shard_map/ppermute | solution.py:30
  83.2 1.7 %collective-permute-start.26 = (bf16[64,2048]{1,0:T(8,128)(2,1)S(1)}, bf16[64,2048]{1,0:T(8,128)(2,1)S(1)}, u32[]{:S(2)}, u32[]{:S(2)}) collective-permute-start(bf16[64,2048]{1,0:T(8,128)(2,1)S(1)} %shard_map.155.refs_0_), channel_id=1, source_target_pairs={{0,6},{2,0},{4,2},{6,4},{1,7},{3,1},{5,3},{7,5},{8,14},{10,8},{12,... | collective-permute-start | bytes 786440 | tf_op jit(solution)/shard_map/ppermute | solution.py:30
  85.0 4.7 %collective-permute-done.14.refs_2_ = bf16[64,2048]{1,0:T(8,128)(2,1)S(1)} collective-permute-done((bf16[64,2048]{1,0:T(8,128)(2,1)S(1)}, bf16[64,2048]{1,0:T(8,128)(2,1)S(1)}, u32[]{:S(2)}, u32[]{:S(2)}) %collective-permute-start.14) | collective-permute-done | bytes 262176 | tf_op jit(solution)/shard_map/ppermute | solution.py:30
  89.7 4.1 %collective-permute-done.24.refs_1_ = bf16[64,2048]{1,0:T(8,128)(2,1)S(1)} collective-permute-done((bf16[64,2048]{1,0:T(8,128)(2,1)S(1)}, bf16[64,2048]{1,0:T(8,128)(2,1)S(1)}, u32[]{:S(2)}, u32[]{:S(2)}) %collective-permute-start.24) | collective-permute-done | bytes 262176 | tf_op jit(solution)/shard_map/ppermute | solution.py:30
  93.9 6.1 %collective-permute-done.25.refs_2_ = bf16[64,2048]{1,0:T(8,128)(2,1)S(1)} collective-permute-done((bf16[64,2048]{1,0:T(8,128)(2,1)S(1)}, bf16[64,2048]{1,0:T(8,128)(2,1)S(1)}, u32[]{:S(2)}, u32[]{:S(2)}) %collective-permute-start.25) | collective-permute-done | bytes 262176 | tf_op jit(solution)/shard_map/ppermute | solution.py:30
  100.0 0.5 collective-permute-start.30
  100.7 0.5 collective-permute-start.17
  101.9 5.7 %shard_map.156 = (bf16[512,1408]{1,0:T(8,128)(2,1)S(1)}, bf16[2048,1408]{1,0:T(8,128)(2,1)S(1)}, bf16[2048,768]{1,0:T(8,128)(2,1)S(1)}) custom-call(s32[4]{0:T(128)S(1)} %pad_add_fusion.sc, bf16[64,2048]{1,0:T(8,128)(2,1)S(1)} %shard_map.155.refs_0_, bf16[64,2048]{1,0:T(8,128)(2,1)S(1)} %collective-permute-done.24.refs_1_, ...), custom_call_target="tpu_custom_call" | custom-call | flops 2952790016 | tf_op jit(solution)/shard_map/pallas_call | solution.py:46
  107.7 2.2 %collective-permute-start.31 = (bf16[16,1408]{1,0:T(8,128)(2,1)S(1)}, bf16[16,1408]{1,0:T(8,128)(2,1)S(1)}, u32[]{:S(2)}, u32[]{:S(2)}) collective-permute-start(bf16[16,1408]{1,0:T(8,128)(2,1)S(1)} %slice.15), channel_id=1, source_target_pairs={{0,8},{8,16},{16,24},{24,32},{32,40},{40,48},{48,56},{56,64},{64,7... | collective-permute-start | bytes 135176 | tf_op jit(solution)/shard_map/ppermute | solution.py:468
  109.9 4.6 %shard_map.157.mine.other = bf16[512,1408]{1,0:T(8,128)(2,1)S(1)} custom-call(s32[4]{0:T(128)S(1)} %pad_add_fusion.sc, bf16[64,2048]{1,0:T(8,128)(2,1)S(1)} %shard_map.152.refs_0_, bf16[64,2048]{1,0:T(8,128)(2,1)S(1)} %collective-permute-done.13.refs_1_, bf16[64,2048]{1,0:T(8,128)(2,1)S(1)} %collective-permute-done.14.refs_2_, ...), custom_call_target="tpu_custom_call" | custom-call | flops 2952790016 | tf_op jit(solution)/shard_map/pallas_call | solution.py:46
  114.6 4.2 %shard_map.160 = (bf16[4,64,2048]{2,1,0:T(8,128)(2,1)S(1)}, bf16[4,64,2048]{2,1,0:T(8,128)(2,1)S(1)}) custom-call(s32[4]{0:T(128)S(1)} %pad_add_fusion.sc, bf16[512,1408]{1,0:T(8,128)(2,1)S(1)} %get-tuple-element.89.other.mine, bf16[512,1408]{1,0:T(8,128)(2,1)S(1)} %shard_map.157.mine.other, bf16[16,1408]{1,0:T(8,128)(2,1)S(1)} %collective-permute-done.31.edge, ...), custom_call_target="tpu_custom_call" | custom-call | flops 2952790016 | tf_op jit(solution)/shard_map/pallas_call | solution.py:46
  119.1 4.2 %shard_map.158 = (bf16[4,64,2048]{2,1,0:T(8,128)(2,1)S(1)}, bf16[4,64,2048]{2,1,0:T(8,128)(2,1)S(1)}) custom-call(s32[4]{0:T(128)S(1)} %pad_add_fusion.sc, bf16[512,1408]{1,0:T(8,128)(2,1)S(1)} %shard_map.157.mine.other, bf16[512,1408]{1,0:T(8,128)(2,1)S(1)} %get-tuple-element.89.other.mine, bf16[16,1408]{1,0:T(8,128)(2,1)S(1)} %collective-permute-done.31.edge, ...), custom_call_target="tpu_custom_call" | custom-call | flops 2952790016 | tf_op jit(solution)/shard_map/pallas_call | solution.py:46
  123.4 0.6 collective-permute-start.32
  124.0 0.7 shard_map.161
  124.7 1.1 collective-permute-start.37
  125.8 2.3 %collective-permute-start.38 = (bf16[64,2048]{1,0:T(8,128)(2,1)S(1)}, bf16[64,2048]{1,0:T(8,128)(2,1)S(1)}, u32[]{:S(2)}, u32[]{:S(2)}) collective-permute-start(bf16[64,2048]{1,0:T(8,128)(2,1)S(1)} %get-tuple-element.99), channel_id=1, source_target_pairs={{0,4},{2,6},{4,0},{6,2},{1,5},{3,7},{5,1},{7,3},{8,12},{10,14},{12... | collective-permute-start | bytes 786440 | tf_op jit(solution)/shard_map/ppermute | solution.py:30
  128.2 0.9 collective-permute-start.39
  129.1 0.7 shard_map.159
  129.8 1.2 collective-permute-start.33
  131.0 1.2 collective-permute-start.34
  132.2 8.4 %collective-permute-done.37.r1 = bf16[64,2048]{1,0:T(8,128)(2,1)S(1)} collective-permute-done((bf16[64,2048]{1,0:T(8,128)(2,1)S(1)}, bf16[64,2048]{1,0:T(8,128)(2,1)S(1)}, u32[]{:S(2)}, u32[]{:S(2)}) %collective-permute-start.37) | collective-permute-done | bytes 262176 | tf_op jit(solution)/shard_map/ppermute | solution.py:30
  140.6 0.4 collective-permute-done.38.r2
  141.0 0.7 collective-permute-done.39.r3
  141.7 1.0 shard_map.162.rest_0_
  142.6 3.5 %collective-permute-done.33.r1 = bf16[64,2048]{1,0:T(8,128)(2,1)S(1)} collective-permute-done((bf16[64,2048]{1,0:T(8,128)(2,1)S(1)}, bf16[64,2048]{1,0:T(8,128)(2,1)S(1)}, u32[]{:S(2)}, u32[]{:S(2)}) %collective-permute-start.33) | collective-permute-done | bytes 262176 | tf_op jit(solution)/shard_map/ppermute | solution.py:30
  146.2 5.1 %collective-permute-done.34.r2 = bf16[64,2048]{1,0:T(8,128)(2,1)S(1)} collective-permute-done((bf16[64,2048]{1,0:T(8,128)(2,1)S(1)}, bf16[64,2048]{1,0:T(8,128)(2,1)S(1)}, u32[]{:S(2)}, u32[]{:S(2)}) %collective-permute-start.34) | collective-permute-done | bytes 262176 | tf_op jit(solution)/shard_map/ppermute | solution.py:30
  151.3 0.4 collective-permute-done.35.r3
  151.7 1.7 %shard_map.163 = bf16[128,2048]{1,0:T(8,128)(2,1)} custom-call(s32[4]{0:T(128)S(1)} %pad_add_fusion.sc, bf16[4,64,2048]{2,1,0:T(8,128)(2,1)S(1)} %get-tuple-element.91.keep, bf16[4,64,2048]{2,1,0:T(8,128)(2,1)S(1)} %collective-permute-done.32.got, bf16[64,2048]{1,0:T(8,128)(2,1)S(1)} %collective-permute-done.33.r1, ...), custom_call_target="tpu_custom_call" | custom-call | flops 52428800 | tf_op jit(solution)/shard_map/pallas_call | solution.py:46
  (59 shorter events, 2.2 us)
Async XLA Ops:
  6.5 95.4 %all-gather.2.cloned.1.call-start = ((), (), s32[]{:S(2)}) async-start(), calls=%async_computation | async-start | bytes 9469952 | tf_op jit(solution)/shard_map/all_gather | solution.py:431
  12.3 31.6 %copy-start.1 = (bf16[512,2048]{1,0:T(8,128)(2,1)S(1)}, bf16[512,2048]{1,0:T(8,128)(2,1)}, u32[]{:S(2)}) copy-start(bf16[512,2048]{1,0:T(8,128)(2,1)} %weight.3) | copy-start | bytes 6291460
  12.3 31.5 %copy-start.2 = (bf16[1024,512]{1,0:T(8,128)(2,1)S(1)}, bf16[1024,512]{1,0:T(8,128)(2,1)}, u32[]{:S(2)}) copy-start(bf16[1024,512]{1,0:T(8,128)(2,1)} %param.18) | copy-start | bytes 3145732
  12.3 6.0 %collective-permute-start = (bf16[80,512]{1,0:T(8,128)(2,1)S(1)}, bf16[80,512]{1,0:T(8,128)(2,1)S(1)}, u32[]{:S(2)}, u32[]{:S(2)}) collective-permute-start(bf16[80,512]{1,0:T(8,128)(2,1)S(1)} %get-tuple-element.58), channel_id=1, source_target_pairs={{0,8},{8,16},{16,24},{24,0},{1,9},{9,17},{17,25},{25,1},{2,10},{10... | collective-permute-start | bytes 245768 | tf_op jit(solution)/shard_map/ppermute | solution.py:30
  14.1 6.8 %collective-permute-start.1 = (bf16[80,512]{1,0:T(8,128)(2,1)S(1)}, bf16[80,512]{1,0:T(8,128)(2,1)S(1)}, u32[]{:S(2)}, u32[]{:S(2)}) collective-permute-start(bf16[80,512]{1,0:T(8,128)(2,1)S(1)} %get-tuple-element.59), channel_id=1, source_target_pairs={{0,16},{8,24},{16,0},{24,8},{1,17},{9,25},{17,1},{25,9},{2,18},{10... | collective-permute-start | bytes 245768 | tf_op jit(solution)/shard_map/ppermute | solution.py:30
  17.0 4.4 %collective-permute-start.2 = (bf16[80,512]{1,0:T(8,128)(2,1)S(1)}, bf16[80,512]{1,0:T(8,128)(2,1)S(1)}, u32[]{:S(2)}, u32[]{:S(2)}) collective-permute-start(bf16[80,512]{1,0:T(8,128)(2,1)S(1)} %get-tuple-element.60), channel_id=1, source_target_pairs={{0,24},{8,0},{16,8},{24,16},{1,25},{9,1},{17,9},{25,17},{2,26},{10... | collective-permute-start | bytes 245768 | tf_op jit(solution)/shard_map/ppermute | solution.py:30
  22.1 8.7 %collective-permute-start.3 = (bf16[80,512]{1,0:T(8,128)(2,1)S(1)}, bf16[80,512]{1,0:T(8,128)(2,1)S(1)}, u32[]{:S(2)}, u32[]{:S(2)}) collective-permute-start(bf16[80,512]{1,0:T(8,128)(2,1)S(1)} %get-tuple-element.61), channel_id=1, source_target_pairs={{0,32},{32,64},{64,96},{96,0},{1,33},{33,65},{65,97},{97,1},{2,34}... | collective-permute-start | bytes 245768 | tf_op jit(solution)/shard_map/ppermute | solution.py:30
  24.1 10.9 %collective-permute-start.4 = (bf16[80,512]{1,0:T(8,128)(2,1)S(1)}, bf16[80,512]{1,0:T(8,128)(2,1)S(1)}, u32[]{:S(2)}, u32[]{:S(2)}) collective-permute-start(bf16[80,512]{1,0:T(8,128)(2,1)S(1)} %get-tuple-element.61), channel_id=1, source_target_pairs={{0,64},{32,96},{64,0},{96,32},{1,65},{33,97},{65,1},{97,33},{2,66}... | collective-permute-start | bytes 245768 | tf_op jit(solution)/shard_map/ppermute | solution.py:30
  27.7 7.4 %collective-permute-start.5 = (bf16[80,512]{1,0:T(8,128)(2,1)S(1)}, bf16[80,512]{1,0:T(8,128)(2,1)S(1)}, u32[]{:S(2)}, u32[]{:S(2)}) collective-permute-start(bf16[80,512]{1,0:T(8,128)(2,1)S(1)} %get-tuple-element.61), channel_id=1, source_target_pairs={{0,96},{32,0},{64,32},{96,64},{1,97},{33,1},{65,33},{97,65},{2,98}... | collective-permute-start | bytes 245768 | tf_op jit(solution)/shard_map/ppermute | solution.py:30
  35.7 6.4 %collective-permute-start.6 = (bf16[64,512]{1,0:T(8,128)(2,1)S(1)}, bf16[64,512]{1,0:T(8,128)(2,1)S(1)}, u32[]{:S(2)}, u32[]{:S(2)}) collective-permute-start(bf16[64,512]{1,0:T(8,128)(2,1)S(1)} %get-tuple-element.65), channel_id=1, source_target_pairs={{0,8},{8,16},{16,24},{24,0},{1,9},{9,17},{17,25},{25,1},{2,10},{10... | collective-permute-start | bytes 196616 | tf_op jit(solution)/shard_map/ppermute | solution.py:30
  35.8 6.7 %collective-permute-start.7 = (bf16[64,512]{1,0:T(8,128)(2,1)S(1)}, bf16[64,512]{1,0:T(8,128)(2,1)S(1)}, u32[]{:S(2)}, u32[]{:S(2)}) collective-permute-start(bf16[64,512]{1,0:T(8,128)(2,1)S(1)} %get-tuple-element.66), channel_id=1, source_target_pairs={{0,16},{8,24},{16,0},{24,8},{1,17},{9,25},{17,1},{25,9},{2,18},{10... | collective-permute-start | bytes 196616 | tf_op jit(solution)/shard_map/ppermute | solution.py:30
  39.6 4.3 %collective-permute-start.8 = (bf16[64,512]{1,0:T(8,128)(2,1)S(1)}, bf16[64,512]{1,0:T(8,128)(2,1)S(1)}, u32[]{:S(2)}, u32[]{:S(2)}) collective-permute-start(bf16[64,512]{1,0:T(8,128)(2,1)S(1)} %get-tuple-element.67), channel_id=1, source_target_pairs={{0,24},{8,0},{16,8},{24,16},{1,25},{9,1},{17,9},{25,17},{2,26},{10... | collective-permute-start | bytes 196616 | tf_op jit(solution)/shard_map/ppermute | solution.py:30
  46.2 3.1 %collective-permute-start.9 = (bf16[4,64,2048]{2,1,0:T(8,128)(2,1)S(1)}, bf16[4,64,2048]{2,1,0:T(8,128)(2,1)S(1)}, u32[]{:S(2)}, u32[]{:S(2)}) collective-permute-start(bf16[4,64,2048]{2,1,0:T(8,128)(2,1)S(1)} %get-tuple-element.78), channel_id=1, source_target_pairs={{0,1},{1,0},{2,3},{3,2},{4,5},{5,4},{6,7},{7,6},{8,9},{9,8},{10,11... | collective-permute-start | bytes 3145736 | tf_op jit(solution)/shard_map/ppermute | solution.py:38
  46.3 15.8 %copy-start.5 = (f32[2,3,704]{2,0,1:T(2,128)S(1)}, f32[2,3,704]{2,0,1:T(2,128)}, u32[]{:S(2)}) copy-start(f32[2,3,704]{2,0,1:T(2,128)} %param.26) | copy-start | bytes 50692
  48.7 18.5 %copy-start = (bf16[1024,2048]{1,0:T(8,128)(2,1)S(1)}, bf16[1024,2048]{1,0:T(8,128)(2,1)}, u32[]{:S(2)}) copy-start(bf16[1024,2048]{1,0:T(8,128)(2,1)} %param.20) | copy-start | bytes 12582916
  48.7 18.5 %copy-start.3 = (f32[2,2048]{1,0:T(2,128)S(1)}, f32[2,2048]{1,0:T(2,128)}, u32[]{:S(2)}) copy-start(f32[2,2048]{1,0:T(2,128)} %gain.7) | copy-start | bytes 49156
  48.7 18.5 %copy-start.4 = (f32[2,2048]{1,0:T(2,128)S(1)}, f32[2,2048]{1,0:T(2,128)}, u32[]{:S(2)}) copy-start(f32[2,2048]{1,0:T(2,128)} %shift.7) | copy-start | bytes 49156
  48.7 7.1 %collective-permute-start.20 = (bf16[4,64,2048]{2,1,0:T(8,128)(2,1)S(1)}, bf16[4,64,2048]{2,1,0:T(8,128)(2,1)S(1)}, u32[]{:S(2)}, u32[]{:S(2)}) collective-permute-start(bf16[4,64,2048]{2,1,0:T(8,128)(2,1)S(1)} %get-tuple-element.83), channel_id=1, source_target_pairs={{0,1},{1,0},{2,3},{3,2},{4,5},{5,4},{6,7},{7,6},{8,9},{9,8},{10,11... | collective-permute-start | bytes 3145736 | tf_op jit(solution)/shard_map/ppermute | solution.py:38
  50.0 9.5 %collective-permute-start.10 = (bf16[64,2048]{1,0:T(8,128)(2,1)S(1)}, bf16[64,2048]{1,0:T(8,128)(2,1)S(1)}, u32[]{:S(2)}, u32[]{:S(2)}) collective-permute-start(bf16[64,2048]{1,0:T(8,128)(2,1)S(1)} %get-tuple-element.79), channel_id=1, source_target_pairs={{0,2},{2,4},{4,6},{6,0},{1,3},{3,5},{5,7},{7,1},{8,10},{10,12},{12... | collective-permute-start | bytes 786440 | tf_op jit(solution)/shard_map/ppermute | solution.py:30
  51.6 15.6 %collective-permute-start.11 = (bf16[64,2048]{1,0:T(8,128)(2,1)S(1)}, bf16[64,2048]{1,0:T(8,128)(2,1)S(1)}, u32[]{:S(2)}, u32[]{:S(2)}) collective-permute-start(bf16[64,2048]{1,0:T(8,128)(2,1)S(1)} %get-tuple-element.80), channel_id=1, source_target_pairs={{0,4},{2,6},{4,0},{6,2},{1,5},{3,7},{5,1},{7,3},{8,12},{10,14},{12... | collective-permute-start | bytes 786440 | tf_op jit(solution)/shard_map/ppermute | solution.py:30
  54.3 12.8 %collective-permute-start.12 = (bf16[64,2048]{1,0:T(8,128)(2,1)S(1)}, bf16[64,2048]{1,0:T(8,128)(2,1)S(1)}, u32[]{:S(2)}, u32[]{:S(2)}) collective-permute-start(bf16[64,2048]{1,0:T(8,128)(2,1)S(1)} %get-tuple-element.81), channel_id=1, source_target_pairs={{0,6},{2,0},{4,2},{6,4},{1,7},{3,1},{5,3},{7,5},{8,14},{10,8},{12,... | collective-permute-start | bytes 786440 | tf_op jit(solution)/shard_map/ppermute | solution.py:30
  56.5 15.8 %collective-permute-start.21 = (bf16[64,2048]{1,0:T(8,128)(2,1)S(1)}, bf16[64,2048]{1,0:T(8,128)(2,1)S(1)}, u32[]{:S(2)}, u32[]{:S(2)}) collective-permute-start(bf16[64,2048]{1,0:T(8,128)(2,1)S(1)} %get-tuple-element.84), channel_id=1, source_target_pairs={{0,2},{2,4},{4,6},{6,0},{1,3},{3,5},{5,7},{7,1},{8,10},{10,12},{12... | collective-permute-start | bytes 786440 | tf_op jit(solution)/shard_map/ppermute | solution.py:30
  57.2 21.3 %collective-permute-start.22 = (bf16[64,2048]{1,0:T(8,128)(2,1)S(1)}, bf16[64,2048]{1,0:T(8,128)(2,1)S(1)}, u32[]{:S(2)}, u32[]{:S(2)}) collective-permute-start(bf16[64,2048]{1,0:T(8,128)(2,1)S(1)} %get-tuple-element.85), channel_id=1, source_target_pairs={{0,4},{2,6},{4,0},{6,2},{1,5},{3,7},{5,1},{7,3},{8,12},{10,14},{12... | collective-permute-start | bytes 786440 | tf_op jit(solution)/shard_map/ppermute | solution.py:30
  59.5 18.9 %collective-permute-start.23 = (bf16[64,2048]{1,0:T(8,128)(2,1)S(1)}, bf16[64,2048]{1,0:T(8,128)(2,1)S(1)}, u32[]{:S(2)}, u32[]{:S(2)}) collective-permute-start(bf16[64,2048]{1,0:T(8,128)(2,1)S(1)} %get-tuple-element.86), channel_id=1, source_target_pairs={{0,6},{2,0},{4,2},{6,4},{1,7},{3,1},{5,3},{7,5},{8,14},{10,8},{12,... | collective-permute-start | bytes 786440 | tf_op jit(solution)/shard_map/ppermute | solution.py:30
  68.1 16.8 %copy-start.6 = (f32[2,704]{1,0:T(2,128)S(1)}, f32[2,704]{1,0:T(2,128)}, u32[]{:S(2)}) copy-start(f32[2,704]{1,0:T(2,128)} %param.27) | copy-start | bytes 16900
  68.2 16.8 %collective-permute-start.13 = (bf16[64,2048]{1,0:T(8,128)(2,1)S(1)}, bf16[64,2048]{1,0:T(8,128)(2,1)S(1)}, u32[]{:S(2)}, u32[]{:S(2)}) collective-permute-start(bf16[64,2048]{1,0:T(8,128)(2,1)S(1)} %shard_map.152.refs_0_), channel_id=1, source_target_pairs={{0,2},{2,4},{4,6},{6,0},{1,3},{3,5},{5,7},{7,1},{8,10},{10,12},{12... | collective-permute-start | bytes 786440 | tf_op jit(solution)/shard_map/ppermute | solution.py:30
  70.5 19.2 %collective-permute-start.14 = (bf16[64,2048]{1,0:T(8,128)(2,1)S(1)}, bf16[64,2048]{1,0:T(8,128)(2,1)S(1)}, u32[]{:S(2)}, u32[]{:S(2)}) collective-permute-start(bf16[64,2048]{1,0:T(8,128)(2,1)S(1)} %shard_map.152.refs_0_), channel_id=1, source_target_pairs={{0,4},{2,6},{4,0},{6,2},{1,5},{3,7},{5,1},{7,3},{8,12},{10,14},{12... | collective-permute-start | bytes 786440 | tf_op jit(solution)/shard_map/ppermute | solution.py:30
  79.4 14.5 %collective-permute-start.24 = (bf16[64,2048]{1,0:T(8,128)(2,1)S(1)}, bf16[64,2048]{1,0:T(8,128)(2,1)S(1)}, u32[]{:S(2)}, u32[]{:S(2)}) collective-permute-start(bf16[64,2048]{1,0:T(8,128)(2,1)S(1)} %shard_map.155.refs_0_), channel_id=1, source_target_pairs={{0,2},{2,4},{4,6},{6,0},{1,3},{3,5},{5,7},{7,1},{8,10},{10,12},{12... | collective-permute-start | bytes 786440 | tf_op jit(solution)/shard_map/ppermute | solution.py:30
  80.1 19.9 %collective-permute-start.25 = (bf16[64,2048]{1,0:T(8,128)(2,1)S(1)}, bf16[64,2048]{1,0:T(8,128)(2,1)S(1)}, u32[]{:S(2)}, u32[]{:S(2)}) collective-permute-start(bf16[64,2048]{1,0:T(8,128)(2,1)S(1)} %shard_map.155.refs_0_), channel_id=1, source_target_pairs={{0,4},{2,6},{4,0},{6,2},{1,5},{3,7},{5,1},{7,3},{8,12},{10,14},{12... | collective-permute-start | bytes 786440 | tf_op jit(solution)/shard_map/ppermute | solution.py:30
  83.2 16.8 %collective-permute-start.26 = (bf16[64,2048]{1,0:T(8,128)(2,1)S(1)}, bf16[64,2048]{1,0:T(8,128)(2,1)S(1)}, u32[]{:S(2)}, u32[]{:S(2)}) collective-permute-start(bf16[64,2048]{1,0:T(8,128)(2,1)S(1)} %shard_map.155.refs_0_), channel_id=1, source_target_pairs={{0,6},{2,0},{4,2},{6,4},{1,7},{3,1},{5,3},{7,5},{8,14},{10,8},{12,... | collective-permute-start | bytes 786440 | tf_op jit(solution)/shard_map/ppermute | solution.py:30
  85.0 15.7 %collective-permute-start.15 = (bf16[64,2048]{1,0:T(8,128)(2,1)S(1)}, bf16[64,2048]{1,0:T(8,128)(2,1)S(1)}, u32[]{:S(2)}, u32[]{:S(2)}) collective-permute-start(bf16[64,2048]{1,0:T(8,128)(2,1)S(1)} %shard_map.152.refs_0_), channel_id=1, source_target_pairs={{0,6},{2,0},{4,2},{6,4},{1,7},{3,1},{5,3},{7,5},{8,14},{10,8},{12,... | collective-permute-start | bytes 786440 | tf_op jit(solution)/shard_map/ppermute | solution.py:30
  89.7 11.0 %collective-permute-start.27 = (bf16[64,2048]{1,0:T(8,128)(2,1)S(1)}, bf16[64,2048]{1,0:T(8,128)(2,1)S(1)}, u32[]{:S(2)}, u32[]{:S(2)}) collective-permute-start(bf16[64,2048]{1,0:T(8,128)(2,1)S(1)} %shard_map.155.refs_0_), channel_id=1, source_target_pairs={{0,1},{1,0},{2,3},{3,2},{4,5},{5,4},{6,7},{7,6},{8,9},{9,8},{10,11... | collective-permute-start | bytes 786440 | tf_op jit(solution)/shard_map/ppermute | solution.py:38
  93.9 7.4 %collective-permute-start.28 = (bf16[64,2048]{1,0:T(8,128)(2,1)S(1)}, bf16[64,2048]{1,0:T(8,128)(2,1)S(1)}, u32[]{:S(2)}, u32[]{:S(2)}) collective-permute-start(bf16[64,2048]{1,0:T(8,128)(2,1)S(1)} %collective-permute-done.24.refs_1_), channel_id=1, source_target_pairs={{0,1},{1,0},{2,3},{3,2},{4,5},{5,4},{6,7},{7,6},{8,9},{9,8},{10,11... | collective-permute-start | bytes 786440 | tf_op jit(solution)/shard_map/ppermute | solution.py:38
  100.0 1.5 collective-permute-start.29
  100.0 1.9 %collective-permute-start.30 = (bf16[64,2048]{1,0:T(8,128)(2,1)S(1)}, bf16[64,2048]{1,0:T(8,128)(2,1)S(1)}, u32[]{:S(2)}, u32[]{:S(2)}) collective-permute-start(bf16[64,2048]{1,0:T(8,128)(2,1)S(1)} %collective-permute-done.26.refs_3_), channel_id=1, source_target_pairs={{0,1},{1,0},{2,3},{3,2},{4,5},{5,4},{6,7},{7,6},{8,9},{9,8},{10,11... | collective-permute-start | bytes 786440 | tf_op jit(solution)/shard_map/ppermute | solution.py:38
  100.7 9.2 %collective-permute-start.16 = (bf16[64,2048]{1,0:T(8,128)(2,1)S(1)}, bf16[64,2048]{1,0:T(8,128)(2,1)S(1)}, u32[]{:S(2)}, u32[]{:S(2)}) collective-permute-start(bf16[64,2048]{1,0:T(8,128)(2,1)S(1)} %shard_map.152.refs_0_), channel_id=1, source_target_pairs={{0,1},{1,0},{2,3},{3,2},{4,5},{5,4},{6,7},{7,6},{8,9},{9,8},{10,11... | collective-permute-start | bytes 786440 | tf_op jit(solution)/shard_map/ppermute | solution.py:38
  100.7 9.2 %collective-permute-start.17 = (bf16[64,2048]{1,0:T(8,128)(2,1)S(1)}, bf16[64,2048]{1,0:T(8,128)(2,1)}, u32[]{:S(2)}, u32[]{:S(2)}) collective-permute-start(bf16[64,2048]{1,0:T(8,128)(2,1)S(1)} %collective-permute-done.13.refs_1_), channel_id=1, source_target_pairs={{0,1},{1,0},{2,3},{3,2},{4,5},{5,4},{6,7},{7,6},{8,9},{9,8},{10,11... | collective-permute-start | bytes 786440 | tf_op jit(solution)/shard_map/ppermute | solution.py:38
  101.2 8.7 %collective-permute-start.18 = (bf16[64,2048]{1,0:T(8,128)(2,1)S(1)}, bf16[64,2048]{1,0:T(8,128)(2,1)}, u32[]{:S(2)}, u32[]{:S(2)}) collective-permute-start(bf16[64,2048]{1,0:T(8,128)(2,1)S(1)} %collective-permute-done.14.refs_2_), channel_id=1, source_target_pairs={{0,1},{1,0},{2,3},{3,2},{4,5},{5,4},{6,7},{7,6},{8,9},{9,8},{10,11... | collective-permute-start | bytes 786440 | tf_op jit(solution)/shard_map/ppermute | solution.py:38
  101.5 8.4 %collective-permute-start.19 = (bf16[64,2048]{1,0:T(8,128)(2,1)S(1)}, bf16[64,2048]{1,0:T(8,128)(2,1)}, u32[]{:S(2)}, u32[]{:S(2)}) collective-permute-start(bf16[64,2048]{1,0:T(8,128)(2,1)S(1)} %collective-permute-done.15.refs_3_), channel_id=1, source_target_pairs={{0,1},{1,0},{2,3},{3,2},{4,5},{5,4},{6,7},{7,6},{8,9},{9,8},{10,11... | collective-permute-start | bytes 786440 | tf_op jit(solution)/shard_map/ppermute | solution.py:38
  107.7 6.9 %collective-permute-start.31 = (bf16[16,1408]{1,0:T(8,128)(2,1)S(1)}, bf16[16,1408]{1,0:T(8,128)(2,1)S(1)}, u32[]{:S(2)}, u32[]{:S(2)}) collective-permute-start(bf16[16,1408]{1,0:T(8,128)(2,1)S(1)} %slice.15), channel_id=1, source_target_pairs={{0,8},{8,16},{16,24},{24,32},{32,40},{40,48},{48,56},{56,64},{64,7... | collective-permute-start | bytes 135176 | tf_op jit(solution)/shard_map/ppermute | solution.py:468
  118.8 5.1 %collective-permute-start.36 = (bf16[4,64,2048]{2,1,0:T(8,128)(2,1)S(1)}, bf16[4,64,2048]{2,1,0:T(8,128)(2,1)S(1)}, u32[]{:S(2)}, u32[]{:S(2)}) collective-permute-start(bf16[4,64,2048]{2,1,0:T(8,128)(2,1)S(1)} %get-tuple-element.97), channel_id=1, source_target_pairs={{0,1},{1,0},{2,3},{3,2},{4,5},{5,4},{6,7},{7,6},{8,9},{9,8},{10,11... | collective-permute-start | bytes 3145736 | tf_op jit(solution)/shard_map/ppermute | solution.py:38
  123.4 5.7 %collective-permute-start.32 = (bf16[4,64,2048]{2,1,0:T(8,128)(2,1)S(1)}, bf16[4,64,2048]{2,1,0:T(8,128)(2,1)S(1)}, u32[]{:S(2)}, u32[]{:S(2)}) collective-permute-start(bf16[4,64,2048]{2,1,0:T(8,128)(2,1)S(1)} %get-tuple-element.92), channel_id=1, source_target_pairs={{0,1},{1,0},{2,3},{3,2},{4,5},{5,4},{6,7},{7,6},{8,9},{9,8},{10,11... | collective-permute-start | bytes 3145736 | tf_op jit(solution)/shard_map/ppermute | solution.py:38
  124.7 15.8 %collective-permute-start.37 = (bf16[64,2048]{1,0:T(8,128)(2,1)S(1)}, bf16[64,2048]{1,0:T(8,128)(2,1)S(1)}, u32[]{:S(2)}, u32[]{:S(2)}) collective-permute-start(bf16[64,2048]{1,0:T(8,128)(2,1)S(1)} %get-tuple-element.98), channel_id=1, source_target_pairs={{0,2},{2,4},{4,6},{6,0},{1,3},{3,5},{5,7},{7,1},{8,10},{10,12},{12... | collective-permute-start | bytes 786440 | tf_op jit(solution)/shard_map/ppermute | solution.py:30
  125.8 15.2 %collective-permute-start.38 = (bf16[64,2048]{1,0:T(8,128)(2,1)S(1)}, bf16[64,2048]{1,0:T(8,128)(2,1)S(1)}, u32[]{:S(2)}, u32[]{:S(2)}) collective-permute-start(bf16[64,2048]{1,0:T(8,128)(2,1)S(1)} %get-tuple-element.99), channel_id=1, source_target_pairs={{0,4},{2,6},{4,0},{6,2},{1,5},{3,7},{5,1},{7,3},{8,12},{10,14},{12... | collective-permute-start | bytes 786440 | tf_op jit(solution)/shard_map/ppermute | solution.py:30
  128.2 13.5 %collective-permute-start.39 = (bf16[64,2048]{1,0:T(8,128)(2,1)S(1)}, bf16[64,2048]{1,0:T(8,128)(2,1)S(1)}, u32[]{:S(2)}, u32[]{:S(2)}) collective-permute-start(bf16[64,2048]{1,0:T(8,128)(2,1)S(1)} %get-tuple-element.100), channel_id=1, source_target_pairs={{0,6},{2,0},{4,2},{6,4},{1,7},{3,1},{5,3},{7,5},{8,14},{10,8},{12,... | collective-permute-start | bytes 786440 | tf_op jit(solution)/shard_map/ppermute | solution.py:30
  129.8 16.3 %collective-permute-start.33 = (bf16[64,2048]{1,0:T(8,128)(2,1)S(1)}, bf16[64,2048]{1,0:T(8,128)(2,1)S(1)}, u32[]{:S(2)}, u32[]{:S(2)}) collective-permute-start(bf16[64,2048]{1,0:T(8,128)(2,1)S(1)} %get-tuple-element.93), channel_id=1, source_target_pairs={{0,2},{2,4},{4,6},{6,0},{1,3},{3,5},{5,7},{7,1},{8,10},{10,12},{12... | collective-permute-start | bytes 786440 | tf_op jit(solution)/shard_map/ppermute | solution.py:30
  131.0 20.3 %collective-permute-start.34 = (bf16[64,2048]{1,0:T(8,128)(2,1)S(1)}, bf16[64,2048]{1,0:T(8,128)(2,1)S(1)}, u32[]{:S(2)}, u32[]{:S(2)}) collective-permute-start(bf16[64,2048]{1,0:T(8,128)(2,1)S(1)} %get-tuple-element.94), channel_id=1, source_target_pairs={{0,4},{2,6},{4,0},{6,2},{1,5},{3,7},{5,1},{7,3},{8,12},{10,14},{12... | collective-permute-start | bytes 786440 | tf_op jit(solution)/shard_map/ppermute | solution.py:30
  140.6 11.2 %collective-permute-start.35 = (bf16[64,2048]{1,0:T(8,128)(2,1)S(1)}, bf16[64,2048]{1,0:T(8,128)(2,1)S(1)}, u32[]{:S(2)}, u32[]{:S(2)}) collective-permute-start(bf16[64,2048]{1,0:T(8,128)(2,1)S(1)} %get-tuple-element.95), channel_id=1, source_target_pairs={{0,6},{2,0},{4,2},{6,4},{1,7},{3,1},{5,3},{7,5},{8,14},{10,8},{12,... | collective-permute-start | bytes 786440 | tf_op jit(solution)/shard_map/ppermute | solution.py:30
Sparse Core Ops, SparseCore 0:
  10.1 77.5 all-gather.1

commit v2 on v1

--- a/solution.py
+++ b/solution.py
@@ -203,14 +203,13 @@
     lax.fori_loop(0, kr.shape[0] // BLOCK, step, 0)
 
 
-def heads_kernel(sc, log, i0, i1, i2, i3, within, scaled, gate, weight, keep, send, start, carried, chunk):
+def gated_kernel(sc, log, i0, i1, i2, i3, within, scaled, gate, out, start, carried, chunk):
     rows = i0.shape[0]
     for d, piece in enumerate((i0, i1, i2, i3)):
         at = pl.multiple_of(lax.rem(sc[1] + 4 - d, 4) * rows, rows)
         start[pl.ds(at, rows), :] = piece[...]
     order = lax.broadcasted_iota(jnp.int32, log.shape, 1)
-    n = keep.shape[1]
-    south = sc[3] == 0
+    n = out.shape[0] // 8
     carried[...] = jnp.dot(scaled[chunk], start[...], preferred_element_type=f32)
     gated = []
     for b in range(log.shape[1] // BLOCK):
@@ -221,8 +220,16 @@
         spread = jnp.mean(centred * centred, axis=1, keepdims=True)
         g = jnp.concatenate([gate[2 * b, chunk], gate[2 * b + 1, chunk]], axis=0).astype(f32)
         gated.append((g * jax.nn.sigmoid(g) * (centred * lax.rsqrt(spread + EPS))).astype(bf16))
-    gated = jnp.concatenate(gated, axis=0)
-    place(keep, send, sc, south, lambda cols: jnp.dot(gated, weight[:, cols], preferred_element_type=f32))
+    out[...] = jnp.concatenate(gated, axis=0)
+
+
+def heads_project_kernel(sc, gated, weight, keep, send):
+    place(keep, send, sc, sc[3] == 0, lambda cols: jnp.dot(gated[...], weight[:, cols], preferred_element_type=f32))
+
+
+def heads_kernel(sc, log, i0, i1, i2, i3, within, scaled, gate, weight, keep, send, start, carried, gated, chunk):
+    gated_kernel(sc, log, i0, i1, i2, i3, within, scaled, gate, gated, start, carried, chunk)
+    heads_project_kernel(sc, gated, weight, keep, send)
 
 
 def place(keep, send, sc, south, product, tile=512):
@@ -367,8 +374,8 @@
     )[0]
 
 
-def down_kernel(sc, mine, other, edge, taps, bias, weight, keep, send, active, chunk):
-    n = keep.shape[1]
+def activate_kernel(sc, mine, other, edge, taps, bias, active, chunk):
+    n = mine.shape[0] // 8
     hidden = active.shape[1]
 
     def conv_group(t, _):
@@ -386,15 +393,31 @@
         return 0
 
     lax.fori_loop(0, 8, conv_group, 0)
+
+
+def project_kernel(sc, active, weight, keep, send):
+    hidden = active.shape[1]
     place(keep, send, sc, sc[3] == 0, lambda cols: lax.dot_general(
         active[...], weight[cols, :hidden], (((1,), (1,)), ((), ())), preferred_element_type=f32
     ))
+
+
+def down_kernel(sc, mine, other, edge, taps, bias, weight, keep, send, active, chunk):
+    activate_kernel(sc, mine, other, edge, taps, bias, active, chunk)
+    project_kernel(sc, active, weight, keep, send)
 
 
 def down_project(sc, mine, other, edge, taps, bias, weights, width, chunk):
     rows, double = mine.shape
     n = rows // 8
     shape = ((4, n, width), bf16)
+    hidden = ((rows, double // 2), bf16)
+    if chunk == 0:
+        sources = (mine, other, edge, taps, bias)
+        active = run(
+            functools.partial(activate_kernel, chunk=chunk), sc, sources, [hidden], flops=rows * width * double
+        )[0]
+        return run(project_kernel, sc, (active, weights), [shape, shape], flops=rows * width * double)
     return run(
         functools.partial(down_kernel, chunk=chunk), sc,
         (mine, other, edge, taps, bias, weights), [shape, shape],
@@ -456,11 +479,20 @@
     normed, ups, rows = [None, None], [None, None], [None, None]
     for k in (1, 0):
         shape = ((4, n, width), bf16)
-        keep, send = run(
-            functools.partial(heads_kernel, chunk=k), sc,
-            (log, *incoming, within, scaled, gates, out_weight), [shape, shape],
-            scratch=[pltpu.VMEM((dk, dv), bf16), pltpu.VMEM((tok // 2, dv), f32)], flops=tok * dv * (dk + width),
-        )
+        sources = (log, *incoming, within, scaled, gates)
+        scratch = [pltpu.VMEM((dk, dv), bf16), pltpu.VMEM((tok // 2, dv), f32)]
+        gated = ((tok // 2, dv), bf16)
+        if k == 0:
+            ready = run(
+                functools.partial(gated_kernel, chunk=k), sc, sources, [gated],
+                scratch=scratch, flops=tok * dv * dk,
+            )[0]
+            keep, send = run(heads_project_kernel, sc, (ready, out_weight), [shape, shape], flops=tok * dv * width)
+        else:
+            keep, send = run(
+                functools.partial(heads_kernel, chunk=k), sc, (*sources, out_weight), [shape, shape],
+                scratch=scratch + [pltpu.VMEM(*gated)], flops=tok * dv * (dk + width),
+            )
         normed[k] = reduce_and_norm(sc, keep, send, bases, norm_gain, norm_bias, 0, k)
         rows[k] = gather_rows(normed[k])
     ups[1], weights, down_weights = first_up(sc, rows[1], weights, 2 * hidden)

time: 161 us -> 161 us (level)
  waiting for transfers between devices: 58 us -> 52.8 us
  starting transfers between devices: 47.9 us -> 51.8 us
    ppermute x27, waiting for transfers between devices: 57.5 us -> 52.7 us  [shift_by(): return lax.ppermute(x, axis, ring(by))]
    ppermute x27, starting transfers between devices: 42.8 us -> 47 us  [shift_by(): return lax.ppermute(x, axis, ring(by))]
    pallas_call x19 -> x21, Pallas kernels: 40.3 us -> 41.5 us  [run(): pl.pallas_call(kernel, in_specs=[pl.BlockSpec(memory_space=pltpu.SMEM)] +...]
  transfers between devices with their start and end apart: 41 -> 41, of which waited for: 20 -> 18; matrix products, arithmetic and copies ran while one was open for 0% -> 0% of each run, Pallas kernels for 19% -> 20%
where the time goes in v2:
time: 161 us; the launch traced here: 160 us
  waiting for transfers between devices  52.8 us (33%)
  starting transfers between devices  51.8 us (32%)
  Pallas kernels  41.5 us (26%)
  between operations  13.7 us (9%)
    ppermute x27, waiting for transfers between devices, shift_by(): return lax.ppermute(x, axis, ring(by))  52.7 us
    ppermute x27, starting transfers between devices, shift_by(): return lax.ppermute(x, axis, ring(by))  47 us
    pallas_call x21, Pallas kernels, run(): pl.pallas_call(kernel, in_specs=[pl.BlockSpec(memory_space=pltpu.SMEM)] +...  41.5 us
  transfers between devices with their start and end apart: 41, of which 18 were waited for; matrix products, arithmetic and copies ran while one was open for 0% of the time, Pallas kernels for 20%

profile of v2, /device:TPU:0, one launch (start us, length us, event | category | flops | bytes accessed | tf_op | source)
XLA Modules:
  0.0 160.2 jit_solution(684375721155443676)
XLA Ops:
  6.6 3.3 %shard_map.145 = (f32[1,1024]{1,0:T(1,128)S(1)}, bf16[1024,256]{1,0:T(8,128)(2,1)S(1)}, bf16[1024,256]{1,0:T(8,128)(2,1)S(1)}, bf16[1024,512]{1,0:T(8,128)(2,1)S...) custom-call(s32[4]{0:T(128)S(1)} %pad_add_fusion.sc, f32[1,1024]{1,0:T(1,128)} %bitcast.23, ...), custom_call_target="tpu_custom_call" | custom-call | flops 67108864 | tf_op jit(solution)/shard_map/pallas_call | solution.py:46
  9.9 2.3 %shard_map.146 = (bf16[1024,256]{1,0:T(8,128)(2,1)S(1)}, f32[1024,128]{1,0:T(8,128)S(1)}, f32[1024,128]{1,0:T(8,128)S(1)}, bf16[4,256,512]{2,1,0:T(8,128)(2,1)S(...) custom-call(s32[4]{0:T(128)S(1)} %pad_add_fusion.sc, ...), custom_call_target="tpu_custom_call" | custom-call | flops 536870912 | tf_op jit(solution)/shard_map/pallas_call | solution.py:46
  12.3 1.8 %collective-permute-start = (bf16[80,512]{1,0:T(8,128)(2,1)S(1)}, bf16[80,512]{1,0:T(8,128)(2,1)S(1)}, u32[]{:S(2)}, u32[]{:S(2)}) collective-permute-start(bf16[80,512]{1,0:T(8,128)(2,1)S(1)} %get-tuple-element.58), channel_id=1, source_target_pairs={{0,8},{8,16},{16,24},{24,0},{1,9},{9,17},{17,25},{25,1},{2,10},{10... | collective-permute-start | bytes 245768 | tf_op jit(solution)/shard_map/ppermute | solution.py:30
  14.1 2.9 %collective-permute-start.1 = (bf16[80,512]{1,0:T(8,128)(2,1)S(1)}, bf16[80,512]{1,0:T(8,128)(2,1)S(1)}, u32[]{:S(2)}, u32[]{:S(2)}) collective-permute-start(bf16[80,512]{1,0:T(8,128)(2,1)S(1)} %get-tuple-element.59), channel_id=1, source_target_pairs={{0,16},{8,24},{16,0},{24,8},{1,17},{9,25},{17,1},{25,9},{2,18},{10... | collective-permute-start | bytes 245768 | tf_op jit(solution)/shard_map/ppermute | solution.py:30
  17.0 1.3 collective-permute-start.2
  18.3 2.6 %collective-permute-done.1.r2 = bf16[80,512]{1,0:T(8,128)(2,1)S(1)} collective-permute-done((bf16[80,512]{1,0:T(8,128)(2,1)S(1)}, bf16[80,512]{1,0:T(8,128)(2,1)S(1)}, u32[]{:S(2)}, u32[]{:S(2)}) %collective-permute-start.1) | collective-permute-done | bytes 81952 | tf_op jit(solution)/shard_map/ppermute | solution.py:30
  21.4 0.7 shard_map.147
  22.1 4.1 %collective-permute-start.5 = (bf16[80,512]{1,0:T(8,128)(2,1)S(1)}, bf16[80,512]{1,0:T(8,128)(2,1)S(1)}, u32[]{:S(2)}, u32[]{:S(2)}) collective-permute-start(bf16[80,512]{1,0:T(8,128)(2,1)S(1)} %get-tuple-element.61), channel_id=1, source_target_pairs={{0,96},{32,0},{64,32},{96,64},{1,97},{33,1},{65,33},{97,65},{2,98}... | collective-permute-start | bytes 245768 | tf_op jit(solution)/shard_map/ppermute | solution.py:30
  26.2 1.3 collective-permute-start.3
  27.4 3.3 %collective-permute-done.5.t3 = bf16[80,512]{1,0:T(8,128)(2,1)S(1)} collective-permute-done((bf16[80,512]{1,0:T(8,128)(2,1)S(1)}, bf16[80,512]{1,0:T(8,128)(2,1)S(1)}, u32[]{:S(2)}, u32[]{:S(2)}) %collective-permute-start.5) | collective-permute-done | bytes 81952 | tf_op jit(solution)/shard_map/ppermute | solution.py:30
  30.8 3.3 %collective-permute-done.4.t2 = bf16[80,512]{1,0:T(8,128)(2,1)S(1)} collective-permute-done((bf16[80,512]{1,0:T(8,128)(2,1)S(1)}, bf16[80,512]{1,0:T(8,128)(2,1)S(1)}, u32[]{:S(2)}, u32[]{:S(2)}) %collective-permute-start.4) | collective-permute-done | bytes 81952 | tf_op jit(solution)/shard_map/ppermute | solution.py:30
  34.1 0.6 collective-permute-done.3.t1
  34.7 0.7 shard_map.148
  35.4 0.7 collective-permute-start.6
  36.1 3.3 %collective-permute-start.7 = (bf16[64,512]{1,0:T(8,128)(2,1)S(1)}, bf16[64,512]{1,0:T(8,128)(2,1)S(1)}, u32[]{:S(2)}, u32[]{:S(2)}) collective-permute-start(bf16[64,512]{1,0:T(8,128)(2,1)S(1)} %get-tuple-element.66), channel_id=1, source_target_pairs={{0,16},{8,24},{16,0},{24,8},{1,17},{9,25},{17,1},{25,9},{2,18},{10... | collective-permute-start | bytes 196616 | tf_op jit(solution)/shard_map/ppermute | solution.py:30
  39.4 0.6 collective-permute-start.8
  40.0 2.4 %shard_map.149 = (f32[2,512,512]{2,1,0:T(8,128)S(1)}, bf16[2,512,256]{2,1,0:T(8,128)(2,1)S(1)}) custom-call(s32[4]{0:T(128)S(1)} %pad_add_fusion.sc, f32[256,16]{1,0:T(8,128)S(1)} %get-tuple-element.68.down, f32[16,256]{1,0:T(8,128)S(1)} %get-tuple-element.69.across, bf16[1024,256]{1,0:T(8,128)(2,1)S(1)} %get-tuple-element.70.kr, ...), custom_call_target="tpu_custom_call" | custom-call | flops 805306368 | tf_op jit(solution)/shard_map/pallas_call | solution.py:46
  42.4 0.8 collective-permute-done.7.i2
  43.7 2.3 %shard_map.154 = (bf16[4,64,2048]{2,1,0:T(8,128)(2,1)S(1)}, bf16[4,64,2048]{2,1,0:T(8,128)(2,1)S(1)}) custom-call(s32[4]{0:T(128)S(1)} %pad_add_fusion.sc, f32[1,1024]{1,0:T(1,128)S(1)} %get-tuple-element.53.log, bf16[64,512]{1,0:T(8,128)(2,1)S(1)} %get-tuple-element.64.i0, bf16[64,512]{1,0:T(8,128)(2,1)S(1)} %collective-permute-done.6.i1, ...), custom_call_target="tpu_custom_call" | custom-call | flops 1207959552 | tf_op jit(solution)/shard_map/pallas_call | solution.py:46
  46.1 1.2 shard_map.150.gated
  47.4 1.8 %shard_map.151 = (bf16[4,64,2048]{2,1,0:T(8,128)(2,1)S(1)}, bf16[4,64,2048]{2,1,0:T(8,128)(2,1)S(1)}) custom-call(s32[4]{0:T(128)S(1)} %pad_add_fusion.sc, bf16[512,512]{1,0:T(8,128)(2,1)S(1)} %shard_map.150.gated, bf16[512,2048]{1,0:T(8,128)(2,1)S(1)} %copy-done.2), custom_call_target="tpu_custom_call" | custom-call | flops 1073741824 | tf_op jit(solution)/shard_map/pallas_call | solution.py:46
  49.3 0.6 collective-permute-start.9
  49.8 0.7 shard_map.155
  50.6 1.6 collective-permute-start.21
  52.1 2.7 %collective-permute-start.22 = (bf16[64,2048]{1,0:T(8,128)(2,1)S(1)}, bf16[64,2048]{1,0:T(8,128)(2,1)S(1)}, u32[]{:S(2)}, u32[]{:S(2)}) collective-permute-start(bf16[64,2048]{1,0:T(8,128)(2,1)S(1)} %get-tuple-element.85), channel_id=1, source_target_pairs={{0,4},{2,6},{4,0},{6,2},{1,5},{3,7},{5,1},{7,3},{8,12},{10,14},{12... | collective-permute-start | bytes 786440 | tf_op jit(solution)/shard_map/ppermute | solution.py:30
  54.8 1.4 collective-permute-start.23
  56.3 0.7 shard_map.152
  57.0 0.6 collective-permute-start.10
  57.7 0.9 collective-permute-start.11
  58.6 1.5 collective-permute-done.21.r1
  60.1 2.5 %collective-permute-start.12 = (bf16[64,2048]{1,0:T(8,128)(2,1)S(1)}, bf16[64,2048]{1,0:T(8,128)(2,1)S(1)}, u32[]{:S(2)}, u32[]{:S(2)}) collective-permute-start(bf16[64,2048]{1,0:T(8,128)(2,1)S(1)} %get-tuple-element.81), channel_id=1, source_target_pairs={{0,6},{2,0},{4,2},{6,4},{1,7},{3,1},{5,3},{7,5},{8,14},{10,8},{12,... | collective-permute-start | bytes 786440 | tf_op jit(solution)/shard_map/ppermute | solution.py:30
  62.6 5.1 %collective-permute-done.22.r2 = bf16[64,2048]{1,0:T(8,128)(2,1)S(1)} collective-permute-done((bf16[64,2048]{1,0:T(8,128)(2,1)S(1)}, bf16[64,2048]{1,0:T(8,128)(2,1)S(1)}, u32[]{:S(2)}, u32[]{:S(2)}) %collective-permute-start.22) | collective-permute-done | bytes 262176 | tf_op jit(solution)/shard_map/ppermute | solution.py:30
  67.7 1.0 shard_map.156.refs_0_
  68.7 2.9 %collective-permute-start.26 = (bf16[64,2048]{1,0:T(8,128)(2,1)S(1)}, bf16[64,2048]{1,0:T(8,128)(2,1)S(1)}, u32[]{:S(2)}, u32[]{:S(2)}) collective-permute-start(bf16[64,2048]{1,0:T(8,128)(2,1)S(1)} %shard_map.156.refs_0_), channel_id=1, source_target_pairs={{0,6},{2,0},{4,2},{6,4},{1,7},{3,1},{5,3},{7,5},{8,14},{10,8},{12,... | collective-permute-start | bytes 786440 | tf_op jit(solution)/shard_map/ppermute | solution.py:30
  71.6 2.4 %collective-permute-start.25 = (bf16[64,2048]{1,0:T(8,128)(2,1)S(1)}, bf16[64,2048]{1,0:T(8,128)(2,1)S(1)}, u32[]{:S(2)}, u32[]{:S(2)}) collective-permute-start(bf16[64,2048]{1,0:T(8,128)(2,1)S(1)} %shard_map.156.refs_0_), channel_id=1, source_target_pairs={{0,4},{2,6},{4,0},{6,2},{1,5},{3,7},{5,1},{7,3},{8,12},{10,14},{12... | collective-permute-start | bytes 786440 | tf_op jit(solution)/shard_map/ppermute | solution.py:30
  74.0 4.8 %collective-permute-done.11.r2 = bf16[64,2048]{1,0:T(8,128)(2,1)S(1)} collective-permute-done((bf16[64,2048]{1,0:T(8,128)(2,1)S(1)}, bf16[64,2048]{1,0:T(8,128)(2,1)S(1)}, u32[]{:S(2)}, u32[]{:S(2)}) %collective-permute-start.11) | collective-permute-done | bytes 262176 | tf_op jit(solution)/shard_map/ppermute | solution.py:30
  78.9 0.9 shard_map.153.refs_0_
  79.9 3.3 %collective-permute-start.15 = (bf16[64,2048]{1,0:T(8,128)(2,1)S(1)}, bf16[64,2048]{1,0:T(8,128)(2,1)S(1)}, u32[]{:S(2)}, u32[]{:S(2)}) collective-permute-start(bf16[64,2048]{1,0:T(8,128)(2,1)S(1)} %shard_map.153.refs_0_), channel_id=1, source_target_pairs={{0,6},{2,0},{4,2},{6,4},{1,7},{3,1},{5,3},{7,5},{8,14},{10,8},{12,... | collective-permute-start | bytes 786440 | tf_op jit(solution)/shard_map/ppermute | solution.py:30
  83.3 1.1 collective-permute-done.26.refs_3_
  84.4 2.4 %collective-permute-start.13 = (bf16[64,2048]{1,0:T(8,128)(2,1)S(1)}, bf16[64,2048]{1,0:T(8,128)(2,1)S(1)}, u32[]{:S(2)}, u32[]{:S(2)}) collective-permute-start(bf16[64,2048]{1,0:T(8,128)(2,1)S(1)} %shard_map.153.refs_0_), channel_id=1, source_target_pairs={{0,2},{2,4},{4,6},{6,0},{1,3},{3,5},{5,7},{7,1},{8,10},{10,12},{12... | collective-permute-start | bytes 786440 | tf_op jit(solution)/shard_map/ppermute | solution.py:30
  86.8 8.0 %collective-permute-done.24.refs_1_ = bf16[64,2048]{1,0:T(8,128)(2,1)S(1)} collective-permute-done((bf16[64,2048]{1,0:T(8,128)(2,1)S(1)}, bf16[64,2048]{1,0:T(8,128)(2,1)S(1)}, u32[]{:S(2)}, u32[]{:S(2)}) %collective-permute-start.24) | collective-permute-done | bytes 262176 | tf_op jit(solution)/shard_map/ppermute | solution.py:30
  94.8 0.9 collective-permute-done.15.refs_3_
  96.4 4.0 %collective-permute-done.13.refs_1_ = bf16[64,2048]{1,0:T(8,128)(2,1)S(1)} collective-permute-done((bf16[64,2048]{1,0:T(8,128)(2,1)S(1)}, bf16[64,2048]{1,0:T(8,128)(2,1)S(1)}, u32[]{:S(2)}, u32[]{:S(2)}) %collective-permute-start.13) | collective-permute-done | bytes 262176 | tf_op jit(solution)/shard_map/ppermute | solution.py:30
  101.0 5.7 %shard_map.157 = (bf16[512,1408]{1,0:T(8,128)(2,1)S(1)}, bf16[2048,1408]{1,0:T(8,128)(2,1)S(1)}, bf16[2048,768]{1,0:T(8,128)(2,1)S(1)}) custom-call(s32[4]{0:T(128)S(1)} %pad_add_fusion.sc, bf16[64,2048]{1,0:T(8,128)(2,1)S(1)} %shard_map.156.refs_0_, bf16[64,2048]{1,0:T(8,128)(2,1)S(1)} %collective-permute-done.24.refs_1_, ...), custom_call_target="tpu_custom_call" | custom-call | flops 2952790016 | tf_op jit(solution)/shard_map/pallas_call | solution.py:46
  106.7 2.1 %collective-permute-start.31 = (bf16[16,1408]{1,0:T(8,128)(2,1)S(1)}, bf16[16,1408]{1,0:T(8,128)(2,1)S(1)}, u32[]{:S(2)}, u32[]{:S(2)}) collective-permute-start(bf16[16,1408]{1,0:T(8,128)(2,1)S(1)} %slice.15), channel_id=1, source_target_pairs={{0,8},{8,16},{16,24},{24,32},{32,40},{40,48},{48,56},{56,64},{64,7... | collective-permute-start | bytes 135176 | tf_op jit(solution)/shard_map/ppermute | solution.py:500
  108.9 4.6 %shard_map.158.mine.other = bf16[512,1408]{1,0:T(8,128)(2,1)S(1)} custom-call(s32[4]{0:T(128)S(1)} %pad_add_fusion.sc, bf16[64,2048]{1,0:T(8,128)(2,1)S(1)} %shard_map.153.refs_0_, bf16[64,2048]{1,0:T(8,128)(2,1)S(1)} %collective-permute-done.13.refs_1_, bf16[64,2048]{1,0:T(8,128)(2,1)S(1)} %collective-permute-done.14.refs_2_, ...), custom_call_target="tpu_custom_call" | custom-call | flops 2952790016 | tf_op jit(solution)/shard_map/pallas_call | solution.py:46
  113.5 4.2 %shard_map.162 = (bf16[4,64,2048]{2,1,0:T(8,128)(2,1)S(1)}, bf16[4,64,2048]{2,1,0:T(8,128)(2,1)S(1)}) custom-call(s32[4]{0:T(128)S(1)} %pad_add_fusion.sc, bf16[512,1408]{1,0:T(8,128)(2,1)S(1)} %get-tuple-element.89.other.mine, bf16[512,1408]{1,0:T(8,128)(2,1)S(1)} %shard_map.158.mine.other, bf16[16,1408]{1,0:T(8,128)(2,1)S(1)} %collective-permute-done.31.edge, ...), custom_call_target="tpu_custom_call" | custom-call | flops 2952790016 | tf_op jit(solution)/shard_map/pallas_call | solution.py:46
  118.0 2.4 %shard_map.159.active = bf16[512,704]{1,0:T(8,128)(2,1)S(1)} custom-call(s32[4]{0:T(128)S(1)} %pad_add_fusion.sc, bf16[512,1408]{1,0:T(8,128)(2,1)S(1)} %shard_map.158.mine.other, bf16[512,1408]{1,0:T(8,128)(2,1)S(1)} %get-tuple-element.89.other.mine, bf16[16,1408]{1,0:T(8,128)(2,1)S(1)} %collective-permute-done.31.edge, ...), custom_call_target="tpu_custom_call" | custom-call | flops 1476395008 | tf_op jit(solution)/shard_map/pallas_call | solution.py:46
  120.4 2.4 %shard_map.160 = (bf16[4,64,2048]{2,1,0:T(8,128)(2,1)S(1)}, bf16[4,64,2048]{2,1,0:T(8,128)(2,1)S(1)}) custom-call(s32[4]{0:T(128)S(1)} %pad_add_fusion.sc, bf16[512,704]{1,0:T(8,128)(2,1)S(1)} %shard_map.159.active, bf16[2048,768]{1,0:T(8,128)(2,1)S(1)} %get-tuple-element.90.weight), custom_call_target="tpu_custom_call" | custom-call | flops 1476395008 | tf_op jit(solution)/shard_map/pallas_call | solution.py:46
  122.8 0.7 collective-permute-start.32
  123.5 0.7 shard_map.163
  124.2 2.6 %collective-permute-start.37 = (bf16[64,2048]{1,0:T(8,128)(2,1)S(1)}, bf16[64,2048]{1,0:T(8,128)(2,1)S(1)}, u32[]{:S(2)}, u32[]{:S(2)}) collective-permute-start(bf16[64,2048]{1,0:T(8,128)(2,1)S(1)} %get-tuple-element.98), channel_id=1, source_target_pairs={{0,2},{2,4},{4,6},{6,0},{1,3},{3,5},{5,7},{7,1},{8,10},{10,12},{12... | collective-permute-start | bytes 786440 | tf_op jit(solution)/shard_map/ppermute | solution.py:30
  126.8 1.7 %collective-permute-start.38 = (bf16[64,2048]{1,0:T(8,128)(2,1)S(1)}, bf16[64,2048]{1,0:T(8,128)(2,1)S(1)}, u32[]{:S(2)}, u32[]{:S(2)}) collective-permute-start(bf16[64,2048]{1,0:T(8,128)(2,1)S(1)} %get-tuple-element.99), channel_id=1, source_target_pairs={{0,4},{2,6},{4,0},{6,2},{1,5},{3,7},{5,1},{7,3},{8,12},{10,14},{12... | collective-permute-start | bytes 786440 | tf_op jit(solution)/shard_map/ppermute | solution.py:30
  128.5 1.1 collective-permute-start.39
  129.6 0.7 shard_map.161
  130.3 1.0 collective-permute-start.33
  131.4 1.8 %collective-permute-start.34 = (bf16[64,2048]{1,0:T(8,128)(2,1)S(1)}, bf16[64,2048]{1,0:T(8,128)(2,1)S(1)}, u32[]{:S(2)}, u32[]{:S(2)}) collective-permute-start(bf16[64,2048]{1,0:T(8,128)(2,1)S(1)} %get-tuple-element.94), channel_id=1, source_target_pairs={{0,4},{2,6},{4,0},{6,2},{1,5},{3,7},{5,1},{7,3},{8,12},{10,14},{12... | collective-permute-start | bytes 786440 | tf_op jit(solution)/shard_map/ppermute | solution.py:30
  133.2 1.1 collective-permute-done.37.r1
  134.3 1.9 %collective-permute-start.35 = (bf16[64,2048]{1,0:T(8,128)(2,1)S(1)}, bf16[64,2048]{1,0:T(8,128)(2,1)S(1)}, u32[]{:S(2)}, u32[]{:S(2)}) collective-permute-start(bf16[64,2048]{1,0:T(8,128)(2,1)S(1)} %get-tuple-element.95), channel_id=1, source_target_pairs={{0,6},{2,0},{4,2},{6,4},{1,7},{3,1},{5,3},{7,5},{8,14},{10,8},{12,... | collective-permute-start | bytes 786440 | tf_op jit(solution)/shard_map/ppermute | solution.py:30
  136.2 5.1 %collective-permute-done.38.r2 = bf16[64,2048]{1,0:T(8,128)(2,1)S(1)} collective-permute-done((bf16[64,2048]{1,0:T(8,128)(2,1)S(1)}, bf16[64,2048]{1,0:T(8,128)(2,1)S(1)}, u32[]{:S(2)}, u32[]{:S(2)}) %collective-permute-start.38) | collective-permute-done | bytes 262176 | tf_op jit(solution)/shard_map/ppermute | solution.py:30
  141.3 1.0 shard_map.164.rest_0_
  142.3 2.8 %collective-permute-done.33.r1 = bf16[64,2048]{1,0:T(8,128)(2,1)S(1)} collective-permute-done((bf16[64,2048]{1,0:T(8,128)(2,1)S(1)}, bf16[64,2048]{1,0:T(8,128)(2,1)S(1)}, u32[]{:S(2)}, u32[]{:S(2)}) %collective-permute-start.33) | collective-permute-done | bytes 262176 | tf_op jit(solution)/shard_map/ppermute | solution.py:30
  145.1 6.5 %collective-permute-done.34.r2 = bf16[64,2048]{1,0:T(8,128)(2,1)S(1)} collective-permute-done((bf16[64,2048]{1,0:T(8,128)(2,1)S(1)}, bf16[64,2048]{1,0:T(8,128)(2,1)S(1)}, u32[]{:S(2)}, u32[]{:S(2)}) %collective-permute-start.34) | collective-permute-done | bytes 262176 | tf_op jit(solution)/shard_map/ppermute | solution.py:30
  151.6 1.7 %shard_map.165 = bf16[128,2048]{1,0:T(8,128)(2,1)} custom-call(s32[4]{0:T(128)S(1)} %pad_add_fusion.sc, bf16[4,64,2048]{2,1,0:T(8,128)(2,1)S(1)} %get-tuple-element.91.keep, bf16[4,64,2048]{2,1,0:T(8,128)(2,1)S(1)} %collective-permute-done.32.got, bf16[64,2048]{1,0:T(8,128)(2,1)S(1)} %collective-permute-done.33.r1, ...), custom_call_target="tpu_custom_call" | custom-call | flops 52428800 | tf_op jit(solution)/shard_map/pallas_call | solution.py:46
  (61 shorter events, 3.0 us)
Async XLA Ops:
  6.5 94.5 %all-gather.2.cloned.1.call-start = ((), (), s32[]{:S(2)}) async-start(), calls=%async_computation | async-start | bytes 9469952 | tf_op jit(solution)/shard_map/all_gather | solution.py:454
  12.3 31.4 %copy-start.1 = (bf16[1024,512]{1,0:T(8,128)(2,1)S(1)}, bf16[1024,512]{1,0:T(8,128)(2,1)}, u32[]{:S(2)}) copy-start(bf16[1024,512]{1,0:T(8,128)(2,1)} %param.18) | copy-start | bytes 3145732
  12.3 31.4 %copy-start.2 = (bf16[512,2048]{1,0:T(8,128)(2,1)S(1)}, bf16[512,2048]{1,0:T(8,128)(2,1)}, u32[]{:S(2)}) copy-start(bf16[512,2048]{1,0:T(8,128)(2,1)} %weight.3) | copy-start | bytes 6291460
  12.3 6.0 %collective-permute-start = (bf16[80,512]{1,0:T(8,128)(2,1)S(1)}, bf16[80,512]{1,0:T(8,128)(2,1)S(1)}, u32[]{:S(2)}, u32[]{:S(2)}) collective-permute-start(bf16[80,512]{1,0:T(8,128)(2,1)S(1)} %get-tuple-element.58), channel_id=1, source_target_pairs={{0,8},{8,16},{16,24},{24,0},{1,9},{9,17},{17,25},{25,1},{2,10},{10... | collective-permute-start | bytes 245768 | tf_op jit(solution)/shard_map/ppermute | solution.py:30
  14.1 6.8 %collective-permute-start.1 = (bf16[80,512]{1,0:T(8,128)(2,1)S(1)}, bf16[80,512]{1,0:T(8,128)(2,1)S(1)}, u32[]{:S(2)}, u32[]{:S(2)}) collective-permute-start(bf16[80,512]{1,0:T(8,128)(2,1)S(1)} %get-tuple-element.59), channel_id=1, source_target_pairs={{0,16},{8,24},{16,0},{24,8},{1,17},{9,25},{17,1},{25,9},{2,18},{10... | collective-permute-start | bytes 245768 | tf_op jit(solution)/shard_map/ppermute | solution.py:30
  17.0 4.4 %collective-permute-start.2 = (bf16[80,512]{1,0:T(8,128)(2,1)S(1)}, bf16[80,512]{1,0:T(8,128)(2,1)S(1)}, u32[]{:S(2)}, u32[]{:S(2)}) collective-permute-start(bf16[80,512]{1,0:T(8,128)(2,1)S(1)} %get-tuple-element.60), channel_id=1, source_target_pairs={{0,24},{8,0},{16,8},{24,16},{1,25},{9,1},{17,9},{25,17},{2,26},{10... | collective-permute-start | bytes 245768 | tf_op jit(solution)/shard_map/ppermute | solution.py:30
  22.1 8.7 %collective-permute-start.5 = (bf16[80,512]{1,0:T(8,128)(2,1)S(1)}, bf16[80,512]{1,0:T(8,128)(2,1)S(1)}, u32[]{:S(2)}, u32[]{:S(2)}) collective-permute-start(bf16[80,512]{1,0:T(8,128)(2,1)S(1)} %get-tuple-element.61), channel_id=1, source_target_pairs={{0,96},{32,0},{64,32},{96,64},{1,97},{33,1},{65,33},{97,65},{2,98}... | collective-permute-start | bytes 245768 | tf_op jit(solution)/shard_map/ppermute | solution.py:30
  26.2 7.9 %collective-permute-start.4 = (bf16[80,512]{1,0:T(8,128)(2,1)S(1)}, bf16[80,512]{1,0:T(8,128)(2,1)S(1)}, u32[]{:S(2)}, u32[]{:S(2)}) collective-permute-start(bf16[80,512]{1,0:T(8,128)(2,1)S(1)} %get-tuple-element.61), channel_id=1, source_target_pairs={{0,64},{32,96},{64,0},{96,32},{1,65},{33,97},{65,1},{97,33},{2,66}... | collective-permute-start | bytes 245768 | tf_op jit(solution)/shard_map/ppermute | solution.py:30
  26.2 8.6 %collective-permute-start.3 = (bf16[80,512]{1,0:T(8,128)(2,1)S(1)}, bf16[80,512]{1,0:T(8,128)(2,1)S(1)}, u32[]{:S(2)}, u32[]{:S(2)}) collective-permute-start(bf16[80,512]{1,0:T(8,128)(2,1)S(1)} %get-tuple-element.61), channel_id=1, source_target_pairs={{0,32},{32,64},{64,96},{96,0},{1,33},{33,65},{65,97},{97,1},{2,34}... | collective-permute-start | bytes 245768 | tf_op jit(solution)/shard_map/ppermute | solution.py:30
  35.4 7.0 %collective-permute-start.6 = (bf16[64,512]{1,0:T(8,128)(2,1)S(1)}, bf16[64,512]{1,0:T(8,128)(2,1)S(1)}, u32[]{:S(2)}, u32[]{:S(2)}) collective-permute-start(bf16[64,512]{1,0:T(8,128)(2,1)S(1)} %get-tuple-element.65), channel_id=1, source_target_pairs={{0,8},{8,16},{16,24},{24,0},{1,9},{9,17},{17,25},{25,1},{2,10},{10... | collective-permute-start | bytes 196616 | tf_op jit(solution)/shard_map/ppermute | solution.py:30
  36.1 7.0 %collective-permute-start.7 = (bf16[64,512]{1,0:T(8,128)(2,1)S(1)}, bf16[64,512]{1,0:T(8,128)(2,1)S(1)}, u32[]{:S(2)}, u32[]{:S(2)}) collective-permute-start(bf16[64,512]{1,0:T(8,128)(2,1)S(1)} %get-tuple-element.66), channel_id=1, source_target_pairs={{0,16},{8,24},{16,0},{24,8},{1,17},{9,25},{17,1},{25,9},{2,18},{10... | collective-permute-start | bytes 196616 | tf_op jit(solution)/shard_map/ppermute | solution.py:30
  39.4 4.3 %collective-permute-start.8 = (bf16[64,512]{1,0:T(8,128)(2,1)S(1)}, bf16[64,512]{1,0:T(8,128)(2,1)S(1)}, u32[]{:S(2)}, u32[]{:S(2)}) collective-permute-start(bf16[64,512]{1,0:T(8,128)(2,1)S(1)} %get-tuple-element.67), channel_id=1, source_target_pairs={{0,24},{8,0},{16,8},{24,16},{1,25},{9,1},{17,9},{25,17},{2,26},{10... | collective-permute-start | bytes 196616 | tf_op jit(solution)/shard_map/ppermute | solution.py:30
  46.0 3.8 %collective-permute-start.20 = (bf16[4,64,2048]{2,1,0:T(8,128)(2,1)S(1)}, bf16[4,64,2048]{2,1,0:T(8,128)(2,1)S(1)}, u32[]{:S(2)}, u32[]{:S(2)}) collective-permute-start(bf16[4,64,2048]{2,1,0:T(8,128)(2,1)S(1)} %get-tuple-element.83), channel_id=1, source_target_pairs={{0,1},{1,0},{2,3},{3,2},{4,5},{5,4},{6,7},{7,6},{8,9},{9,8},{10,11... | collective-permute-start | bytes 3145736 | tf_op jit(solution)/shard_map/ppermute | solution.py:38
  47.4 15.2 %copy-start.5 = (f32[2,3,704]{2,0,1:T(2,128)S(1)}, f32[2,3,704]{2,0,1:T(2,128)}, u32[]{:S(2)}) copy-start(f32[2,3,704]{2,0,1:T(2,128)} %param.26) | copy-start | bytes 50692
  47.4 20.3 %copy-start = (bf16[1024,2048]{1,0:T(8,128)(2,1)S(1)}, bf16[1024,2048]{1,0:T(8,128)(2,1)}, u32[]{:S(2)}) copy-start(bf16[1024,2048]{1,0:T(8,128)(2,1)} %param.20) | copy-start | bytes 12582916
  47.4 20.3 %copy-start.3 = (f32[2,2048]{1,0:T(2,128)S(1)}, f32[2,2048]{1,0:T(2,128)}, u32[]{:S(2)}) copy-start(f32[2,2048]{1,0:T(2,128)} %gain.7) | copy-start | bytes 49156
  47.4 20.3 %copy-start.4 = (f32[2,2048]{1,0:T(2,128)S(1)}, f32[2,2048]{1,0:T(2,128)}, u32[]{:S(2)}) copy-start(f32[2,2048]{1,0:T(2,128)} %shift.7) | copy-start | bytes 49156
  49.3 7.0 %collective-permute-start.9 = (bf16[4,64,2048]{2,1,0:T(8,128)(2,1)S(1)}, bf16[4,64,2048]{2,1,0:T(8,128)(2,1)S(1)}, u32[]{:S(2)}, u32[]{:S(2)}) collective-permute-start(bf16[4,64,2048]{2,1,0:T(8,128)(2,1)S(1)} %get-tuple-element.78), channel_id=1, source_target_pairs={{0,1},{1,0},{2,3},{3,2},{4,5},{5,4},{6,7},{7,6},{8,9},{9,8},{10,11... | collective-permute-start | bytes 3145736 | tf_op jit(solution)/shard_map/ppermute | solution.py:38
  50.6 9.5 %collective-permute-start.21 = (bf16[64,2048]{1,0:T(8,128)(2,1)S(1)}, bf16[64,2048]{1,0:T(8,128)(2,1)S(1)}, u32[]{:S(2)}, u32[]{:S(2)}) collective-permute-start(bf16[64,2048]{1,0:T(8,128)(2,1)S(1)} %get-tuple-element.84), channel_id=1, source_target_pairs={{0,2},{2,4},{4,6},{6,0},{1,3},{3,5},{5,7},{7,1},{8,10},{10,12},{12... | collective-permute-start | bytes 786440 | tf_op jit(solution)/shard_map/ppermute | solution.py:30
  52.1 15.5 %collective-permute-start.22 = (bf16[64,2048]{1,0:T(8,128)(2,1)S(1)}, bf16[64,2048]{1,0:T(8,128)(2,1)S(1)}, u32[]{:S(2)}, u32[]{:S(2)}) collective-permute-start(bf16[64,2048]{1,0:T(8,128)(2,1)S(1)} %get-tuple-element.85), channel_id=1, source_target_pairs={{0,4},{2,6},{4,0},{6,2},{1,5},{3,7},{5,1},{7,3},{8,12},{10,14},{12... | collective-permute-start | bytes 786440 | tf_op jit(solution)/shard_map/ppermute | solution.py:30
  54.8 12.8 %collective-permute-start.23 = (bf16[64,2048]{1,0:T(8,128)(2,1)S(1)}, bf16[64,2048]{1,0:T(8,128)(2,1)S(1)}, u32[]{:S(2)}, u32[]{:S(2)}) collective-permute-start(bf16[64,2048]{1,0:T(8,128)(2,1)S(1)} %get-tuple-element.86), channel_id=1, source_target_pairs={{0,6},{2,0},{4,2},{6,4},{1,7},{3,1},{5,3},{7,5},{8,14},{10,8},{12,... | collective-permute-start | bytes 786440 | tf_op jit(solution)/shard_map/ppermute | solution.py:30
  57.0 14.6 %collective-permute-start.10 = (bf16[64,2048]{1,0:T(8,128)(2,1)S(1)}, bf16[64,2048]{1,0:T(8,128)(2,1)S(1)}, u32[]{:S(2)}, u32[]{:S(2)}) collective-permute-start(bf16[64,2048]{1,0:T(8,128)(2,1)S(1)} %get-tuple-element.79), channel_id=1, source_target_pairs={{0,2},{2,4},{4,6},{6,0},{1,3},{3,5},{5,7},{7,1},{8,10},{10,12},{12... | collective-permute-start | bytes 786440 | tf_op jit(solution)/shard_map/ppermute | solution.py:30
  57.7 21.2 %collective-permute-start.11 = (bf16[64,2048]{1,0:T(8,128)(2,1)S(1)}, bf16[64,2048]{1,0:T(8,128)(2,1)S(1)}, u32[]{:S(2)}, u32[]{:S(2)}) collective-permute-start(bf16[64,2048]{1,0:T(8,128)(2,1)S(1)} %get-tuple-element.80), channel_id=1, source_target_pairs={{0,4},{2,6},{4,0},{6,2},{1,5},{3,7},{5,1},{7,3},{8,12},{10,14},{12... | collective-permute-start | bytes 786440 | tf_op jit(solution)/shard_map/ppermute | solution.py:30
  60.1 18.8 %collective-permute-start.12 = (bf16[64,2048]{1,0:T(8,128)(2,1)S(1)}, bf16[64,2048]{1,0:T(8,128)(2,1)S(1)}, u32[]{:S(2)}, u32[]{:S(2)}) collective-permute-start(bf16[64,2048]{1,0:T(8,128)(2,1)S(1)} %get-tuple-element.81), channel_id=1, source_target_pairs={{0,6},{2,0},{4,2},{6,4},{1,7},{3,1},{5,3},{7,5},{8,14},{10,8},{12,... | collective-permute-start | bytes 786440 | tf_op jit(solution)/shard_map/ppermute | solution.py:30
  68.6 14.5 %copy-start.6 = (f32[2,704]{1,0:T(2,128)S(1)}, f32[2,704]{1,0:T(2,128)}, u32[]{:S(2)}) copy-start(f32[2,704]{1,0:T(2,128)} %param.27) | copy-start | bytes 16900
  68.6 14.5 %collective-permute-start.27 = (bf16[64,2048]{1,0:T(8,128)(2,1)S(1)}, bf16[64,2048]{1,0:T(8,128)(2,1)S(1)}, u32[]{:S(2)}, u32[]{:S(2)}) collective-permute-start(bf16[64,2048]{1,0:T(8,128)(2,1)S(1)} %shard_map.156.refs_0_), channel_id=1, source_target_pairs={{0,1},{1,0},{2,3},{3,2},{4,5},{5,4},{6,7},{7,6},{8,9},{9,8},{10,11... | collective-permute-start | bytes 786440 | tf_op jit(solution)/shard_map/ppermute | solution.py:38
  68.7 15.7 %collective-permute-start.26 = (bf16[64,2048]{1,0:T(8,128)(2,1)S(1)}, bf16[64,2048]{1,0:T(8,128)(2,1)S(1)}, u32[]{:S(2)}, u32[]{:S(2)}) collective-permute-start(bf16[64,2048]{1,0:T(8,128)(2,1)S(1)} %shard_map.156.refs_0_), channel_id=1, source_target_pairs={{0,6},{2,0},{4,2},{6,4},{1,7},{3,1},{5,3},{7,5},{8,14},{10,8},{12,... | collective-permute-start | bytes 786440 | tf_op jit(solution)/shard_map/ppermute | solution.py:30
  71.6 15.2 %collective-permute-start.25 = (bf16[64,2048]{1,0:T(8,128)(2,1)S(1)}, bf16[64,2048]{1,0:T(8,128)(2,1)S(1)}, u32[]{:S(2)}, u32[]{:S(2)}) collective-permute-start(bf16[64,2048]{1,0:T(8,128)(2,1)S(1)} %shard_map.156.refs_0_), channel_id=1, source_target_pairs={{0,4},{2,6},{4,0},{6,2},{1,5},{3,7},{5,1},{7,3},{8,12},{10,14},{12... | collective-permute-start | bytes 786440 | tf_op jit(solution)/shard_map/ppermute | solution.py:30
  78.9 16.0 %collective-permute-start.24 = (bf16[64,2048]{1,0:T(8,128)(2,1)S(1)}, bf16[64,2048]{1,0:T(8,128)(2,1)S(1)}, u32[]{:S(2)}, u32[]{:S(2)}) collective-permute-start(bf16[64,2048]{1,0:T(8,128)(2,1)S(1)} %shard_map.156.refs_0_), channel_id=1, source_target_pairs={{0,2},{2,4},{4,6},{6,0},{1,3},{3,5},{5,7},{7,1},{8,10},{10,12},{12... | collective-permute-start | bytes 786440 | tf_op jit(solution)/shard_map/ppermute | solution.py:30
  79.9 15.9 %collective-permute-start.15 = (bf16[64,2048]{1,0:T(8,128)(2,1)S(1)}, bf16[64,2048]{1,0:T(8,128)(2,1)S(1)}, u32[]{:S(2)}, u32[]{:S(2)}) collective-permute-start(bf16[64,2048]{1,0:T(8,128)(2,1)S(1)} %shard_map.153.refs_0_), channel_id=1, source_target_pairs={{0,6},{2,0},{4,2},{6,4},{1,7},{3,1},{5,3},{7,5},{8,14},{10,8},{12,... | collective-permute-start | bytes 786440 | tf_op jit(solution)/shard_map/ppermute | solution.py:30
  83.2 12.7 %collective-permute-start.14 = (bf16[64,2048]{1,0:T(8,128)(2,1)S(1)}, bf16[64,2048]{1,0:T(8,128)(2,1)S(1)}, u32[]{:S(2)}, u32[]{:S(2)}) collective-permute-start(bf16[64,2048]{1,0:T(8,128)(2,1)S(1)} %shard_map.153.refs_0_), channel_id=1, source_target_pairs={{0,4},{2,6},{4,0},{6,2},{1,5},{3,7},{5,1},{7,3},{8,12},{10,14},{12... | collective-permute-start | bytes 786440 | tf_op jit(solution)/shard_map/ppermute | solution.py:30
  84.4 16.0 %collective-permute-start.13 = (bf16[64,2048]{1,0:T(8,128)(2,1)S(1)}, bf16[64,2048]{1,0:T(8,128)(2,1)S(1)}, u32[]{:S(2)}, u32[]{:S(2)}) collective-permute-start(bf16[64,2048]{1,0:T(8,128)(2,1)S(1)} %shard_map.153.refs_0_), channel_id=1, source_target_pairs={{0,2},{2,4},{4,6},{6,0},{1,3},{3,5},{5,7},{7,1},{8,10},{10,12},{12... | collective-permute-start | bytes 786440 | tf_op jit(solution)/shard_map/ppermute | solution.py:30
  86.8 13.6 %collective-permute-start.30 = (bf16[64,2048]{1,0:T(8,128)(2,1)S(1)}, bf16[64,2048]{1,0:T(8,128)(2,1)S(1)}, u32[]{:S(2)}, u32[]{:S(2)}) collective-permute-start(bf16[64,2048]{1,0:T(8,128)(2,1)S(1)} %collective-permute-done.26.refs_3_), channel_id=1, source_target_pairs={{0,1},{1,0},{2,3},{3,2},{4,5},{5,4},{6,7},{7,6},{8,9},{9,8},{10,11... | collective-permute-start | bytes 786440 | tf_op jit(solution)/shard_map/ppermute | solution.py:38
  94.8 6.1 %collective-permute-start.29 = (bf16[64,2048]{1,0:T(8,128)(2,1)S(1)}, bf16[64,2048]{1,0:T(8,128)(2,1)S(1)}, u32[]{:S(2)}, u32[]{:S(2)}) collective-permute-start(bf16[64,2048]{1,0:T(8,128)(2,1)S(1)} %collective-permute-done.25.refs_2_), channel_id=1, source_target_pairs={{0,1},{1,0},{2,3},{3,2},{4,5},{5,4},{6,7},{7,6},{8,9},{9,8},{10,11... | collective-permute-start | bytes 786440 | tf_op jit(solution)/shard_map/ppermute | solution.py:38
  95.7 5.3 %collective-permute-start.28 = (bf16[64,2048]{1,0:T(8,128)(2,1)S(1)}, bf16[64,2048]{1,0:T(8,128)(2,1)S(1)}, u32[]{:S(2)}, u32[]{:S(2)}) collective-permute-start(bf16[64,2048]{1,0:T(8,128)(2,1)S(1)} %collective-permute-done.24.refs_1_), channel_id=1, source_target_pairs={{0,1},{1,0},{2,3},{3,2},{4,5},{5,4},{6,7},{7,6},{8,9},{9,8},{10,11... | collective-permute-start | bytes 786440 | tf_op jit(solution)/shard_map/ppermute | solution.py:38
  95.9 13.0 %collective-permute-start.16 = (bf16[64,2048]{1,0:T(8,128)(2,1)S(1)}, bf16[64,2048]{1,0:T(8,128)(2,1)S(1)}, u32[]{:S(2)}, u32[]{:S(2)}) collective-permute-start(bf16[64,2048]{1,0:T(8,128)(2,1)S(1)} %shard_map.153.refs_0_), channel_id=1, source_target_pairs={{0,1},{1,0},{2,3},{3,2},{4,5},{5,4},{6,7},{7,6},{8,9},{9,8},{10,11... | collective-permute-start | bytes 786440 | tf_op jit(solution)/shard_map/ppermute | solution.py:38
  100.4 8.4 %collective-permute-start.19 = (bf16[64,2048]{1,0:T(8,128)(2,1)S(1)}, bf16[64,2048]{1,0:T(8,128)(2,1)}, u32[]{:S(2)}, u32[]{:S(2)}) collective-permute-start(bf16[64,2048]{1,0:T(8,128)(2,1)S(1)} %collective-permute-done.15.refs_3_), channel_id=1, source_target_pairs={{0,1},{1,0},{2,3},{3,2},{4,5},{5,4},{6,7},{7,6},{8,9},{9,8},{10,11... | collective-permute-start | bytes 786440 | tf_op jit(solution)/shard_map/ppermute | solution.py:38
  100.4 8.4 %collective-permute-start.18 = (bf16[64,2048]{1,0:T(8,128)(2,1)S(1)}, bf16[64,2048]{1,0:T(8,128)(2,1)}, u32[]{:S(2)}, u32[]{:S(2)}) collective-permute-start(bf16[64,2048]{1,0:T(8,128)(2,1)S(1)} %collective-permute-done.14.refs_2_), channel_id=1, source_target_pairs={{0,1},{1,0},{2,3},{3,2},{4,5},{5,4},{6,7},{7,6},{8,9},{9,8},{10,11... | collective-permute-start | bytes 786440 | tf_op jit(solution)/shard_map/ppermute | solution.py:38
  100.9 7.9 %collective-permute-start.17 = (bf16[64,2048]{1,0:T(8,128)(2,1)S(1)}, bf16[64,2048]{1,0:T(8,128)(2,1)}, u32[]{:S(2)}, u32[]{:S(2)}) collective-permute-start(bf16[64,2048]{1,0:T(8,128)(2,1)S(1)} %collective-permute-done.13.refs_1_), channel_id=1, source_target_pairs={{0,1},{1,0},{2,3},{3,2},{4,5},{5,4},{6,7},{7,6},{8,9},{9,8},{10,11... | collective-permute-start | bytes 786440 | tf_op jit(solution)/shard_map/ppermute | solution.py:38
  106.7 6.8 %collective-permute-start.31 = (bf16[16,1408]{1,0:T(8,128)(2,1)S(1)}, bf16[16,1408]{1,0:T(8,128)(2,1)S(1)}, u32[]{:S(2)}, u32[]{:S(2)}) collective-permute-start(bf16[16,1408]{1,0:T(8,128)(2,1)S(1)} %slice.15), channel_id=1, source_target_pairs={{0,8},{8,16},{16,24},{24,32},{32,40},{40,48},{48,56},{56,64},{64,7... | collective-permute-start | bytes 135176 | tf_op jit(solution)/shard_map/ppermute | solution.py:500
  117.8 5.7 %collective-permute-start.36 = (bf16[4,64,2048]{2,1,0:T(8,128)(2,1)S(1)}, bf16[4,64,2048]{2,1,0:T(8,128)(2,1)S(1)}, u32[]{:S(2)}, u32[]{:S(2)}) collective-permute-start(bf16[4,64,2048]{2,1,0:T(8,128)(2,1)S(1)} %get-tuple-element.97), channel_id=1, source_target_pairs={{0,1},{1,0},{2,3},{3,2},{4,5},{5,4},{6,7},{7,6},{8,9},{9,8},{10,11... | collective-permute-start | bytes 3145736 | tf_op jit(solution)/shard_map/ppermute | solution.py:38
  122.8 6.8 %collective-permute-start.32 = (bf16[4,64,2048]{2,1,0:T(8,128)(2,1)S(1)}, bf16[4,64,2048]{2,1,0:T(8,128)(2,1)S(1)}, u32[]{:S(2)}, u32[]{:S(2)}) collective-permute-start(bf16[4,64,2048]{2,1,0:T(8,128)(2,1)S(1)} %get-tuple-element.92), channel_id=1, source_target_pairs={{0,1},{1,0},{2,3},{3,2},{4,5},{5,4},{6,7},{7,6},{8,9},{9,8},{10,11... | collective-permute-start | bytes 3145736 | tf_op jit(solution)/shard_map/ppermute | solution.py:38
  124.2 10.1 %collective-permute-start.37 = (bf16[64,2048]{1,0:T(8,128)(2,1)S(1)}, bf16[64,2048]{1,0:T(8,128)(2,1)S(1)}, u32[]{:S(2)}, u32[]{:S(2)}) collective-permute-start(bf16[64,2048]{1,0:T(8,128)(2,1)S(1)} %get-tuple-element.98), channel_id=1, source_target_pairs={{0,2},{2,4},{4,6},{6,0},{1,3},{3,5},{5,7},{7,1},{8,10},{10,12},{12... | collective-permute-start | bytes 786440 | tf_op jit(solution)/shard_map/ppermute | solution.py:30
  126.8 14.5 %collective-permute-start.38 = (bf16[64,2048]{1,0:T(8,128)(2,1)S(1)}, bf16[64,2048]{1,0:T(8,128)(2,1)S(1)}, u32[]{:S(2)}, u32[]{:S(2)}) collective-permute-start(bf16[64,2048]{1,0:T(8,128)(2,1)S(1)} %get-tuple-element.99), channel_id=1, source_target_pairs={{0,4},{2,6},{4,0},{6,2},{1,5},{3,7},{5,1},{7,3},{8,12},{10,14},{12... | collective-permute-start | bytes 786440 | tf_op jit(solution)/shard_map/ppermute | solution.py:30
  128.5 12.8 %collective-permute-start.39 = (bf16[64,2048]{1,0:T(8,128)(2,1)S(1)}, bf16[64,2048]{1,0:T(8,128)(2,1)S(1)}, u32[]{:S(2)}, u32[]{:S(2)}) collective-permute-start(bf16[64,2048]{1,0:T(8,128)(2,1)S(1)} %get-tuple-element.100), channel_id=1, source_target_pairs={{0,6},{2,0},{4,2},{6,4},{1,7},{3,1},{5,3},{7,5},{8,14},{10,8},{12,... | collective-permute-start | bytes 786440 | tf_op jit(solution)/shard_map/ppermute | solution.py:30
  130.3 14.8 %collective-permute-start.33 = (bf16[64,2048]{1,0:T(8,128)(2,1)S(1)}, bf16[64,2048]{1,0:T(8,128)(2,1)S(1)}, u32[]{:S(2)}, u32[]{:S(2)}) collective-permute-start(bf16[64,2048]{1,0:T(8,128)(2,1)S(1)} %get-tuple-element.93), channel_id=1, source_target_pairs={{0,2},{2,4},{4,6},{6,0},{1,3},{3,5},{5,7},{7,1},{8,10},{10,12},{12... | collective-permute-start | bytes 786440 | tf_op jit(solution)/shard_map/ppermute | solution.py:30
  131.4 20.3 %collective-permute-start.34 = (bf16[64,2048]{1,0:T(8,128)(2,1)S(1)}, bf16[64,2048]{1,0:T(8,128)(2,1)S(1)}, u32[]{:S(2)}, u32[]{:S(2)}) collective-permute-start(bf16[64,2048]{1,0:T(8,128)(2,1)S(1)} %get-tuple-element.94), channel_id=1, source_target_pairs={{0,4},{2,6},{4,0},{6,2},{1,5},{3,7},{5,1},{7,3},{8,12},{10,14},{12... | collective-permute-start | bytes 786440 | tf_op jit(solution)/shard_map/ppermute | solution.py:30
  134.3 17.3 %collective-permute-start.35 = (bf16[64,2048]{1,0:T(8,128)(2,1)S(1)}, bf16[64,2048]{1,0:T(8,128)(2,1)S(1)}, u32[]{:S(2)}, u32[]{:S(2)}) collective-permute-start(bf16[64,2048]{1,0:T(8,128)(2,1)S(1)} %get-tuple-element.95), channel_id=1, source_target_pairs={{0,6},{2,0},{4,2},{6,4},{1,7},{3,1},{5,3},{7,5},{8,14},{10,8},{12,... | collective-permute-start | bytes 786440 | tf_op jit(solution)/shard_map/ppermute | solution.py:30
Sparse Core Ops, SparseCore 0:
  10.1 79.0 all-gather.1

commit v3 on v2

--- a/solution.py
+++ b/solution.py
@@ -223,16 +223,28 @@
     out[...] = jnp.concatenate(gated, axis=0)
 
 
-def heads_project_kernel(sc, gated, weight, keep, send):
-    place(keep, send, sc, sc[3] == 0, lambda cols: jnp.dot(gated[...], weight[:, cols], preferred_element_type=f32))
-
-
-def heads_kernel(sc, log, i0, i1, i2, i3, within, scaled, gate, weight, keep, send, start, carried, gated, chunk):
+def project(out, sc, own, active, product, tile=256):
+    n = out.shape[1]
+    core = sc[3] if own else 1 - sc[3]
+    rows = [active[pl.ds(pl.multiple_of((2 * chip + core) * n, n), n), :] for chip in range(4)]
+    rows = jnp.concatenate(rows, axis=0)
+    for j in range(out.shape[2] // tile):
+        cols = slice(j * tile, (j + 1) * tile)
+        part = product(rows, cols).astype(bf16)
+        for chip in range(4):
+            out[lax.rem(chip + 4 - sc[2], 4), :, cols] = part[chip * n : (chip + 1) * n]
+
+
+def heads_project_kernel(sc, gated, weight, out, own):
+    project(out, sc, own, gated, lambda rows, cols: jnp.dot(rows, weight[:, cols], preferred_element_type=f32))
+
+
+def heads_kernel(sc, log, i0, i1, i2, i3, within, scaled, gate, weight, gated, send, start, carried, chunk):
     gated_kernel(sc, log, i0, i1, i2, i3, within, scaled, gate, gated, start, carried, chunk)
-    heads_project_kernel(sc, gated, weight, keep, send)
-
-
-def place(keep, send, sc, south, product, tile=512):
+    heads_project_kernel(sc, gated, weight, send, False)
+
+
+def place(keep, send, sc, south, product, tile=256):
     n = keep.shape[1]
     for j in range(keep.shape[2] // tile):
         cols = slice(j * tile, (j + 1) * tile)
@@ -294,9 +306,9 @@
 
 
 def opening_kernel(sc, *refs):
-    sources, gate, value, down = refs[:5], *refs[5:8]
-    homes, shard = refs[8:13], refs[13]
-    gate_v, value_v, down_v, both, sems, weight_sems = refs[14:]
+    sources, gate, value, down = refs[:4], *refs[4:7]
+    homes, shard = refs[7:11], refs[11]
+    gate_v, value_v, down_v, both, sems, weight_sems = refs[12:]
     loads = [
         pltpu.make_async_copy(src, dst, weight_sems.at[i])
         for i, (src, dst) in enumerate(((gate, gate_v), (value, value_v), (down, down_v)))
@@ -442,14 +454,14 @@
 
     tables = jnp.asarray(trig_tables(dk // 2, 128, 128))
     padded = -(-3 * hidden // 128) * 128
-    near = (log_decay.T, query_proj, key_proj, value_proj, tables)
+    near = (log_decay.T, key_proj, value_proj, tables)
     column = ((hidden, up_gate.shape[0]), bf16)
-    log, query, key, value, tables, shard = run(
+    log, key, value, tables, shard = run(
         opening_kernel, sc, (*near, up_gate.T, up_value.T, down_weight),
         [(a.shape, a.dtype) for a in near] + [((up_gate.shape[0], padded), bf16)],
         scratch=[pltpu.VMEM(*column)] * 3
-        + [pltpu.VMEM((up_gate.shape[0], padded), bf16), pltpu.SemaphoreType.DMA((5,)), pltpu.SemaphoreType.DMA((4,))],
-        flops=1 << 26, far=8, far_outs=1,
+        + [pltpu.VMEM((up_gate.shape[0], padded), bf16), pltpu.SemaphoreType.DMA((4,)), pltpu.SemaphoreType.DMA((4,))],
+        flops=1 << 26, far=7, far_outs=1,
     )
     weights = lax.all_gather(shard, SP, axis=0, tiled=True)
     piece = ((dk // 4 + EXTRA, dv), bf16)
@@ -462,7 +474,7 @@
     )
     got = [pieces[0]] + [shift_by(pieces[d], "y", d) for d in (1, 2, 3)]
     within, scaled = run(
-        within_kernel, sc, (down_logs, across_logs, key_rot, cosine, sine, prefix, query, value),
+        within_kernel, sc, (down_logs, across_logs, key_rot, cosine, sine, prefix, query_proj, value),
         [((2, tok // 2, dv), f32), ((2, tok // 2, dk), bf16)],
         flops=4 * tok * BLOCK * (dk + dv),
     )
@@ -482,17 +494,17 @@
         sources = (log, *incoming, within, scaled, gates)
         scratch = [pltpu.VMEM((dk, dv), bf16), pltpu.VMEM((tok // 2, dv), f32)]
         gated = ((tok // 2, dv), bf16)
+        flops = tok * dv * width
+        side = lambda own: functools.partial(heads_project_kernel, own=own)
         if k == 0:
-            ready = run(
-                functools.partial(gated_kernel, chunk=k), sc, sources, [gated],
-                scratch=scratch, flops=tok * dv * dk,
-            )[0]
-            keep, send = run(heads_project_kernel, sc, (ready, out_weight), [shape, shape], flops=tok * dv * width)
+            ready = run(functools.partial(gated_kernel, chunk=0), sc, sources, [gated], scratch=scratch, flops=flops)[0]
+            send = run(side(False), sc, (ready, out_weight), [shape], flops=flops)[0]
         else:
-            keep, send = run(
-                functools.partial(heads_kernel, chunk=k), sc, (*sources, out_weight), [shape, shape],
-                scratch=scratch + [pltpu.VMEM(*gated)], flops=tok * dv * (dk + width),
+            ready, send = run(
+                functools.partial(heads_kernel, chunk=1), sc, (*sources, out_weight), [gated, shape],
+                scratch=scratch, flops=flops,
             )
+        keep = run(side(True), sc, (ready, out_weight), [shape], flops=flops)[0]
         normed[k] = reduce_and_norm(sc, keep, send, bases, norm_gain, norm_bias, 0, k)
         rows[k] = gather_rows(normed[k])
     ups[1], weights, down_weights = first_up(sc, rows[1], weights, 2 * hidden)

time: 161 us -> 162 us (level)
  waiting for transfers between devices: 52.8 us -> 56.7 us
  starting transfers between devices: 51.8 us -> 48 us
    ppermute x27, starting transfers between devices: 47 us -> 42.8 us  [shift_by(): return lax.ppermute(x, axis, ring(by))]
    ppermute x27, waiting for transfers between devices: 52.7 us -> 56.2 us  [shift_by(): return lax.ppermute(x, axis, ring(by))]
    pallas_call x21 -> x23, Pallas kernels: 41.5 us -> 43 us  [run(): pl.pallas_call(kernel, in_specs=[pl.BlockSpec(memory_space=pltpu.SMEM)] +...]
  transfers between devices with their start and end apart: 41 -> 41, of which waited for: 18 -> 21; matrix products, arithmetic and copies ran while one was open for 0% -> 0% of each run, Pallas kernels for 20% -> 21%
where the time goes in v3:
time: 162 us
  waiting for transfers between devices  56.7 us (35%)
  starting transfers between devices  48 us (30%)
  Pallas kernels  43 us (27%)
  between operations  13.8 us (9%)
    ppermute x27, waiting for transfers between devices, shift_by(): return lax.ppermute(x, axis, ring(by))  56.2 us
    pallas_call x23, Pallas kernels, run(): pl.pallas_call(kernel, in_specs=[pl.BlockSpec(memory_space=pltpu.SMEM)] +...  43 us
    ppermute x27, starting transfers between devices, shift_by(): return lax.ppermute(x, axis, ring(by))  42.8 us
  transfers between devices with their start and end apart: 41, of which 21 were waited for; matrix products, arithmetic and copies ran while one was open for 0% of the time, Pallas kernels for 21%

profile of v3, /device:TPU:0, one launch (start us, length us, event | category | flops | bytes accessed | tf_op | source)
XLA Modules:
  0.0 161.8 jit_solution(15366286250716225019)
XLA Ops:
  6.6 3.2 %shard_map.145 = (f32[1,1024]{1,0:T(1,128)S(1)}, bf16[1024,256]{1,0:T(8,128)(2,1)S(1)}, bf16[1024,512]{1,0:T(8,128)(2,1)S(1)}, f32[4,128,128]{2,1,0:T(8,128)S(1)}, bf16[128,2176]{1,0:T(8,128)(2,1)}) custom-call(s32[4]{0:T(128)S(1)} %pad_add_fusion.sc, f32[1,1024]{1,0:T(1,128)} %bitcast.23, bf16[1024,256]{1,0:T(8,128)(2,1)} %refs_1_.1, ...), custom_call_target="tpu_custom_call" | custom-call | flops 67108864 | tf_op jit(solution)/shard_map/pallas_call | solution.py:46
  9.8 2.3 %shard_map.146 = (bf16[1024,256]{1,0:T(8,128)(2,1)S(1)}, f32[1024,128]{1,0:T(8,128)S(1)}, f32[1024,128]{1,0:T(8,128)S(1)}, bf16[4,256,512]{2,1,0:T(8,128)(2,1)S(...) custom-call(s32[4]{0:T(128)S(1)} %pad_add_fusion.sc, ...), custom_call_target="tpu_custom_call" | custom-call | flops 536870912 | tf_op jit(solution)/shard_map/pallas_call | solution.py:46
  12.2 1.8 %collective-permute-start = (bf16[80,512]{1,0:T(8,128)(2,1)S(1)}, bf16[80,512]{1,0:T(8,128)(2,1)S(1)}, u32[]{:S(2)}, u32[]{:S(2)}) collective-permute-start(bf16[80,512]{1,0:T(8,128)(2,1)S(1)} %get-tuple-element.55), channel_id=1, source_target_pairs={{0,8},{8,16},{16,24},{24,0},{1,9},{9,17},{17,25},{25,1},{2,10},{10... | collective-permute-start | bytes 245768 | tf_op jit(solution)/shard_map/ppermute | solution.py:30
  13.9 2.9 %collective-permute-start.1 = (bf16[80,512]{1,0:T(8,128)(2,1)S(1)}, bf16[80,512]{1,0:T(8,128)(2,1)S(1)}, u32[]{:S(2)}, u32[]{:S(2)}) collective-permute-start(bf16[80,512]{1,0:T(8,128)(2,1)S(1)} %get-tuple-element.56), channel_id=1, source_target_pairs={{0,16},{8,24},{16,0},{24,8},{1,17},{9,25},{17,1},{25,9},{2,18},{10... | collective-permute-start | bytes 245768 | tf_op jit(solution)/shard_map/ppermute | solution.py:30
  16.8 1.4 collective-permute-start.2
  18.2 2.5 %collective-permute-done.1.r2 = bf16[80,512]{1,0:T(8,128)(2,1)S(1)} collective-permute-done((bf16[80,512]{1,0:T(8,128)(2,1)S(1)}, bf16[80,512]{1,0:T(8,128)(2,1)S(1)}, u32[]{:S(2)}, u32[]{:S(2)}) %collective-permute-start.1) | collective-permute-done | bytes 81952 | tf_op jit(solution)/shard_map/ppermute | solution.py:30
  20.7 0.5 collective-permute-done.2.r3
  21.3 0.7 shard_map.147
  21.9 2.0 %collective-permute-start.3 = (bf16[80,512]{1,0:T(8,128)(2,1)S(1)}, bf16[80,512]{1,0:T(8,128)(2,1)S(1)}, u32[]{:S(2)}, u32[]{:S(2)}) collective-permute-start(bf16[80,512]{1,0:T(8,128)(2,1)S(1)} %get-tuple-element.58), channel_id=1, source_target_pairs={{0,32},{32,64},{64,96},{96,0},{1,33},{33,65},{65,97},{97,1},{2,34}... | collective-permute-start | bytes 245768 | tf_op jit(solution)/shard_map/ppermute | solution.py:30
  23.9 3.6 %collective-permute-start.4 = (bf16[80,512]{1,0:T(8,128)(2,1)S(1)}, bf16[80,512]{1,0:T(8,128)(2,1)S(1)}, u32[]{:S(2)}, u32[]{:S(2)}) collective-permute-start(bf16[80,512]{1,0:T(8,128)(2,1)S(1)} %get-tuple-element.58), channel_id=1, source_target_pairs={{0,64},{32,96},{64,0},{96,32},{1,65},{33,97},{65,1},{97,33},{2,66}... | collective-permute-start | bytes 245768 | tf_op jit(solution)/shard_map/ppermute | solution.py:30
  27.5 1.0 collective-permute-start.5
  28.5 2.1 %collective-permute-done.3.t1 = bf16[80,512]{1,0:T(8,128)(2,1)S(1)} collective-permute-done((bf16[80,512]{1,0:T(8,128)(2,1)S(1)}, bf16[80,512]{1,0:T(8,128)(2,1)S(1)}, u32[]{:S(2)}, u32[]{:S(2)}) %collective-permute-start.3) | collective-permute-done | bytes 81952 | tf_op jit(solution)/shard_map/ppermute | solution.py:30
  30.7 4.2 %collective-permute-done.4.t2 = bf16[80,512]{1,0:T(8,128)(2,1)S(1)} collective-permute-done((bf16[80,512]{1,0:T(8,128)(2,1)S(1)}, bf16[80,512]{1,0:T(8,128)(2,1)S(1)}, u32[]{:S(2)}, u32[]{:S(2)}) %collective-permute-start.4) | collective-permute-done | bytes 81952 | tf_op jit(solution)/shard_map/ppermute | solution.py:30
  34.9 0.7 shard_map.148
  35.7 3.7 %collective-permute-start.7 = (bf16[64,512]{1,0:T(8,128)(2,1)S(1)}, bf16[64,512]{1,0:T(8,128)(2,1)S(1)}, u32[]{:S(2)}, u32[]{:S(2)}) collective-permute-start(bf16[64,512]{1,0:T(8,128)(2,1)S(1)} %get-tuple-element.63), channel_id=1, source_target_pairs={{0,16},{8,24},{16,0},{24,8},{1,17},{9,25},{17,1},{25,9},{2,18},{10... | collective-permute-start | bytes 196616 | tf_op jit(solution)/shard_map/ppermute | solution.py:30
  39.6 2.4 %shard_map.149 = (f32[2,512,512]{2,1,0:T(8,128)S(1)}, bf16[2,512,256]{2,1,0:T(8,128)(2,1)S(1)}) custom-call(s32[4]{0:T(128)S(1)} %pad_add_fusion.sc, f32[256,16]{1,0:T(8,128)S(1)} %get-tuple-element.65.down, f32[16,256]{1,0:T(8,128)S(1)} %get-tuple-element.66.across, bf16[1024,256]{1,0:T(8,128)(2,1)S(1)} %get-tuple-element.67.kr, ...), custom_call_target="tpu_custom_call" | custom-call | flops 805306368 | tf_op jit(solution)/shard_map/pallas_call | solution.py:46
  42.4 1.3 collective-permute-done.8.i3
  43.7 1.2 shard_map.150.gated
  44.9 1.3 shard_map.152
  46.3 2.0 %shard_map.155 = (bf16[512,512]{1,0:T(8,128)(2,1)S(1)}, bf16[4,64,2048]{2,1,0:T(8,128)(2,1)S(1)}) custom-call(s32[4]{0:T(128)S(1)} %pad_add_fusion.sc, f32[1,1024]{1,0:T(1,128)S(1)} %get-tuple-element.50.log, bf16[64,512]{1,0:T(8,128)(2,1)S(1)} %get-tuple-element.61.i0, bf16[64,512]{1,0:T(8,128)(2,1)S(1)} %collective-permute-done.6.i1, ...), custom_call_target="tpu_custom_call" | custom-call | flops 1073741824 | tf_op jit(solution)/shard_map/pallas_call | solution.py:46
  48.3 0.6 collective-permute-start.20
  48.8 1.2 shard_map.151.keep
  50.1 0.7 shard_map.153
  50.9 1.5 collective-permute-start.10
  52.4 2.8 %collective-permute-start.11 = (bf16[64,2048]{1,0:T(8,128)(2,1)S(1)}, bf16[64,2048]{1,0:T(8,128)(2,1)S(1)}, u32[]{:S(2)}, u32[]{:S(2)}) collective-permute-start(bf16[64,2048]{1,0:T(8,128)(2,1)S(1)} %get-tuple-element.74), channel_id=1, source_target_pairs={{0,4},{2,6},{4,0},{6,2},{1,5},{3,7},{5,1},{7,3},{8,12},{10,14},{12... | collective-permute-start | bytes 786440 | tf_op jit(solution)/shard_map/ppermute | solution.py:30
  55.2 1.4 collective-permute-start.12
  56.6 1.3 shard_map.156.keep
  57.9 0.7 shard_map.157
  58.6 0.7 collective-permute-start.21
  59.3 0.8 collective-permute-start.22
  60.4 2.5 %collective-permute-start.23 = (bf16[64,2048]{1,0:T(8,128)(2,1)S(1)}, bf16[64,2048]{1,0:T(8,128)(2,1)S(1)}, u32[]{:S(2)}, u32[]{:S(2)}) collective-permute-start(bf16[64,2048]{1,0:T(8,128)(2,1)S(1)} %get-tuple-element.80), channel_id=1, source_target_pairs={{0,6},{2,0},{4,2},{6,4},{1,7},{3,1},{5,3},{7,5},{8,14},{10,8},{12,... | collective-permute-start | bytes 786440 | tf_op jit(solution)/shard_map/ppermute | solution.py:30
  62.9 5.1 %collective-permute-done.11.r2 = bf16[64,2048]{1,0:T(8,128)(2,1)S(1)} collective-permute-done((bf16[64,2048]{1,0:T(8,128)(2,1)S(1)}, bf16[64,2048]{1,0:T(8,128)(2,1)S(1)}, u32[]{:S(2)}, u32[]{:S(2)}) %collective-permute-start.11) | collective-permute-done | bytes 262176 | tf_op jit(solution)/shard_map/ppermute | solution.py:30
  68.0 1.0 shard_map.154.refs_0_
  69.0 2.3 %collective-permute-start.13 = (bf16[64,2048]{1,0:T(8,128)(2,1)S(1)}, bf16[64,2048]{1,0:T(8,128)(2,1)S(1)}, u32[]{:S(2)}, u32[]{:S(2)}) collective-permute-start(bf16[64,2048]{1,0:T(8,128)(2,1)S(1)} %shard_map.154.refs_0_), channel_id=1, source_target_pairs={{0,2},{2,4},{4,6},{6,0},{1,3},{3,5},{5,7},{7,1},{8,10},{10,12},{12... | collective-permute-start | bytes 786440 | tf_op jit(solution)/shard_map/ppermute | solution.py:30
  71.3 1.8 %collective-permute-start.14 = (bf16[64,2048]{1,0:T(8,128)(2,1)S(1)}, bf16[64,2048]{1,0:T(8,128)(2,1)S(1)}, u32[]{:S(2)}, u32[]{:S(2)}) collective-permute-start(bf16[64,2048]{1,0:T(8,128)(2,1)S(1)} %shard_map.154.refs_0_), channel_id=1, source_target_pairs={{0,4},{2,6},{4,0},{6,2},{1,5},{3,7},{5,1},{7,3},{8,12},{10,14},{12... | collective-permute-start | bytes 786440 | tf_op jit(solution)/shard_map/ppermute | solution.py:30
  73.3 5.9 %collective-permute-done.22.r2 = bf16[64,2048]{1,0:T(8,128)(2,1)S(1)} collective-permute-done((bf16[64,2048]{1,0:T(8,128)(2,1)S(1)}, bf16[64,2048]{1,0:T(8,128)(2,1)S(1)}, u32[]{:S(2)}, u32[]{:S(2)}) %collective-permute-start.22) | collective-permute-done | bytes 262176 | tf_op jit(solution)/shard_map/ppermute | solution.py:30
  79.3 0.9 shard_map.158.refs_0_
  80.3 0.7 collective-permute-start.24
  81.0 3.1 %collective-permute-start.25 = (bf16[64,2048]{1,0:T(8,128)(2,1)S(1)}, bf16[64,2048]{1,0:T(8,128)(2,1)S(1)}, u32[]{:S(2)}, u32[]{:S(2)}) collective-permute-start(bf16[64,2048]{1,0:T(8,128)(2,1)S(1)} %shard_map.158.refs_0_), channel_id=1, source_target_pairs={{0,4},{2,6},{4,0},{6,2},{1,5},{3,7},{5,1},{7,3},{8,12},{10,14},{12... | collective-permute-start | bytes 786440 | tf_op jit(solution)/shard_map/ppermute | solution.py:30
  84.1 1.7 %collective-permute-start.26 = (bf16[64,2048]{1,0:T(8,128)(2,1)S(1)}, bf16[64,2048]{1,0:T(8,128)(2,1)S(1)}, u32[]{:S(2)}, u32[]{:S(2)}) collective-permute-start(bf16[64,2048]{1,0:T(8,128)(2,1)S(1)} %shard_map.158.refs_0_), channel_id=1, source_target_pairs={{0,6},{2,0},{4,2},{6,4},{1,7},{3,1},{5,3},{7,5},{8,14},{10,8},{12,... | collective-permute-start | bytes 786440 | tf_op jit(solution)/shard_map/ppermute | solution.py:30
  85.9 4.7 %collective-permute-done.14.refs_2_ = bf16[64,2048]{1,0:T(8,128)(2,1)S(1)} collective-permute-done((bf16[64,2048]{1,0:T(8,128)(2,1)S(1)}, bf16[64,2048]{1,0:T(8,128)(2,1)S(1)}, u32[]{:S(2)}, u32[]{:S(2)}) %collective-permute-start.14) | collective-permute-done | bytes 262176 | tf_op jit(solution)/shard_map/ppermute | solution.py:30
  90.6 4.7 %collective-permute-done.24.refs_1_ = bf16[64,2048]{1,0:T(8,128)(2,1)S(1)} collective-permute-done((bf16[64,2048]{1,0:T(8,128)(2,1)S(1)}, bf16[64,2048]{1,0:T(8,128)(2,1)S(1)}, u32[]{:S(2)}, u32[]{:S(2)}) %collective-permute-start.24) | collective-permute-done | bytes 262176 | tf_op jit(solution)/shard_map/ppermute | solution.py:30
  95.2 5.6 %collective-permute-done.25.refs_2_ = bf16[64,2048]{1,0:T(8,128)(2,1)S(1)} collective-permute-done((bf16[64,2048]{1,0:T(8,128)(2,1)S(1)}, bf16[64,2048]{1,0:T(8,128)(2,1)S(1)}, u32[]{:S(2)}, u32[]{:S(2)}) %collective-permute-start.25) | collective-permute-done | bytes 262176 | tf_op jit(solution)/shard_map/ppermute | solution.py:30
  100.9 0.5 collective-permute-start.30
  102.8 5.7 %shard_map.159 = (bf16[512,1408]{1,0:T(8,128)(2,1)S(1)}, bf16[2048,1408]{1,0:T(8,128)(2,1)S(1)}, bf16[2048,768]{1,0:T(8,128)(2,1)S(1)}) custom-call(s32[4]{0:T(128)S(1)} %pad_add_fusion.sc, bf16[64,2048]{1,0:T(8,128)(2,1)S(1)} %shard_map.158.refs_0_, bf16[64,2048]{1,0:T(8,128)(2,1)S(1)} %collective-permute-done.24.refs_1_, ...), custom_call_target="tpu_custom_call" | custom-call | flops 2952790016 | tf_op jit(solution)/shard_map/pallas_call | solution.py:46
  108.5 2.4 %collective-permute-start.31 = (bf16[16,1408]{1,0:T(8,128)(2,1)S(1)}, bf16[16,1408]{1,0:T(8,128)(2,1)S(1)}, u32[]{:S(2)}, u32[]{:S(2)}) collective-permute-start(bf16[16,1408]{1,0:T(8,128)(2,1)S(1)} %slice.15), channel_id=1, source_target_pairs={{0,8},{8,16},{16,24},{24,32},{32,40},{40,48},{48,56},{56,64},{64,7... | collective-permute-start | bytes 135176 | tf_op jit(solution)/shard_map/ppermute | solution.py:512
  110.9 4.6 %shard_map.160.mine.other = bf16[512,1408]{1,0:T(8,128)(2,1)S(1)} custom-call(s32[4]{0:T(128)S(1)} %pad_add_fusion.sc, bf16[64,2048]{1,0:T(8,128)(2,1)S(1)} %shard_map.154.refs_0_, bf16[64,2048]{1,0:T(8,128)(2,1)S(1)} %collective-permute-done.13.refs_1_, bf16[64,2048]{1,0:T(8,128)(2,1)S(1)} %collective-permute-done.14.refs_2_, ...), custom_call_target="tpu_custom_call" | custom-call | flops 2952790016 | tf_op jit(solution)/shard_map/pallas_call | solution.py:46
  115.6 4.2 %shard_map.164 = (bf16[4,64,2048]{2,1,0:T(8,128)(2,1)S(1)}, bf16[4,64,2048]{2,1,0:T(8,128)(2,1)S(1)}) custom-call(s32[4]{0:T(128)S(1)} %pad_add_fusion.sc, bf16[512,1408]{1,0:T(8,128)(2,1)S(1)} %get-tuple-element.83.other.mine, bf16[512,1408]{1,0:T(8,128)(2,1)S(1)} %shard_map.160.mine.other, bf16[16,1408]{1,0:T(8,128)(2,1)S(1)} %collective-permute-done.31.edge, ...), custom_call_target="tpu_custom_call" | custom-call | flops 2952790016 | tf_op jit(solution)/shard_map/pallas_call | solution.py:46
  120.1 2.4 %shard_map.161.active = bf16[512,704]{1,0:T(8,128)(2,1)S(1)} custom-call(s32[4]{0:T(128)S(1)} %pad_add_fusion.sc, bf16[512,1408]{1,0:T(8,128)(2,1)S(1)} %shard_map.160.mine.other, bf16[512,1408]{1,0:T(8,128)(2,1)S(1)} %get-tuple-element.83.other.mine, bf16[16,1408]{1,0:T(8,128)(2,1)S(1)} %collective-permute-done.31.edge, ...), custom_call_target="tpu_custom_call" | custom-call | flops 1476395008 | tf_op jit(solution)/shard_map/pallas_call | solution.py:46
  122.5 2.4 %shard_map.162 = (bf16[4,64,2048]{2,1,0:T(8,128)(2,1)S(1)}, bf16[4,64,2048]{2,1,0:T(8,128)(2,1)S(1)}) custom-call(s32[4]{0:T(128)S(1)} %pad_add_fusion.sc, bf16[512,704]{1,0:T(8,128)(2,1)S(1)} %shard_map.161.active, bf16[2048,768]{1,0:T(8,128)(2,1)S(1)} %get-tuple-element.84.weight), custom_call_target="tpu_custom_call" | custom-call | flops 1476395008 | tf_op jit(solution)/shard_map/pallas_call | solution.py:46
  124.9 0.6 collective-permute-start.32
  125.5 0.7 shard_map.165
  126.2 1.1 collective-permute-start.37
  127.4 2.4 %collective-permute-start.38 = (bf16[64,2048]{1,0:T(8,128)(2,1)S(1)}, bf16[64,2048]{1,0:T(8,128)(2,1)S(1)}, u32[]{:S(2)}, u32[]{:S(2)}) collective-permute-start(bf16[64,2048]{1,0:T(8,128)(2,1)S(1)} %get-tuple-element.93), channel_id=1, source_target_pairs={{0,4},{2,6},{4,0},{6,2},{1,5},{3,7},{5,1},{7,3},{8,12},{10,14},{12... | collective-permute-start | bytes 786440 | tf_op jit(solution)/shard_map/ppermute | solution.py:30
  129.8 0.9 collective-permute-start.39
  130.6 0.7 shard_map.163
  131.4 1.2 collective-permute-start.33
  132.6 1.1 collective-permute-start.34
  133.7 8.3 %collective-permute-done.37.r1 = bf16[64,2048]{1,0:T(8,128)(2,1)S(1)} collective-permute-done((bf16[64,2048]{1,0:T(8,128)(2,1)S(1)}, bf16[64,2048]{1,0:T(8,128)(2,1)S(1)}, u32[]{:S(2)}, u32[]{:S(2)}) %collective-permute-start.37) | collective-permute-done | bytes 262176 | tf_op jit(solution)/shard_map/ppermute | solution.py:30
  142.6 0.7 collective-permute-done.39.r3
  143.2 1.0 shard_map.166.rest_0_
  144.2 3.5 %collective-permute-done.33.r1 = bf16[64,2048]{1,0:T(8,128)(2,1)S(1)} collective-permute-done((bf16[64,2048]{1,0:T(8,128)(2,1)S(1)}, bf16[64,2048]{1,0:T(8,128)(2,1)S(1)}, u32[]{:S(2)}, u32[]{:S(2)}) %collective-permute-start.33) | collective-permute-done | bytes 262176 | tf_op jit(solution)/shard_map/ppermute | solution.py:30
  147.7 5.2 %collective-permute-done.34.r2 = bf16[64,2048]{1,0:T(8,128)(2,1)S(1)} collective-permute-done((bf16[64,2048]{1,0:T(8,128)(2,1)S(1)}, bf16[64,2048]{1,0:T(8,128)(2,1)S(1)}, u32[]{:S(2)}, u32[]{:S(2)}) %collective-permute-start.34) | collective-permute-done | bytes 262176 | tf_op jit(solution)/shard_map/ppermute | solution.py:30
  153.3 1.7 %shard_map.167 = bf16[128,2048]{1,0:T(8,128)(2,1)} custom-call(s32[4]{0:T(128)S(1)} %pad_add_fusion.sc, bf16[4,64,2048]{2,1,0:T(8,128)(2,1)S(1)} %get-tuple-element.85.keep, bf16[4,64,2048]{2,1,0:T(8,128)(2,1)S(1)} %collective-permute-done.32.got, bf16[64,2048]{1,0:T(8,128)(2,1)S(1)} %collective-permute-done.33.r1, ...), custom_call_target="tpu_custom_call" | custom-call | flops 52428800 | tf_op jit(solution)/shard_map/pallas_call | solution.py:46
  (65 shorter events, 4.2 us)
Async XLA Ops:
  6.5 33.0 %copy-start.3 = (bf16[1024,256]{1,0:T(8,128)(2,1)S(1)}, bf16[1024,256]{1,0:T(8,128)(2,1)}, u32[]{:S(2)}) copy-start(bf16[1024,256]{1,0:T(8,128)(2,1)} %q.1) | copy-start | bytes 1572868
  6.5 96.2 %all-gather.2.cloned.1.call-start = ((), (), s32[]{:S(2)}) async-start(), calls=%async_computation | async-start | bytes 9469952 | tf_op jit(solution)/shard_map/all_gather | solution.py:466
  12.1 31.5 %copy-start.1 = (bf16[1024,512]{1,0:T(8,128)(2,1)S(1)}, bf16[1024,512]{1,0:T(8,128)(2,1)}, u32[]{:S(2)}) copy-start(bf16[1024,512]{1,0:T(8,128)(2,1)} %param.18) | copy-start | bytes 3145732
  12.2 6.0 %collective-permute-start = (bf16[80,512]{1,0:T(8,128)(2,1)S(1)}, bf16[80,512]{1,0:T(8,128)(2,1)S(1)}, u32[]{:S(2)}, u32[]{:S(2)}) collective-permute-start(bf16[80,512]{1,0:T(8,128)(2,1)S(1)} %get-tuple-element.55), channel_id=1, source_target_pairs={{0,8},{8,16},{16,24},{24,0},{1,9},{9,17},{17,25},{25,1},{2,10},{10... | collective-permute-start | bytes 245768 | tf_op jit(solution)/shard_map/ppermute | solution.py:30
  13.9 6.8 %collective-permute-start.1 = (bf16[80,512]{1,0:T(8,128)(2,1)S(1)}, bf16[80,512]{1,0:T(8,128)(2,1)S(1)}, u32[]{:S(2)}, u32[]{:S(2)}) collective-permute-start(bf16[80,512]{1,0:T(8,128)(2,1)S(1)} %get-tuple-element.56), channel_id=1, source_target_pairs={{0,16},{8,24},{16,0},{24,8},{1,17},{9,25},{17,1},{25,9},{2,18},{10... | collective-permute-start | bytes 245768 | tf_op jit(solution)/shard_map/ppermute | solution.py:30
  16.8 4.4 %collective-permute-start.2 = (bf16[80,512]{1,0:T(8,128)(2,1)S(1)}, bf16[80,512]{1,0:T(8,128)(2,1)S(1)}, u32[]{:S(2)}, u32[]{:S(2)}) collective-permute-start(bf16[80,512]{1,0:T(8,128)(2,1)S(1)} %get-tuple-element.57), channel_id=1, source_target_pairs={{0,24},{8,0},{16,8},{24,16},{1,25},{9,1},{17,9},{25,17},{2,26},{10... | collective-permute-start | bytes 245768 | tf_op jit(solution)/shard_map/ppermute | solution.py:30
  21.9 8.7 %collective-permute-start.3 = (bf16[80,512]{1,0:T(8,128)(2,1)S(1)}, bf16[80,512]{1,0:T(8,128)(2,1)S(1)}, u32[]{:S(2)}, u32[]{:S(2)}) collective-permute-start(bf16[80,512]{1,0:T(8,128)(2,1)S(1)} %get-tuple-element.58), channel_id=1, source_target_pairs={{0,32},{32,64},{64,96},{96,0},{1,33},{33,65},{65,97},{97,1},{2,34}... | collective-permute-start | bytes 245768 | tf_op jit(solution)/shard_map/ppermute | solution.py:30
  23.9 10.9 %collective-permute-start.4 = (bf16[80,512]{1,0:T(8,128)(2,1)S(1)}, bf16[80,512]{1,0:T(8,128)(2,1)S(1)}, u32[]{:S(2)}, u32[]{:S(2)}) collective-permute-start(bf16[80,512]{1,0:T(8,128)(2,1)S(1)} %get-tuple-element.58), channel_id=1, source_target_pairs={{0,64},{32,96},{64,0},{96,32},{1,65},{33,97},{65,1},{97,33},{2,66}... | collective-permute-start | bytes 245768 | tf_op jit(solution)/shard_map/ppermute | solution.py:30
  27.5 7.4 %collective-permute-start.5 = (bf16[80,512]{1,0:T(8,128)(2,1)S(1)}, bf16[80,512]{1,0:T(8,128)(2,1)S(1)}, u32[]{:S(2)}, u32[]{:S(2)}) collective-permute-start(bf16[80,512]{1,0:T(8,128)(2,1)S(1)} %get-tuple-element.58), channel_id=1, source_target_pairs={{0,96},{32,0},{64,32},{96,64},{1,97},{33,1},{65,33},{97,65},{2,98}... | collective-permute-start | bytes 245768 | tf_op jit(solution)/shard_map/ppermute | solution.py:30
  35.6 6.4 %collective-permute-start.6 = (bf16[64,512]{1,0:T(8,128)(2,1)S(1)}, bf16[64,512]{1,0:T(8,128)(2,1)S(1)}, u32[]{:S(2)}, u32[]{:S(2)}) collective-permute-start(bf16[64,512]{1,0:T(8,128)(2,1)S(1)} %get-tuple-element.62), channel_id=1, source_target_pairs={{0,8},{8,16},{16,24},{24,0},{1,9},{9,17},{17,25},{25,1},{2,10},{10... | collective-permute-start | bytes 196616 | tf_op jit(solution)/shard_map/ppermute | solution.py:30
  35.7 6.6 %collective-permute-start.7 = (bf16[64,512]{1,0:T(8,128)(2,1)S(1)}, bf16[64,512]{1,0:T(8,128)(2,1)S(1)}, u32[]{:S(2)}, u32[]{:S(2)}) collective-permute-start(bf16[64,512]{1,0:T(8,128)(2,1)S(1)} %get-tuple-element.63), channel_id=1, source_target_pairs={{0,16},{8,24},{16,0},{24,8},{1,17},{9,25},{17,1},{25,9},{2,18},{10... | collective-permute-start | bytes 196616 | tf_op jit(solution)/shard_map/ppermute | solution.py:30
  39.4 4.3 %collective-permute-start.8 = (bf16[64,512]{1,0:T(8,128)(2,1)S(1)}, bf16[64,512]{1,0:T(8,128)(2,1)S(1)}, u32[]{:S(2)}, u32[]{:S(2)}) collective-permute-start(bf16[64,512]{1,0:T(8,128)(2,1)S(1)} %get-tuple-element.64), channel_id=1, source_target_pairs={{0,24},{8,0},{16,8},{24,16},{1,25},{9,1},{17,9},{25,17},{2,26},{10... | collective-permute-start | bytes 196616 | tf_op jit(solution)/shard_map/ppermute | solution.py:30
  41.9 3.0 %copy-start.2 = (bf16[512,2048]{1,0:T(8,128)(2,1)S(1)}, bf16[512,2048]{1,0:T(8,128)(2,1)}, u32[]{:S(2)}) copy-start(bf16[512,2048]{1,0:T(8,128)(2,1)} %weight.7) | copy-start | bytes 6291460
  46.2 3.9 %collective-permute-start.9 = (bf16[4,64,2048]{2,1,0:T(8,128)(2,1)S(1)}, bf16[4,64,2048]{2,1,0:T(8,128)(2,1)S(1)}, u32[]{:S(2)}, u32[]{:S(2)}) collective-permute-start(bf16[4,64,2048]{2,1,0:T(8,128)(2,1)S(1)} %shard_map.152), channel_id=1, source_target_pairs={{0,1},{1,0},{2,3},{3,2},{4,5},{5,4},{6,7},{7,6},{8,9},{9,8},{10,11... | collective-permute-start | bytes 3145736 | tf_op jit(solution)/shard_map/ppermute | solution.py:38
  48.3 9.6 %collective-permute-start.20 = (bf16[4,64,2048]{2,1,0:T(8,128)(2,1)S(1)}, bf16[4,64,2048]{2,1,0:T(8,128)(2,1)S(1)}, u32[]{:S(2)}, u32[]{:S(2)}) collective-permute-start(bf16[4,64,2048]{2,1,0:T(8,128)(2,1)S(1)} %get-tuple-element.77), channel_id=1, source_target_pairs={{0,1},{1,0},{2,3},{3,2},{4,5},{5,4},{6,7},{7,6},{8,9},{9,8},{10,11... | collective-permute-start | bytes 3145736 | tf_op jit(solution)/shard_map/ppermute | solution.py:38
  50.8 12.1 %copy-start.6 = (f32[2,3,704]{2,0,1:T(2,128)S(1)}, f32[2,3,704]{2,0,1:T(2,128)}, u32[]{:S(2)}) copy-start(f32[2,3,704]{2,0,1:T(2,128)} %param.26) | copy-start | bytes 50692
  50.8 17.2 %copy-start = (bf16[1024,2048]{1,0:T(8,128)(2,1)S(1)}, bf16[1024,2048]{1,0:T(8,128)(2,1)}, u32[]{:S(2)}) copy-start(bf16[1024,2048]{1,0:T(8,128)(2,1)} %param.20) | copy-start | bytes 12582916
  50.8 17.2 %copy-start.4 = (f32[2,2048]{1,0:T(2,128)S(1)}, f32[2,2048]{1,0:T(2,128)}, u32[]{:S(2)}) copy-start(f32[2,2048]{1,0:T(2,128)} %gain.7) | copy-start | bytes 49156
  50.9 17.2 %copy-start.5 = (f32[2,2048]{1,0:T(2,128)S(1)}, f32[2,2048]{1,0:T(2,128)}, u32[]{:S(2)}) copy-start(f32[2,2048]{1,0:T(2,128)} %shift.7) | copy-start | bytes 49156
  50.9 9.5 %collective-permute-start.10 = (bf16[64,2048]{1,0:T(8,128)(2,1)S(1)}, bf16[64,2048]{1,0:T(8,128)(2,1)S(1)}, u32[]{:S(2)}, u32[]{:S(2)}) collective-permute-start(bf16[64,2048]{1,0:T(8,128)(2,1)S(1)} %get-tuple-element.73), channel_id=1, source_target_pairs={{0,2},{2,4},{4,6},{6,0},{1,3},{3,5},{5,7},{7,1},{8,10},{10,12},{12... | collective-permute-start | bytes 786440 | tf_op jit(solution)/shard_map/ppermute | solution.py:30
  52.4 15.6 %collective-permute-start.11 = (bf16[64,2048]{1,0:T(8,128)(2,1)S(1)}, bf16[64,2048]{1,0:T(8,128)(2,1)S(1)}, u32[]{:S(2)}, u32[]{:S(2)}) collective-permute-start(bf16[64,2048]{1,0:T(8,128)(2,1)S(1)} %get-tuple-element.74), channel_id=1, source_target_pairs={{0,4},{2,6},{4,0},{6,2},{1,5},{3,7},{5,1},{7,3},{8,12},{10,14},{12... | collective-permute-start | bytes 786440 | tf_op jit(solution)/shard_map/ppermute | solution.py:30
  55.2 12.8 %collective-permute-start.12 = (bf16[64,2048]{1,0:T(8,128)(2,1)S(1)}, bf16[64,2048]{1,0:T(8,128)(2,1)S(1)}, u32[]{:S(2)}, u32[]{:S(2)}) collective-permute-start(bf16[64,2048]{1,0:T(8,128)(2,1)S(1)} %get-tuple-element.75), channel_id=1, source_target_pairs={{0,6},{2,0},{4,2},{6,4},{1,7},{3,1},{5,3},{7,5},{8,14},{10,8},{12,... | collective-permute-start | bytes 786440 | tf_op jit(solution)/shard_map/ppermute | solution.py:30
  58.6 14.7 %collective-permute-start.21 = (bf16[64,2048]{1,0:T(8,128)(2,1)S(1)}, bf16[64,2048]{1,0:T(8,128)(2,1)S(1)}, u32[]{:S(2)}, u32[]{:S(2)}) collective-permute-start(bf16[64,2048]{1,0:T(8,128)(2,1)S(1)} %get-tuple-element.78), channel_id=1, source_target_pairs={{0,2},{2,4},{4,6},{6,0},{1,3},{3,5},{5,7},{7,1},{8,10},{10,12},{12... | collective-permute-start | bytes 786440 | tf_op jit(solution)/shard_map/ppermute | solution.py:30
  59.3 20.0 %collective-permute-start.22 = (bf16[64,2048]{1,0:T(8,128)(2,1)S(1)}, bf16[64,2048]{1,0:T(8,128)(2,1)S(1)}, u32[]{:S(2)}, u32[]{:S(2)}) collective-permute-start(bf16[64,2048]{1,0:T(8,128)(2,1)S(1)} %get-tuple-element.79), channel_id=1, source_target_pairs={{0,4},{2,6},{4,0},{6,2},{1,5},{3,7},{5,1},{7,3},{8,12},{10,14},{12... | collective-permute-start | bytes 786440 | tf_op jit(solution)/shard_map/ppermute | solution.py:30
  60.4 18.9 %collective-permute-start.23 = (bf16[64,2048]{1,0:T(8,128)(2,1)S(1)}, bf16[64,2048]{1,0:T(8,128)(2,1)S(1)}, u32[]{:S(2)}, u32[]{:S(2)}) collective-permute-start(bf16[64,2048]{1,0:T(8,128)(2,1)S(1)} %get-tuple-element.80), channel_id=1, source_target_pairs={{0,6},{2,0},{4,2},{6,4},{1,7},{3,1},{5,3},{7,5},{8,14},{10,8},{12,... | collective-permute-start | bytes 786440 | tf_op jit(solution)/shard_map/ppermute | solution.py:30
  69.0 16.8 %copy-start.7 = (f32[2,704]{1,0:T(2,128)S(1)}, f32[2,704]{1,0:T(2,128)}, u32[]{:S(2)}) copy-start(f32[2,704]{1,0:T(2,128)} %param.27) | copy-start | bytes 16900
  69.0 16.8 %collective-permute-start.13 = (bf16[64,2048]{1,0:T(8,128)(2,1)S(1)}, bf16[64,2048]{1,0:T(8,128)(2,1)S(1)}, u32[]{:S(2)}, u32[]{:S(2)}) collective-permute-start(bf16[64,2048]{1,0:T(8,128)(2,1)S(1)} %shard_map.154.refs_0_), channel_id=1, source_target_pairs={{0,2},{2,4},{4,6},{6,0},{1,3},{3,5},{5,7},{7,1},{8,10},{10,12},{12... | collective-permute-start | bytes 786440 | tf_op jit(solution)/shard_map/ppermute | solution.py:30
  71.3 19.2 %collective-permute-start.14 = (bf16[64,2048]{1,0:T(8,128)(2,1)S(1)}, bf16[64,2048]{1,0:T(8,128)(2,1)S(1)}, u32[]{:S(2)}, u32[]{:S(2)}) collective-permute-start(bf16[64,2048]{1,0:T(8,128)(2,1)S(1)} %shard_map.154.refs_0_), channel_id=1, source_target_pairs={{0,4},{2,6},{4,0},{6,2},{1,5},{3,7},{5,1},{7,3},{8,12},{10,14},{12... | collective-permute-start | bytes 786440 | tf_op jit(solution)/shard_map/ppermute | solution.py:30
  80.3 15.0 %collective-permute-start.24 = (bf16[64,2048]{1,0:T(8,128)(2,1)S(1)}, bf16[64,2048]{1,0:T(8,128)(2,1)S(1)}, u32[]{:S(2)}, u32[]{:S(2)}) collective-permute-start(bf16[64,2048]{1,0:T(8,128)(2,1)S(1)} %shard_map.158.refs_0_), channel_id=1, source_target_pairs={{0,2},{2,4},{4,6},{6,0},{1,3},{3,5},{5,7},{7,1},{8,10},{10,12},{12... | collective-permute-start | bytes 786440 | tf_op jit(solution)/shard_map/ppermute | solution.py:30
  81.0 19.9 %collective-permute-start.25 = (bf16[64,2048]{1,0:T(8,128)(2,1)S(1)}, bf16[64,2048]{1,0:T(8,128)(2,1)S(1)}, u32[]{:S(2)}, u32[]{:S(2)}) collective-permute-start(bf16[64,2048]{1,0:T(8,128)(2,1)S(1)} %shard_map.158.refs_0_), channel_id=1, source_target_pairs={{0,4},{2,6},{4,0},{6,2},{1,5},{3,7},{5,1},{7,3},{8,12},{10,14},{12... | collective-permute-start | bytes 786440 | tf_op jit(solution)/shard_map/ppermute | solution.py:30
  84.1 16.8 %collective-permute-start.26 = (bf16[64,2048]{1,0:T(8,128)(2,1)S(1)}, bf16[64,2048]{1,0:T(8,128)(2,1)S(1)}, u32[]{:S(2)}, u32[]{:S(2)}) collective-permute-start(bf16[64,2048]{1,0:T(8,128)(2,1)S(1)} %shard_map.158.refs_0_), channel_id=1, source_target_pairs={{0,6},{2,0},{4,2},{6,4},{1,7},{3,1},{5,3},{7,5},{8,14},{10,8},{12,... | collective-permute-start | bytes 786440 | tf_op jit(solution)/shard_map/ppermute | solution.py:30
  85.8 15.7 %collective-permute-start.15 = (bf16[64,2048]{1,0:T(8,128)(2,1)S(1)}, bf16[64,2048]{1,0:T(8,128)(2,1)S(1)}, u32[]{:S(2)}, u32[]{:S(2)}) collective-permute-start(bf16[64,2048]{1,0:T(8,128)(2,1)S(1)} %shard_map.154.refs_0_), channel_id=1, source_target_pairs={{0,6},{2,0},{4,2},{6,4},{1,7},{3,1},{5,3},{7,5},{8,14},{10,8},{12,... | collective-permute-start | bytes 786440 | tf_op jit(solution)/shard_map/ppermute | solution.py:30
  90.6 11.0 %collective-permute-start.27 = (bf16[64,2048]{1,0:T(8,128)(2,1)S(1)}, bf16[64,2048]{1,0:T(8,128)(2,1)S(1)}, u32[]{:S(2)}, u32[]{:S(2)}) collective-permute-start(bf16[64,2048]{1,0:T(8,128)(2,1)S(1)} %shard_map.158.refs_0_), channel_id=1, source_target_pairs={{0,1},{1,0},{2,3},{3,2},{4,5},{5,4},{6,7},{7,6},{8,9},{9,8},{10,11... | collective-permute-start | bytes 786440 | tf_op jit(solution)/shard_map/ppermute | solution.py:38
  95.2 6.8 %collective-permute-start.28 = (bf16[64,2048]{1,0:T(8,128)(2,1)S(1)}, bf16[64,2048]{1,0:T(8,128)(2,1)S(1)}, u32[]{:S(2)}, u32[]{:S(2)}) collective-permute-start(bf16[64,2048]{1,0:T(8,128)(2,1)S(1)} %collective-permute-done.24.refs_1_), channel_id=1, source_target_pairs={{0,1},{1,0},{2,3},{3,2},{4,5},{5,4},{6,7},{7,6},{8,9},{9,8},{10,11... | collective-permute-start | bytes 786440 | tf_op jit(solution)/shard_map/ppermute | solution.py:38
  100.9 1.5 collective-permute-start.29
  100.9 1.9 %collective-permute-start.30 = (bf16[64,2048]{1,0:T(8,128)(2,1)S(1)}, bf16[64,2048]{1,0:T(8,128)(2,1)S(1)}, u32[]{:S(2)}, u32[]{:S(2)}) collective-permute-start(bf16[64,2048]{1,0:T(8,128)(2,1)S(1)} %collective-permute-done.26.refs_3_), channel_id=1, source_target_pairs={{0,1},{1,0},{2,3},{3,2},{4,5},{5,4},{6,7},{7,6},{8,9},{9,8},{10,11... | collective-permute-start | bytes 786440 | tf_op jit(solution)/shard_map/ppermute | solution.py:38
  101.5 9.3 %collective-permute-start.16 = (bf16[64,2048]{1,0:T(8,128)(2,1)S(1)}, bf16[64,2048]{1,0:T(8,128)(2,1)S(1)}, u32[]{:S(2)}, u32[]{:S(2)}) collective-permute-start(bf16[64,2048]{1,0:T(8,128)(2,1)S(1)} %shard_map.154.refs_0_), channel_id=1, source_target_pairs={{0,1},{1,0},{2,3},{3,2},{4,5},{5,4},{6,7},{7,6},{8,9},{9,8},{10,11... | collective-permute-start | bytes 786440 | tf_op jit(solution)/shard_map/ppermute | solution.py:38
  101.6 9.3 %collective-permute-start.17 = (bf16[64,2048]{1,0:T(8,128)(2,1)S(1)}, bf16[64,2048]{1,0:T(8,128)(2,1)}, u32[]{:S(2)}, u32[]{:S(2)}) collective-permute-start(bf16[64,2048]{1,0:T(8,128)(2,1)S(1)} %collective-permute-done.13.refs_1_), channel_id=1, source_target_pairs={{0,1},{1,0},{2,3},{3,2},{4,5},{5,4},{6,7},{7,6},{8,9},{9,8},{10,11... | collective-permute-start | bytes 786440 | tf_op jit(solution)/shard_map/ppermute | solution.py:38
  102.1 8.8 %collective-permute-start.18 = (bf16[64,2048]{1,0:T(8,128)(2,1)S(1)}, bf16[64,2048]{1,0:T(8,128)(2,1)}, u32[]{:S(2)}, u32[]{:S(2)}) collective-permute-start(bf16[64,2048]{1,0:T(8,128)(2,1)S(1)} %collective-permute-done.14.refs_2_), channel_id=1, source_target_pairs={{0,1},{1,0},{2,3},{3,2},{4,5},{5,4},{6,7},{7,6},{8,9},{9,8},{10,11... | collective-permute-start | bytes 786440 | tf_op jit(solution)/shard_map/ppermute | solution.py:38
  102.4 8.5 %collective-permute-start.19 = (bf16[64,2048]{1,0:T(8,128)(2,1)S(1)}, bf16[64,2048]{1,0:T(8,128)(2,1)}, u32[]{:S(2)}, u32[]{:S(2)}) collective-permute-start(bf16[64,2048]{1,0:T(8,128)(2,1)S(1)} %collective-permute-done.15.refs_3_), channel_id=1, source_target_pairs={{0,1},{1,0},{2,3},{3,2},{4,5},{5,4},{6,7},{7,6},{8,9},{9,8},{10,11... | collective-permute-start | bytes 786440 | tf_op jit(solution)/shard_map/ppermute | solution.py:38
  108.5 7.1 %collective-permute-start.31 = (bf16[16,1408]{1,0:T(8,128)(2,1)S(1)}, bf16[16,1408]{1,0:T(8,128)(2,1)S(1)}, u32[]{:S(2)}, u32[]{:S(2)}) collective-permute-start(bf16[16,1408]{1,0:T(8,128)(2,1)S(1)} %slice.15), channel_id=1, source_target_pairs={{0,8},{8,16},{16,24},{24,32},{32,40},{40,48},{48,56},{56,64},{64,7... | collective-permute-start | bytes 135176 | tf_op jit(solution)/shard_map/ppermute | solution.py:512
  119.8 5.7 %collective-permute-start.36 = (bf16[4,64,2048]{2,1,0:T(8,128)(2,1)S(1)}, bf16[4,64,2048]{2,1,0:T(8,128)(2,1)S(1)}, u32[]{:S(2)}, u32[]{:S(2)}) collective-permute-start(bf16[4,64,2048]{2,1,0:T(8,128)(2,1)S(1)} %get-tuple-element.91), channel_id=1, source_target_pairs={{0,1},{1,0},{2,3},{3,2},{4,5},{5,4},{6,7},{7,6},{8,9},{9,8},{10,11... | collective-permute-start | bytes 3145736 | tf_op jit(solution)/shard_map/ppermute | solution.py:38
  124.9 5.7 %collective-permute-start.32 = (bf16[4,64,2048]{2,1,0:T(8,128)(2,1)S(1)}, bf16[4,64,2048]{2,1,0:T(8,128)(2,1)S(1)}, u32[]{:S(2)}, u32[]{:S(2)}) collective-permute-start(bf16[4,64,2048]{2,1,0:T(8,128)(2,1)S(1)} %get-tuple-element.86), channel_id=1, source_target_pairs={{0,1},{1,0},{2,3},{3,2},{4,5},{5,4},{6,7},{7,6},{8,9},{9,8},{10,11... | collective-permute-start | bytes 3145736 | tf_op jit(solution)/shard_map/ppermute | solution.py:38
  126.2 15.8 %collective-permute-start.37 = (bf16[64,2048]{1,0:T(8,128)(2,1)S(1)}, bf16[64,2048]{1,0:T(8,128)(2,1)S(1)}, u32[]{:S(2)}, u32[]{:S(2)}) collective-permute-start(bf16[64,2048]{1,0:T(8,128)(2,1)S(1)} %get-tuple-element.92), channel_id=1, source_target_pairs={{0,2},{2,4},{4,6},{6,0},{1,3},{3,5},{5,7},{7,1},{8,10},{10,12},{12... | collective-permute-start | bytes 786440 | tf_op jit(solution)/shard_map/ppermute | solution.py:30
  127.4 15.2 %collective-permute-start.38 = (bf16[64,2048]{1,0:T(8,128)(2,1)S(1)}, bf16[64,2048]{1,0:T(8,128)(2,1)S(1)}, u32[]{:S(2)}, u32[]{:S(2)}) collective-permute-start(bf16[64,2048]{1,0:T(8,128)(2,1)S(1)} %get-tuple-element.93), channel_id=1, source_target_pairs={{0,4},{2,6},{4,0},{6,2},{1,5},{3,7},{5,1},{7,3},{8,12},{10,14},{12... | collective-permute-start | bytes 786440 | tf_op jit(solution)/shard_map/ppermute | solution.py:30
  129.8 13.5 %collective-permute-start.39 = (bf16[64,2048]{1,0:T(8,128)(2,1)S(1)}, bf16[64,2048]{1,0:T(8,128)(2,1)S(1)}, u32[]{:S(2)}, u32[]{:S(2)}) collective-permute-start(bf16[64,2048]{1,0:T(8,128)(2,1)S(1)} %get-tuple-element.94), channel_id=1, source_target_pairs={{0,6},{2,0},{4,2},{6,4},{1,7},{3,1},{5,3},{7,5},{8,14},{10,8},{12,... | collective-permute-start | bytes 786440 | tf_op jit(solution)/shard_map/ppermute | solution.py:30
  131.4 16.3 %collective-permute-start.33 = (bf16[64,2048]{1,0:T(8,128)(2,1)S(1)}, bf16[64,2048]{1,0:T(8,128)(2,1)S(1)}, u32[]{:S(2)}, u32[]{:S(2)}) collective-permute-start(bf16[64,2048]{1,0:T(8,128)(2,1)S(1)} %get-tuple-element.87), channel_id=1, source_target_pairs={{0,2},{2,4},{4,6},{6,0},{1,3},{3,5},{5,7},{7,1},{8,10},{10,12},{12... | collective-permute-start | bytes 786440 | tf_op jit(solution)/shard_map/ppermute | solution.py:30
  132.6 20.3 %collective-permute-start.34 = (bf16[64,2048]{1,0:T(8,128)(2,1)S(1)}, bf16[64,2048]{1,0:T(8,128)(2,1)S(1)}, u32[]{:S(2)}, u32[]{:S(2)}) collective-permute-start(bf16[64,2048]{1,0:T(8,128)(2,1)S(1)} %get-tuple-element.88), channel_id=1, source_target_pairs={{0,4},{2,6},{4,0},{6,2},{1,5},{3,7},{5,1},{7,3},{8,12},{10,14},{12... | collective-permute-start | bytes 786440 | tf_op jit(solution)/shard_map/ppermute | solution.py:30
  142.1 11.2 %collective-permute-start.35 = (bf16[64,2048]{1,0:T(8,128)(2,1)S(1)}, bf16[64,2048]{1,0:T(8,128)(2,1)S(1)}, u32[]{:S(2)}, u32[]{:S(2)}) collective-permute-start(bf16[64,2048]{1,0:T(8,128)(2,1)S(1)} %get-tuple-element.89), channel_id=1, source_target_pairs={{0,6},{2,0},{4,2},{6,4},{1,7},{3,1},{5,3},{7,5},{8,14},{10,8},{12,... | collective-permute-start | bytes 786440 | tf_op jit(solution)/shard_map/ppermute | solution.py:30
Sparse Core Ops, SparseCore 0:
  9.9 77.5 all-gather.1
